TPU v7x, 256 devices: a whole 4x4x8 slice. The times are simulated.
256 devices in a mesh: sp: 16 (over y, x), tp: 16 (over z, core).
Axes of the slice: x: 4, y: 4, z: 8, core: 2. Of those that a mesh axis runs over, the one named last changes fastest.
Arguments:
- conv_outer: bfloat16 [2048, 4096], P('tp', 'sp'), may hold values from -6 to 6
- conv_inner: bfloat16 [2048, 4096], P('tp', 'sp'), may hold values from -6 to 6
- conv_input: bfloat16 [2048, 4096], P('tp', 'sp'), may hold values from -6 to 6
- conv_taps: float32 [3, 2048], P(None, 'tp'), may hold values from -3 to 3
- out_proj: bfloat16 [2048, 4096], P('tp'), may hold values from -0.125 to 0.125
- mixed_state: bfloat16 [4096, 4096], P('sp', 'tp'), may hold values from -6 to 6
- route_ids: int32 [4096, 2], P('sp'), may hold values from 0 to 15, all different within a row; in each aligned block of 256 rows (0 to 255, 256 to 511, ...) at most 64 rows name the same one
- route_weights: float32 [4096, 2], P('sp'), may hold values from 0.1 to 1
- w_gate: bfloat16 [16, 2048, 4096], P('sp', 'tp'), may hold values from -0.09375 to 0.09375
- w_up: bfloat16 [16, 2048, 4096], P('sp', 'tp'), may hold values from -0.09375 to 0.09375
- w_down: bfloat16 [16, 2048, 4096], P('sp', 'tp'), may hold values from -0.125 to 0.125
- cotangent: bfloat16 [4096, 4096], P('sp', 'tp'), may hold values from -8 to 8
Outputs:
- grad_gate: float32 [16, 2048, 4096], P('sp', 'tp')
- grad_up: float32 [16, 2048, 4096], P('sp', 'tp')
- grad_down: float32 [16, 2048, 4096], P('sp', 'tp')
- grad_mixed: bfloat16 [4096, 4096], P('sp', 'tp')
- grad_proj: float32 [2048, 4096], P('tp', 'sp')
- grad_outer: bfloat16 [2048, 4096], P('tp', 'sp')
- grad_inner: bfloat16 [2048, 4096], P('tp', 'sp')
- grad_input: bfloat16 [2048, 4096], P('tp', 'sp')
Inputs may be any that keep to these rules, and one draw needn't show every extreme that they name: `route_ids`: each row names 2 different experts; among the tokens of one index of sp no expert is named more than 64 times, a bound that some block reaches.
All inputs are finite; a program needn't handle non-finite values.
Results may differ from a plain program's by a relative error of at most 0.022.
Values may be sent and summed in bfloat16 or wider, within the bound.
No kernel may reach another device: no remote copies, remote signals or barrier semaphores. Data moves between devices by JAX's collectives and lax.ppermute only.
A program may use at most 128 MiB of HBM per device.

v0:
```python
import jax
import jax.numpy as jnp
from jax import lax
from jax.sharding import Mesh
from jax.sharding import PartitionSpec as P

TP = ("tp_0", "tp_1")


def sent_together(arrays, axis, split_dim, concat_dim, along):
    both = jnp.concatenate(arrays, axis=along)
    whole, at, finished = (
        lax.all_to_all(both, axis, split_axis=split_dim, concat_axis=concat_dim, tiled=True),
        0,
        [],
    )
    for a in arrays:
        finished.append(lax.slice_in_dim(whole, at, at + a.shape[along], axis=along))
        at += a.shape[along]
    return tuple(finished)


def in_one_piece(arrays, axis, dim, along):
    both = jnp.concatenate(arrays, axis=along)
    whole, at, finished = (lax.all_gather(both, axis, axis=dim, tiled=True), 0, [])
    for a in arrays:
        finished.append(lax.slice_in_dim(whole, at, at + a.shape[along], axis=along))
        at += a.shape[along]
    return tuple(finished)


def from_behind(value, axis, steps):
    count = lax.axis_size(axis)
    first, last = (max(0, -steps), min(count, count - steps))
    return lax.ppermute(value, axis, [(source, source + steps) for source in range(first, last)])


def whole_of(shard, axes, dim):
    for axis in reversed(axes):
        shard = lax.all_gather(shard, axis, axis=dim, tiled=True)
    return shard


def split_up(shard, dim, size):
    shape = shard.shape
    blocks = shard.reshape(*shape[:dim], size, shape[dim] // size, *shape[dim + 1 :])
    return jnp.moveaxis(blocks, dim, 0)


def summed_on_arrival(shard, axis, dim):
    size = lax.axis_size(axis)
    blocks = lax.all_to_all(split_up(shard, dim, size), axis, 0, 0, tiled=True)
    return jnp.sum(blocks.astype(jnp.float32), axis=0)


def expert_step(rows_in, rows_grad, gate_w, up_w, down_w):
    gate_pre = jnp.einsum("rd,fd->rf", rows_in, gate_w, preferred_element_type=jnp.float32)
    up_pre = jnp.einsum("rd,fd->rf", rows_in, up_w, preferred_element_type=jnp.float32)
    sig_gate = jax.nn.sigmoid(gate_pre)
    silu_gate = gate_pre * sig_gate
    hidden = (silu_gate * up_pre).astype(jnp.bfloat16)
    back_hidden = jnp.einsum("rd,fd->rf", rows_grad, down_w, preferred_element_type=jnp.float32)
    back_gate = (back_hidden * up_pre * sig_gate * (1.0 + gate_pre * (1.0 - sig_gate))).astype(
        jnp.bfloat16
    )
    back_up = (back_hidden * silu_gate).astype(jnp.bfloat16)
    grad_down_e = jnp.einsum("rf,rd->fd", hidden, rows_grad, preferred_element_type=jnp.float32)
    grad_gate_e = jnp.einsum("rf,rd->fd", back_gate, rows_in, preferred_element_type=jnp.float32)
    grad_up_e = jnp.einsum("rf,rd->fd", back_up, rows_in, preferred_element_type=jnp.float32)
    partial_value = jnp.dot(back_gate, gate_w, preferred_element_type=jnp.float32) + jnp.dot(
        back_up, up_w, preferred_element_type=jnp.float32
    )
    return (partial_value, grad_gate_e, grad_up_e, grad_down_e)


def shards(
    conv_outer,
    conv_inner,
    conv_input,
    conv_taps,
    out_proj,
    mixed_state,
    route_ids,
    route_weights,
    w_gate,
    w_up,
    w_down,
    cotangent,
):
    tok_count = mixed_state.shape[0]
    col_count = mixed_state.shape[1]
    top_count = route_ids.shape[1]
    sp_size = lax.axis_size("sp")
    local_experts = w_gate.shape[0]
    experts = local_experts * sp_size
    capacity = 4 * tok_count // experts
    flat_ids = route_ids.reshape(-1)
    onehot = (flat_ids[:, None] == jnp.arange(experts, dtype=jnp.int32)[None, :]).astype(jnp.int32)
    slot_pos = jnp.sum(jnp.cumsum(onehot, axis=0) * onehot, axis=1) - 1
    slot_dest = flat_ids * capacity + slot_pos
    token_of = jnp.arange(flat_ids.shape[0], dtype=jnp.int32) // top_count
    scale_flat = route_weights.reshape(-1)[:, None]

    def pack_rows(rows):
        buffer = jnp.zeros((experts * capacity, rows.shape[1]), rows.dtype).at[slot_dest].set(rows)
        return buffer.reshape(sp_size, local_experts, capacity, rows.shape[1])

    sent_state = pack_rows(mixed_state[token_of])
    sent_grad = pack_rows(
        (cotangent[token_of].astype(jnp.float32) * scale_flat).astype(jnp.bfloat16)
    )
    recv_state, recv_grad = sent_together((sent_state, sent_grad), "sp", 0, 0, 1)
    state_rows, grad_rows = in_one_piece((recv_state[:, 0], recv_grad[:, 0]), TP, 2, 0)
    width = state_rows.shape[2]
    rows_in = state_rows.reshape(-1, width)
    rows_grad = grad_rows.reshape(-1, width)
    partial_value, grad_gate_e, grad_up_e, grad_down_e = expert_step(
        rows_in, rows_grad, w_gate[0], w_up[0], w_down[0]
    )
    summed = lax.psum_scatter(
        partial_value.astype(jnp.bfloat16), TP, scatter_dimension=1, tiled=True
    )
    back_rows = summed.reshape(sp_size, capacity, col_count)
    arrived = lax.all_to_all(
        back_rows[:, None], "sp", split_axis=0, concat_axis=0, tiled=True
    ).reshape(experts * capacity, col_count)
    picked = arrived[slot_dest].astype(jnp.float32).reshape(tok_count, top_count, col_count)
    grad_mixed = (cotangent.astype(jnp.float32) + jnp.sum(picked, axis=1)).astype(jnp.bfloat16)
    taps_count = conv_taps.shape[0]
    rim_width = taps_count - 1
    head_block = from_behind(
        jnp.stack([conv_inner[:, tok_count - rim_width :], conv_input[:, tok_count - rim_width :]]),
        "sp",
        1,
    )
    inner_ext = jnp.concatenate([head_block[0], conv_inner], axis=1).astype(jnp.float32)
    input_ext = jnp.concatenate([head_block[1], conv_input], axis=1).astype(jnp.float32)
    inner_prod = inner_ext * input_ext
    conv_out = jnp.zeros((conv_inner.shape[0], tok_count), jnp.float32)
    for offset in range(taps_count):
        conv_out = (
            conv_out + conv_taps[offset][:, None] * inner_prod[:, offset : offset + tok_count]
        )
    outer_f = conv_outer.astype(jnp.float32)
    mixer_act = (outer_f * conv_out).astype(jnp.bfloat16)
    full_back = whole_of(grad_mixed, TP, 1)
    back_mixer = jnp.einsum("cd,td->ct", out_proj, full_back, preferred_element_type=jnp.float32)
    proj_term = jnp.dot(mixer_act, full_back, preferred_element_type=jnp.float32)
    grad_proj = summed_on_arrival(proj_term.astype(jnp.bfloat16), "sp", 1)
    grad_outer = (back_mixer * conv_out).astype(jnp.bfloat16)
    back_conv = back_mixer * outer_f
    tail_back = from_behind(back_conv[:, :rim_width], "sp", -1)
    back_ext = jnp.concatenate([back_conv, tail_back], axis=1)
    back_prod = jnp.zeros_like(back_conv)
    for offset in range(taps_count):
        shift_by = rim_width - offset
        back_prod = (
            back_prod + conv_taps[offset][:, None] * back_ext[:, shift_by : shift_by + tok_count]
        )
    grad_inner = (back_prod * conv_input.astype(jnp.float32)).astype(jnp.bfloat16)
    grad_input = (back_prod * conv_inner.astype(jnp.float32)).astype(jnp.bfloat16)
    return (
        grad_gate_e[None],
        grad_up_e[None],
        grad_down_e[None],
        grad_mixed,
        grad_proj,
        grad_outer,
        grad_inner,
        grad_input,
    )


def solution(mesh):
    torus = Mesh(mesh.devices.reshape(mesh.shape["sp"], 8, 2), ("sp", "tp_0", "tp_1"))
    return jax.shard_map(
        shards,
        mesh=torus,
        in_specs=(
            P(TP, "sp"),
            P(TP, "sp"),
            P(TP, "sp"),
            P(None, TP),
            P(TP, None),
            P("sp", TP),
            P("sp", None),
            P("sp", None),
            P("sp", TP, None),
            P("sp", TP, None),
            P("sp", TP, None),
            P("sp", TP),
        ),
        out_specs=(
            P("sp", TP, None),
            P("sp", TP, None),
            P("sp", TP, None),
            P("sp", TP),
            P(TP, "sp"),
            P(TP, "sp"),
            P(TP, "sp"),
            P(TP, "sp"),
        ),
        check_vma=False,
    )
```

profile of v0, /device:TPU:24, one launch (start us, length us, event | category | flops | bytes accessed | tf_op | source)
XLA Modules:
  0.0 345.1 jit_solution(3194688719886497391)
XLA Ops:
  7.2 0.0 copy-start
  7.2 0.0 all-gather.3.cloned.1.call-start
  7.2 0.8 broadcast_multiply_fusion
  8.0 0.8 copy.46
  8.8 0.1 eq.25
  9.0 0.1 eq.29
  9.1 0.1 copy.45
  9.3 0.1 mul.118
  9.4 1.2 reduce-window.6
  10.6 0.2 slice_reduce_fusion
  10.8 0.1 fusion.27
  10.9 0.8 copy.49
  11.8 0.1 mul.120
  11.9 5.8 %scatter_custom_fusion = bf16[1024,256]{1,0:T(8,128)(2,1)S(1)} fusion(s32[512]{0:T(512)S(1)} %bitcast.100, bf16[256,256]{1,0:T(8,128)(2,1)} %param.17, s32[1024]{0:T(1024)S(1)} %pad_clamp_fusion.1, bf16[]{:T(256)} %constant.27.clone.1), kind=kCustom, calls=%fused_computation.33 | custom fusion | bytes 524800 | tf_op jit(solution)/shard_map/scatter | solution.py:105
  17.7 5.9 %scatter_custom_fusion.1 = bf16[1024,256]{1,0:T(8,128)(2,1)S(1)} fusion(s32[512]{0:T(512)S(1)} %bitcast.101, f32[512]{0:T(512)S(1)} %mul.120, bf16[]{:T(256)} %constant.27.clone.1, bf16[256,256]{1,0:T(8,128)(2,1)} %param.23, s32[1024]{0:T(1024)S(1)} %pad_clamp_fusion.1), kind=kCustom, calls=%fused_computation.32 | custom fusion | flops 393216 | bytes 661506 | tf_op jit(solution)/shard_map/scatter | solution.py:105
  23.6 0.1 pad_maximum_fusion
  23.7 21.8 %all_to_all.15 = bf16[16,2,64,256]{3,2,1,0:T(8,128)(2,1)S(1)} all-to-all(bf16[16,2,64,256]{3,2,1,0:T(8,128)(2,1)S(1)} %pad_maximum_fusion), channel_id=1, replica_groups=mesh['sp'=16,'tp_0'=8,'tp_1'=2] {'sp'}, dimensions={0} | all-to-all | bytes 2097152 | tf_op jit(solution)/shard_map/all_to_all | solution.py:13
  45.5 0.1 slice_bitcast_fusion.1
  45.6 1.1 pad_maximum_fusion.1
  46.7 0.0 all-gather.3.cloned.1.call-update
  46.7 0.2 reduce-scatter.2.cloned.1.call-start
  46.9 102.5 %all-gather.3.cloned.1.call-done = bf16[32,64,4096]{2,1,0:T(8,128)(2,1)} async-done(((bf16[32,64,256]{2,1,0:T(8,128)(2,1)}), bf16[32,64,4096]{2,1,0:T(8,128)(2,1)}) %all-gather.3.cloned.1.call-update) | async-done | bytes 16777232 | tf_op jit(solution)/shard_map/all_gather | solution.py:25
  149.4 6.9 %fusion.33 = (bf16[16,64,4096]{2,1,0:T(8,128)(2,1)S(1)}, bf16[16,64,4096]{2,1,0:T(8,128)(2,1)S(1)}) fusion(bf16[32,64,4096]{2,1,0:T(8,128)(2,1)} %all-gather.3.cloned.1.call-done), kind=kLoop, calls=%fused_computation.87 | loop fusion | bytes 33554432 | tf_op jit(solution)/shard_map/slice | solution.py:27
  156.3 0.0 copy-start.4
  156.3 2.3 fusion.2
  158.7 0.0 copy-start.12
  158.7 2.3 fusion.5
  161.0 1.3 copy-done.3
  162.4 2.4 multiply_convert_fusion.1
  164.8 8.1 %fusion = f32[1024,4096]{1,0:T(8,128)} fusion(bf16[1024,128]{1,0:T(8,128)(2,1)S(1)} %get-tuple-element.39, bf16[1,128,4096]{2,1,0:T(8,128)(2,1)S(1)} %copy-done), kind=kOutput, calls=%fused_computation.15 | convolution fusion | flops 1073741824 | bytes 18087936 | tf_op jit(solution)/shard_map/dot_general | solution.py:70
  172.8 11.3 %add_convert_fusion = bf16[1024,4096]{1,0:T(8,128)(2,1)} fusion(f32[1024,4096]{1,0:T(8,128)} %fusion, bf16[1024,128]{1,0:T(8,128)(2,1)S(1)} %get-tuple-element.38, bf16[1,128,4096]{2,1,0:T(8,128)(2,1)S(1)} %copy-done.4), kind=kOutput, calls=%fused_computation.5 | convolution fusion | flops 1082130432 | bytes 26476544 | tf_op jit(solution)/shard_map/dot_general | solution.py:70
  184.2 0.0 copy-start.10
  184.2 0.0 reduce-scatter.2.cloned.1.call-update
  184.2 69.2 %reduce-scatter.2.cloned.1.call-done = bf16[1024,256]{1,0:T(8,128)(2,1)} async-done(((bf16[1024,4096]{1,0:T(8,128)(2,1)}), bf16[1024,256]{1,0:T(8,128)(2,1)}) %reduce-scatter.2.cloned.1.call-update) | async-done | bytes 524304 | tf_op jit(solution)/shard_map/reduce_scatter | solution.py:120
  253.3 7.2 %all-to-all-start.1 = ((bf16[16,1,64,256]{3,2,1,0:T(8,128)(2,1)}), bf16[16,1,64,256]{3,2,1,0:T(8,128)(2,1)S(1)}, u32[]{:S(2)}, u32[]{:S(2)}) async-start(bf16[16,1,64,256]{3,2,1,0:T(8,128)(2,1)} %bitcast.99), calls=%async_computation.2 | async-start | bytes 1048576 | tf_op jit(solution)/shard_map/all_to_all | solution.py:124
  260.6 0.0 all-gather.5.cloned.1.call-start
  260.6 7.8 %all-to-all-done.1 = bf16[16,1,64,256]{3,2,1,0:T(8,128)(2,1)S(1)} async-done(((bf16[16,1,64,256]{3,2,1,0:T(8,128)(2,1)}), bf16[16,1,64,256]{3,2,1,0:T(8,128)(2,1)S(1)}, u32[]{:S(2)}, u32[]{:S(2)}) %all-to-all-start.1) | async-done | bytes 524320 | tf_op jit(solution)/shard_map/all_to_all | solution.py:124
  268.4 1.9 gather_fusion
  270.4 0.3 reshape.143
  270.6 0.6 reduce_sum.28
  271.3 0.0 copy-start.6
  271.3 2.1 all_gather.10
  273.4 0.0 all-gather.5.cloned.1.call-update
  273.5 0.1 copy.53
  273.6 0.1 copy.54
  273.7 2.5 collective-permute-start
  276.3 0.1 copy.52
  276.4 4.9 %collective-permute-done = bf16[2,128,2]{1,2,0:T(2,128)(2,1)S(1)} collective-permute-done((bf16[2,128,2]{1,2,0:T(2,128)(2,1)S(1)}, bf16[2,128,2]{1,2,0:T(2,128)(2,1)S(1)}, u32[]{:S(2)}, u32[]{:S(2)}) %collective-permute-start) | collective-permute-done | bytes 1056 | tf_op jit(solution)/shard_map/ppermute | solution.py:35
  281.4 6.1 %convolution_bitcast_fusion.2 = f32[1,128,4096]{2,1,0:T(8,128)} fusion(bf16[1024,128]{1,0:T(8,128)(2,1)S(1)} %get-tuple-element.39, bf16[1024,4096]{1,0:T(8,128)(2,1)} %bitcast.91), kind=kOutput, calls=%fused_computation.8 | convolution fusion | flops 1073741824 | bytes 10747904 | tf_op jit(solution)/shard_map/rf,rd->fd/dot_general | solution.py:68
  287.5 6.2 %convolution_bitcast_fusion = f32[1,128,4096]{2,1,0:T(8,128)} fusion(bf16[1024,4096]{1,0:T(8,128)(2,1)} %bitcast.94, f32[1024,128]{1,0:T(8,128)S(1)} %fusion.5, f32[1024,128]{1,0:T(8,128)S(1)} %fusion.2), kind=kOutput, calls=%fused_computation.6 | convolution fusion | flops 1074528256 | bytes 11534336 | tf_op jit(solution)/shard_map/rf,rd->fd/dot_general | solution.py:67
  293.6 18.2 %all-gather.5.cloned.1.call-done = bf16[256,4096]{1,0:T(8,128)(2,1)} async-done(((bf16[256,512]{1,0:T(8,128)(2,1)}), bf16[256,4096]{1,0:T(8,128)(2,1)}) %all-gather.5.cloned.1.call-update) | async-done | bytes 2097168 | tf_op jit(solution)/shard_map/all_gather | solution.py:40
  311.8 2.3 multiply_convert_fusion.8
  314.1 2.1 convolution_convert_fusion
  316.2 1.1 copy.68
  317.3 7.2 %all-to-all-start.2 = ((bf16[16,128,256]{2,1,0:T(8,128)(2,1)}), bf16[16,128,256]{2,1,0:T(8,128)(2,1)S(1)}, u32[]{:S(2)}, u32[]{:S(2)}) async-start(bf16[16,128,256]{2,1,0:T(8,128)(2,1)} %bitcast.88), calls=%async_computation.3 | async-start | bytes 2097152 | tf_op jit(solution)/shard_map/all_to_all | solution.py:52
  324.5 5.0 %collective-permute-start.1 = (f32[128,2]{0,1:T(2,128)S(1)}, f32[128,2]{0,1:T(2,128)S(1)}, u32[]{:S(2)}, u32[]{:S(2)}) collective-permute-start(f32[128,2]{0,1:T(2,128)S(1)} %slice.97), channel_id=1, source_target_pairs={{16,0},{32,16},{48,32},{64,48},{80,64},{96,80},{112,96},{128,112},... | collective-permute-start | bytes 3080 | tf_op jit(solution)/shard_map/ppermute | solution.py:35
  329.5 6.0 %convolution_bitcast_fusion.1 = f32[1,128,4096]{2,1,0:T(8,128)} fusion(bf16[1024,128]{1,0:T(8,128)(2,1)S(1)} %get-tuple-element.38, bf16[1024,4096]{1,0:T(8,128)(2,1)} %bitcast.92), kind=kOutput, calls=%fused_computation.7 | convolution fusion | flops 1073741824 | bytes 10747904 | tf_op jit(solution)/shard_map/rf,rd->fd/dot_general | solution.py:69
  335.5 0.7 copy.60
  336.2 0.0 collective-permute-done.1
  336.2 0.1 multiply_convert_fusion.6
  336.3 0.7 copy.61
  337.1 0.7 copy.62
  337.8 0.0 all-to-all-done.2
  337.8 0.8 convert_reduce_fusion
  (36 shorter events, 0.2 us)
Async XLA Ops:
  7.2 149.2 %copy-start = (bf16[1,128,4096]{2,1,0:T(8,128)(2,1)S(1)}, bf16[1,128,4096]{2,1,0:T(8,128)(2,1)}, u32[]{:S(2)}) copy-start(bf16[1,128,4096]{2,1,0:T(8,128)(2,1)} %param.20) | copy-start | bytes 3145732
  7.2 142.2 %all-gather.3.cloned.1.call-start = ((), (), s32[]{:S(2)}) async-start(), calls=%async_computation.4 | async-start | bytes 17825792 | tf_op jit(solution)/shard_map/all_gather | solution.py:25
  46.7 206.7 %reduce-scatter.2.cloned.1.call-start = ((), (), s32[]{:S(2)}) async-start(), calls=%async_computation.5 | async-start | bytes 8912896 | tf_op jit(solution)/shard_map/reduce_scatter | solution.py:120
  156.3 4.7 %copy-start.2 = (bf16[16,64,4096]{2,1,0:T(8,128)(2,1)}, bf16[16,64,4096]{2,1,0:T(8,128)(2,1)S(1)}, u32[]{:S(2)}) copy-start(bf16[16,64,4096]{2,1,0:T(8,128)(2,1)S(1)} %get-tuple-element.37) | copy-start | bytes 25165828
  156.3 6.1 %copy-start.3 = (bf16[16,64,4096]{2,1,0:T(8,128)(2,1)}, bf16[16,64,4096]{2,1,0:T(8,128)(2,1)S(1)}, u32[]{:S(2)}) copy-start(bf16[16,64,4096]{2,1,0:T(8,128)(2,1)S(1)} %get-tuple-element.36) | copy-start | bytes 25165828
  156.3 2.4 copy-start.4
  158.7 3.7 %copy-start.12 = (bf16[1,128,4096]{2,1,0:T(8,128)(2,1)S(1)}, bf16[1,128,4096]{2,1,0:T(8,128)(2,1)}, u32[]{:S(2)}) copy-start(bf16[1,128,4096]{2,1,0:T(8,128)(2,1)} %param.22) | copy-start | bytes 3145732
  184.1 87.1 %copy-start.7 = (bf16[256,256]{1,0:T(8,128)(2,1)S(1)}, bf16[256,256]{1,0:T(8,128)(2,1)}, u32[]{:S(2)}) copy-start(bf16[256,256]{1,0:T(8,128)(2,1)} %param.23) | copy-start | bytes 393220
  184.1 89.3 %copy-start.8 = (bf16[128,256]{1,0:T(8,128)(2,1)S(1)}, bf16[128,256]{1,0:T(8,128)(2,1)}, u32[]{:S(2)}) copy-start(bf16[128,256]{1,0:T(8,128)(2,1)} %param.13) | copy-start | bytes 196612
  184.1 89.4 %copy-start.9 = (bf16[128,256]{1,0:T(8,128)(2,1)S(1)}, bf16[128,256]{1,0:T(8,128)(2,1)}, u32[]{:S(2)}) copy-start(bf16[128,256]{1,0:T(8,128)(2,1)} %param.14) | copy-start | bytes 196612
  184.2 92.1 %copy-start.11 = (f32[3,128]{1,0:T(4,128)S(1)}, f32[3,128]{1,0:T(4,128)}, u32[]{:S(2)}) copy-start(f32[3,128]{1,0:T(4,128)} %param.15) | copy-start | bytes 4612
  184.2 92.1 %copy-start.10 = (bf16[128,256]{1,0:T(8,128)(2,1)S(1)}, bf16[128,256]{1,0:T(8,128)(2,1)}, u32[]{:S(2)}) copy-start(bf16[128,256]{1,0:T(8,128)(2,1)} %param.12) | copy-start | bytes 196612
  253.3 15.1 %all-to-all-start.1 = ((bf16[16,1,64,256]{3,2,1,0:T(8,128)(2,1)}), bf16[16,1,64,256]{3,2,1,0:T(8,128)(2,1)S(1)}, u32[]{:S(2)}, u32[]{:S(2)}) async-start(bf16[16,1,64,256]{3,2,1,0:T(8,128)(2,1)} %bitcast.99), calls=%async_computation.2 | async-start | bytes 1048576 | tf_op jit(solution)/shard_map/all_to_all | solution.py:124
  260.6 51.2 %all-gather.5.cloned.1.call-start = ((), (), s32[]{:S(2)}) async-start(), calls=%async_computation.6 | async-start | bytes 2359296 | tf_op jit(solution)/shard_map/all_gather | solution.py:40
  271.3 22.3 %copy-start.6 = (bf16[256,256]{1,0:T(8,128)(2,1)}, bf16[256,256]{1,0:T(8,128)(2,1)S(1)}, u32[]{:S(2)}) copy-start(bf16[256,256]{1,0:T(8,128)(2,1)S(1)} %add_convert_fusion.1) | copy-start | bytes 393220
  273.7 7.6 %collective-permute-start = (bf16[2,128,2]{1,2,0:T(2,128)(2,1)S(1)}, bf16[2,128,2]{1,2,0:T(2,128)(2,1)S(1)}, u32[]{:S(2)}, u32[]{:S(2)}) collective-permute-start(bf16[2,128,2]{1,2,0:T(2,128)(2,1)S(1)} %pad_maximum_fusion.3), channel_id=1, source_target_pairs={{0,16},{16,32},{32,48},{48,64},{64,80},{80,96},{96,112},{112,128},... | collective-permute-start | bytes 3080 | tf_op jit(solution)/shard_map/ppermute | solution.py:35
  287.4 24.3 %copy-start.5 = (bf16[128,4096]{1,0:T(8,128)(2,1)S(1)}, bf16[128,4096]{1,0:T(8,128)(2,1)}, u32[]{:S(2)}) copy-start(bf16[128,4096]{1,0:T(8,128)(2,1)} %param.16) | copy-start | bytes 3145732
  317.3 20.6 %all-to-all-start.2 = ((bf16[16,128,256]{2,1,0:T(8,128)(2,1)}), bf16[16,128,256]{2,1,0:T(8,128)(2,1)S(1)}, u32[]{:S(2)}, u32[]{:S(2)}) async-start(bf16[16,128,256]{2,1,0:T(8,128)(2,1)} %bitcast.88), calls=%async_computation.3 | async-start | bytes 2097152 | tf_op jit(solution)/shard_map/all_to_all | solution.py:52
  324.5 14.1 %copy-start.1 = (bf16[1,128,4096]{2,1,0:T(8,128)(2,1)S(1)}, bf16[1,128,4096]{2,1,0:T(8,128)(2,1)}, u32[]{:S(2)}) copy-start(bf16[1,128,4096]{2,1,0:T(8,128)(2,1)} %param.20) | copy-start | bytes 3145732
  324.5 11.7 %collective-permute-start.1 = (f32[128,2]{0,1:T(2,128)S(1)}, f32[128,2]{0,1:T(2,128)S(1)}, u32[]{:S(2)}, u32[]{:S(2)}) collective-permute-start(f32[128,2]{0,1:T(2,128)S(1)} %slice.97), channel_id=1, source_target_pairs={{16,0},{32,16},{48,32},{64,48},{80,64},{96,80},{112,96},{128,112},... | collective-permute-start | bytes 3080 | tf_op jit(solution)/shard_map/ppermute | solution.py:35
Sparse Core Ops, SparseCore 0:
  46.8 102.5 all-gather.2
  184.3 68.9 reduce-scatter.1
  273.6 38.1 all-gather.4
where the time goes:
time: 346 us; the launch traced here: 345 us
  waiting for transfers between devices  203 us (59%)
  matrix products  49 us (14%)
  blocking collectives  24 us (7%)
  local copies, waits for them, and re-layouts  22.5 us (7%)
  starting transfers between devices  22.2 us (6%)
  between operations  14.1 us (4%)
  other arithmetic  10.7 us (3%)
    all_gather x1, waiting for transfers between devices, in_one_piece(): lax.all_gather(both, axis, axis=dim, tiled=True)  102 us
    reduce_scatter x1, waiting for transfers between devices, shards(): lax.psum_scatter(partial_value.astype(jnp.bfloat16), TP, scatter_dimensio...  69.2 us
    all_to_all x1, blocking collectives, sent_together(): lax.all_to_all(both, axis, split_axis=split_dim, concat_axis=concat_dim,...  21.8 us
    all_gather x1, waiting for transfers between devices, whole_of(): shard = lax.all_gather(shard, axis, axis=dim, tiled=True)  18.2 us
    dot_general x1, matrix products, expert_step(): jnp.dot(back_up, up_w, preferred_element_type=jnp.float32)  11.3 us
    dot_general x1, matrix products, expert_step(): jnp.dot(back_gate, gate_w, preferred_element_type=jnp.float32)  8.07 us
    all_to_all x1, waiting for transfers between devices, shards(): lax.all_to_all(back_rows[:, None], 'sp', split_axis=0, concat_axis=0, til...  7.79 us
    ppermute x2, starting transfers between devices, from_behind(): lax.ppermute(value, axis, [(source, source + steps) for source in range(f...  7.48 us
  transfers between devices with their start and end apart: 7, of which 5 were waited for; matrix products, arithmetic and copies ran while one was open for 6% of the time, Pallas kernels for 0%

commit v1 on v0

v1 whole, which is shorter than its diff:
```python
import functools

import jax
import jax.numpy as jnp
from jax import lax
from jax.experimental import pallas as pl
from jax.experimental.pallas import tpu as pltpu
from jax.sharding import Mesh
from jax.sharding import PartitionSpec as P


TP = ("z", "c")
BF16 = jnp.bfloat16
F32 = jnp.float32


def dot_nn(a, b):
    return lax.dot_general(a, b, (((1,), (0,)), ((), ())), preferred_element_type=F32)


def dot_nt(a, b):
    return lax.dot_general(a, b, (((1,), (1,)), ((), ())), preferred_element_type=F32)


def dot_tn(a, b):
    return lax.dot_general(a, b, (((0,), (0,)), ((), ())), preferred_element_type=F32)


def cost(flops, nbytes):
    return pl.CostEstimate(flops=int(flops), bytes_accessed=int(nbytes), transcendentals=0)


def route_kernel(experts, cap, ids_ref, wts_ref, state_ref, sent_ref, pick_ref, scale_ref):
    tokens = ids_ref.shape[1]
    first, second = ids_ref[0:1, :], ids_ref[1:2, :]
    expert = lax.broadcasted_iota(jnp.int32, (experts, tokens), 0)
    is_first, is_second = first == expert, second == expert
    named = jnp.logical_or(is_first, is_second)
    before = lax.broadcasted_iota(jnp.int32, (tokens, tokens), 0) < lax.broadcasted_iota(
        jnp.int32, (tokens, tokens), 1
    )
    earlier = dot_nn(named.astype(F32).astype(BF16), before.astype(F32).astype(BF16))
    slot = jnp.where(named, earlier.astype(jnp.int32), -1)
    weight = jnp.where(is_first, wts_ref[0:1, :], jnp.where(is_second, wts_ref[1:2, :], 0.0))
    place = lax.broadcasted_iota(jnp.int32, (cap, tokens), 0)
    for e in range(experts):
        hit = slot[e : e + 1, :] == place
        pick_ref[e * cap : (e + 1) * cap, :] = hit.astype(F32).astype(BF16)
        taken = jnp.sum(jnp.where(hit, weight[e : e + 1, :], 0.0), axis=1, keepdims=True)
        scale_ref[e * cap : (e + 1) * cap, :] = jnp.broadcast_to(taken, (cap, 128))
    sent_ref[...] = dot_nn(pick_ref[...], state_ref[...]).astype(BF16)


def spread_kernel(pick_ref, scale_ref, *refs):
    pieces, (low_ref, high_ref) = refs[:-2], refs[-2:]
    width = pieces[0].shape[1]
    half = len(pieces) // 2
    scale = scale_ref[:, 0:1]
    for j, piece in enumerate(pieces):
        rows = (dot_nn(pick_ref[...], piece[...]) * scale).astype(BF16)
        out = low_ref if j < half else high_ref
        out[:, (j % half) * width : (j % half + 1) * width] = rows


def expert_kernel(
    slab_ref, state_ref, ml_ref, mh_ref, tl_ref, th_ref, wg_ref, wu_ref, wd_ref, part_ref, act_ref, wgu_ref
):
    slabs, width = state_ref.shape[0], state_ref.shape[2]
    hidden_n = wd_ref.shape[0]

    @pl.when(pl.program_id(0) == 0)
    def _():
        wgu_ref[:hidden_n] = wg_ref[...]
        wgu_ref[hidden_n:] = wu_ref[...]

    rows = jnp.concatenate([state_ref[s] for s in range(slabs)], axis=1)
    pre = dot_nt(rows, wgu_ref[...])
    gate_pre, up_pre = pre[:, :hidden_n], pre[:, hidden_n:]
    back_hidden = jnp.zeros(gate_pre.shape, F32)
    per = ml_ref.shape[1] // width
    for q, ref in enumerate((ml_ref, mh_ref, tl_ref, th_ref)):
        pieces = [
            wd_ref[:, pl.ds(pl.multiple_of(slab_ref[q * per + j] * width, width), width)]
            for j in range(per)
        ]
        back_hidden = back_hidden + dot_nt(ref[...], jnp.concatenate(pieces, axis=1))
    sig_gate = jax.nn.sigmoid(gate_pre)
    silu_gate = gate_pre * sig_gate
    hidden = (silu_gate * up_pre).astype(BF16)
    back_gate = (back_hidden * up_pre * sig_gate * (1.0 + gate_pre * (1.0 - sig_gate))).astype(BF16)
    back_up = (back_hidden * silu_gate).astype(BF16)
    back = jnp.concatenate([back_gate, back_up], axis=1)
    act_ref[:, : 2 * hidden_n] = back
    act_ref[:, 2 * hidden_n :] = hidden
    for s in range(slabs):
        part_ref[s] = dot_nn(back, wgu_ref[:, s * width : (s + 1) * width]).astype(BF16)


def weight_grad_kernel(slab_ref, act_ref, state_ref, ml_ref, mh_ref, tl_ref, th_ref, gg_ref, gu_ref, gd_ref):
    hidden_n = gg_ref.shape[0]
    step, per = pl.program_id(0), pl.num_programs(0) // 4
    both = dot_tn(act_ref[:, : 2 * hidden_n], state_ref[0])
    gg_ref[...] = both[:hidden_n]
    gu_ref[...] = both[hidden_n:]
    for q, ref in enumerate((ml_ref, mh_ref, tl_ref, th_ref)):

        @pl.when(step // per == q)
        def _(ref=ref):
            gd_ref[...] = dot_tn(act_ref[:, 2 * hidden_n :], ref[...])


def combine_kernel(pick_ref, rows_ref, cot_ref, out_ref):
    total = dot_tn(pick_ref[...], rows_ref[...])
    out_ref[...] = (cot_ref[...].astype(F32) + total).astype(BF16)


def proj_kernel(slab_ref, act_ref, *refs):
    pieces, out_ref = refs[:-1], refs[-1]
    for j, piece in enumerate(pieces):
        out_ref[slab_ref[j]] = dot_nn(act_ref[...], piece[...]).astype(BF16)


def mixer_kernel(slab_ref, proj_ref, conv_ref, outer_ref, *refs):
    pieces, (grad_ref, back_ref) = refs[:-2], refs[-2:]
    width = pieces[0].shape[1]
    back = jnp.zeros(back_ref.shape, F32)
    for j, piece in enumerate(pieces):
        start = pl.multiple_of(slab_ref[j] * width, width)
        back = back + dot_nt(proj_ref[:, pl.ds(start, width)], piece[...])
    grad_ref[...] = (back * conv_ref[...]).astype(BF16)
    back_ref[...] = back * outer_ref[...].astype(F32)


def ring_steps(size):
    steps = [0]
    for k in range(1, size // 2):
        steps += [k, -k]
    return steps + [size // 2]


def gathered(value, axis):
    size = lax.axis_size(axis)
    pieces = [value]
    for k in ring_steps(size)[1:]:
        pieces.append(lax.ppermute(value, axis, [(i, (i + k) % size) for i in range(size)]))
    return pieces


def from_behind(value, axis, steps):
    count = lax.axis_size(axis)
    first, last = (max(0, -steps), min(count, count - steps))
    return lax.ppermute(value, axis, [(source, source + steps) for source in range(first, last)])


def shards(
    conv_outer,
    conv_inner,
    conv_input,
    conv_taps,
    out_proj,
    mixed_state,
    route_ids,
    route_weights,
    w_gate,
    w_up,
    w_down,
    cotangent,
):
    tok_count, width = mixed_state.shape
    sp_size = lax.axis_size("sp")
    z_size = lax.axis_size("z")
    slabs = 2 * z_size
    local_experts, hidden_n, features = w_gate.shape
    experts = local_experts * sp_size
    cap = 4 * tok_count // experts
    slots = experts * cap
    core, place = lax.axis_index("c"), lax.axis_index("z")
    origin = (place - jnp.array(ring_steps(z_size), jnp.int32)) % z_size
    slab_of = jnp.concatenate([2 * origin + core, 2 * origin + 1 - core]).astype(jnp.int32)
    shape = jax.ShapeDtypeStruct

    cot_pieces = gathered(cotangent, "z")

    sent_state, pick, scale = pl.pallas_call(
        functools.partial(route_kernel, experts, cap),
        out_shape=(
            shape((slots, width), BF16),
            shape((slots, tok_count), BF16),
            shape((slots, 128), F32),
        ),
        cost_estimate=cost(2 * slots * tok_count * width, 4 * slots * width),
        name="route",
    )(route_ids.T, route_weights.T, mixed_state)
    recv_state = lax.all_to_all(
        sent_state.reshape(experts, cap, width), "sp", split_axis=0, concat_axis=0, tiled=True
    )
    state_all = lax.all_gather(recv_state.reshape(slots, width), TP, axis=0, tiled=False)

    half = z_size // 2 * width
    cot_low, cot_high = pl.pallas_call(
        spread_kernel,
        out_shape=(shape((slots, half), BF16),) * 2,
        cost_estimate=cost(4 * slots * tok_count * half, 8 * slots * half),
        name="spread",
    )(pick, scale, *cot_pieces)
    swap = [(0, 1), (1, 0)]

    def exchanged(part):
        got = lax.all_to_all(
            part.reshape(experts, cap, half), "sp", split_axis=0, concat_axis=0, tiled=True
        ).reshape(slots, half)
        return got, lax.ppermute(got, "c", swap)

    my_low, their_low = exchanged(cot_low)
    my_high, their_high = exchanged(cot_high)
    cots = (my_low, my_high, their_low, their_high)

    block = 256
    whole = lambda *dims: pl.BlockSpec(dims, lambda *_: (0,) * len(dims))
    cot_rows = pl.BlockSpec((block, half), lambda r, core: (r, 0))
    partial_value, acts = pl.pallas_call(
        expert_kernel,
        grid_spec=pltpu.PrefetchScalarGridSpec(
            num_scalar_prefetch=1,
            grid=(slots // block,),
            in_specs=[
                pl.BlockSpec((slabs, block, width), lambda r, core: (0, r, 0)),
                *[cot_rows] * 4,
                *[whole(hidden_n, features)] * 3,
            ],
            out_specs=[
                pl.BlockSpec((slabs, block, width), lambda r, core: (0, r, 0)),
                pl.BlockSpec((block, 3 * hidden_n), lambda r, core: (r, 0)),
            ],
            scratch_shapes=[pltpu.VMEM((2 * hidden_n, features), BF16)],
        ),
        out_shape=(shape((slabs, slots, width), BF16), shape((slots, 3 * hidden_n), BF16)),
        cost_estimate=cost(10 * slots * hidden_n * features, 6 * slots * features),
        name="expert",
    )(slab_of, state_all, *cots, w_gate[0], w_up[0], w_down[0])

    row_back = lax.psum_scatter(partial_value, TP, scatter_dimension=0, tiled=False)

    quarter = slabs // 4

    def cot_piece(q):
        return pl.BlockSpec(
            (slots, width), lambda s, core: (0, jnp.clip(s - q * quarter, 0, quarter - 1))
        )

    grad_out = pl.BlockSpec((hidden_n, width), lambda s, slab: (0, slab[s]))
    grad_gate, grad_up, grad_down = pl.pallas_call(
        weight_grad_kernel,
        grid_spec=pltpu.PrefetchScalarGridSpec(
            num_scalar_prefetch=1,
            grid=(slabs,),
            in_specs=[
                whole(slots, 3 * hidden_n),
                pl.BlockSpec((1, slots, width), lambda s, slab: (slab[s], 0, 0)),
                *[cot_piece(q) for q in range(4)],
            ],
            out_specs=[grad_out] * 3,
        ),
        out_shape=(shape((hidden_n, features), F32),) * 3,
        cost_estimate=cost(6 * slots * hidden_n * features, 6 * slots * features),
        name="weight_grads",
    )(slab_of, acts, state_all, *cots)
    row_back, grad_gate, grad_up, grad_down = lax.optimization_barrier(
        (row_back, grad_gate, grad_up, grad_down)
    )

    arrived = lax.all_to_all(
        row_back.reshape(experts, cap, width), "sp", split_axis=0, concat_axis=0, tiled=True
    ).reshape(slots, width)
    grad_mixed = pl.pallas_call(
        combine_kernel,
        out_shape=shape((tok_count, width), BF16),
        cost_estimate=cost(2 * slots * tok_count * width, 4 * slots * width),
        name="combine",
    )(pick, arrived, cotangent)
    near = gathered(grad_mixed, "z")
    full_back = near + [lax.ppermute(piece, "c", swap) for piece in near]

    taps_count = conv_taps.shape[0]
    rim_width = taps_count - 1
    channels = conv_inner.shape[0]
    head_block = from_behind(
        jnp.stack([conv_inner[:, tok_count - rim_width :], conv_input[:, tok_count - rim_width :]]),
        "sp",
        1,
    )
    inner_ext = jnp.concatenate([head_block[0], conv_inner], axis=1).astype(F32)
    input_ext = jnp.concatenate([head_block[1], conv_input], axis=1).astype(F32)
    inner_prod = inner_ext * input_ext
    conv_out = jnp.zeros((channels, tok_count), F32)
    for offset in range(taps_count):
        conv_out = (
            conv_out + conv_taps[offset][:, None] * inner_prod[:, offset : offset + tok_count]
        )
    mixer_act = (conv_outer.astype(F32) * conv_out).astype(BF16)

    vmem, smem = pl.BlockSpec(memory_space=pltpu.VMEM), pl.BlockSpec(memory_space=pltpu.SMEM)
    proj_term = pl.pallas_call(
        proj_kernel,
        in_specs=[smem] + [vmem] * (1 + slabs),
        out_shape=shape((slabs, channels, width), BF16),
        cost_estimate=cost(2 * channels * tok_count * features, 4 * tok_count * features),
        name="proj",
    )(slab_of, mixer_act, *full_back)
    landed = lax.all_to_all(proj_term, "sp", split_axis=0, concat_axis=0, tiled=True)
    grad_proj = jnp.sum(landed.astype(F32), axis=0)
    grad_outer, back_conv = pl.pallas_call(
        mixer_kernel,
        in_specs=[smem] + [vmem] * (3 + slabs),
        out_shape=(shape((channels, tok_count), BF16), shape((channels, tok_count), F32)),
        cost_estimate=cost(2 * channels * tok_count * features, 4 * tok_count * features),
        name="mixer",
    )(slab_of, out_proj, conv_out, conv_outer, *full_back)
    tail_back = from_behind(back_conv[:, :rim_width], "sp", -1)
    back_ext = jnp.concatenate([back_conv, tail_back], axis=1)
    back_prod = jnp.zeros_like(back_conv)
    for offset in range(taps_count):
        shift_by = rim_width - offset
        back_prod = (
            back_prod + conv_taps[offset][:, None] * back_ext[:, shift_by : shift_by + tok_count]
        )
    grad_inner = (back_prod * conv_input.astype(F32)).astype(BF16)
    grad_input = (back_prod * conv_inner.astype(F32)).astype(BF16)
    return (
        grad_gate[None],
        grad_up[None],
        grad_down[None],
        grad_mixed,
        grad_proj,
        grad_outer,
        grad_inner,
        grad_input,
    )


def solution(mesh):
    torus = Mesh(mesh.devices.reshape(mesh.shape["sp"], mesh.shape["tp"] // 2, 2), ("sp", "z", "c"))

    return jax.shard_map(
        shards,
        mesh=torus,
        in_specs=(
            P(TP, "sp"),
            P(TP, "sp"),
            P(TP, "sp"),
            P(None, TP),
            P(TP, None),
            P("sp", TP),
            P("sp", None),
            P("sp", None),
            P("sp", TP, None),
            P("sp", TP, None),
            P("sp", TP, None),
            P("sp", TP),
        ),
        out_specs=(
            P("sp", TP, None),
            P("sp", TP, None),
            P("sp", TP, None),
            P("sp", TP),
            P(TP, "sp"),
            P(TP, "sp"),
            P(TP, "sp"),
            P(TP, "sp"),
        ),
        check_vma=False,
    )
```

time: 346 us -> 303 us (0.88); the launches traced: 345 us -> 298 us
  waiting for transfers between devices: 203 us -> 117 us
  Pallas kernels: 0 us -> 49.3 us
  matrix products: 49 us -> 0 us
  starting transfers between devices: 22.2 us -> 66.3 us
  local copies, waits for them, and re-layouts: 22.5 us -> 4.34 us
  blocking collectives: 24 us -> 41.1 us
  other arithmetic: 10.7 us -> 4.77 us
    all_gather x2 -> x1, waiting for transfers between devices: 121 us -> 0.01 us  [shards(): lax.all_gather(recv_state.reshape(slots, width), TP, axis=0, tiled=False)]
    pallas_call x0 -> x7, Pallas kernels: none -> 49.3 us  [the longest x1 19.4 us: shards(): pl.pallas_call(weight_grad_kernel, grid_spec=pltpu.PrefetchScalarGridSpec...]
    dot_general x10 -> x0, matrix products: 49 us -> none  [the longest x1 11.3 us: expert_step(): jnp.dot(back_up, up_w, preferred_element_type=jnp.float32)]
    ppermute x0 -> x24, starting transfers between devices: none -> 38.4 us  [the longest x14 36.7 us: gathered(): lax.ppermute(value, axis, [(i, (i + k) % size) for i in range(size)])]
    ppermute x0 -> x24, waiting for transfers between devices: none -> 28.9 us  [the longest x14 24.7 us: gathered(): lax.ppermute(value, axis, [(i, (i + k) % size) for i in range(size)])]
    all_to_all x1 -> x2, blocking collectives: 21.8 us -> 41.1 us  [the longest x1 24.6 us: exchanged(): lax.all_to_all(part.reshape(experts, cap, half), 'sp', split_axis=0, conc...]
    all_to_all x2 -> x3, waiting for transfers between devices: 7.8 us -> 24.6 us  [the longest x1 20.6 us: exchanged(): lax.all_to_all(part.reshape(experts, cap, half), 'sp', split_axis=0, conc...]
    reduce_scatter x1, waiting for transfers between devices: 69.2 us -> 58.8 us  [shards(): lax.psum_scatter(partial_value, TP, scatter_dimension=0, tiled=False)]
  transfers between devices with their start and end apart: 7 -> 31, of which waited for: 5 -> 13; matrix products, arithmetic and copies ran while one was open for 6% -> 2% of each run, Pallas kernels for 0% -> 10%
where the time goes in v1:
time: 303 us; the launch traced here: 298 us
  waiting for transfers between devices  117 us (39%)
  starting transfers between devices  66.3 us (22%)
  Pallas kernels  49.3 us (16%)
  blocking collectives  41.1 us (14%)
  between operations  14.3 us (5%)
  other arithmetic  4.77 us (2%)
  local copies, waits for them, and re-layouts  4.34 us (1%)
    reduce_scatter x1, waiting for transfers between devices, shards(): lax.psum_scatter(partial_value, TP, scatter_dimension=0, tiled=False)  58.8 us
    ppermute x14, starting transfers between devices, gathered(): lax.ppermute(value, axis, [(i, (i + k) % size) for i in range(size)])  36.7 us
    ppermute x14, waiting for transfers between devices, gathered(): lax.ppermute(value, axis, [(i, (i + k) % size) for i in range(size)])  24.7 us
    all_to_all x1, blocking collectives, exchanged(): lax.all_to_all(part.reshape(experts, cap, half), 'sp', split_axis=0, conc...  24.6 us
    all_to_all x1, waiting for transfers between devices, exchanged(): lax.all_to_all(part.reshape(experts, cap, half), 'sp', split_axis=0, conc...  20.6 us
    pallas_call x1, Pallas kernels, shards(): pl.pallas_call(weight_grad_kernel, grid_spec=pltpu.PrefetchScalarGridSpec...  19.4 us
    all_to_all x1, blocking collectives, shards(): lax.all_to_all(sent_state.reshape(experts, cap, width), 'sp', split_axis=...  16.5 us
    pallas_call x1, Pallas kernels, shards(): pl.pallas_call(expert_kernel, grid_spec=pltpu.PrefetchScalarGridSpec(num_...  14.4 us
  transfers between devices with their start and end apart: 31, of which 13 were waited for; matrix products, arithmetic and copies ran while one was open for 2% of the time, Pallas kernels for 10%

profile of v1, /device:TPU:24, one launch (start us, length us, event | category | flops | bytes accessed | tf_op | source)
XLA Modules:
  0.0 297.5 jit_solution(398769903529043475)
XLA Ops:
  7.2 2.5 route.1
  9.7 16.5 %all_to_all.25 = bf16[16,64,256]{2,1,0:T(8,128)(2,1)} all-to-all(bf16[16,64,256]{2,1,0:T(8,128)(2,1)} %bitcast.40), channel_id=1, replica_groups=mesh['sp'=16,'z'=8,'c'=2] {'sp'}, dimensions={0} | all-to-all | bytes 1048576 | tf_op jit(solution)/shard_map/all_to_all | solution.py:194
  26.2 2.0 collective-permute-start
  28.2 4.0 %collective-permute-start.1 = (bf16[256,256]{1,0:T(8,128)(2,1)}, bf16[256,256]{1,0:T(8,128)(2,1)S(1)}, u32[]{:S(2)}, u32[]{:S(2)}) collective-permute-start(bf16[256,256]{1,0:T(8,128)(2,1)} %cot_ref.1), channel_id=1, source_target_pairs={{0,14},{2,0},{4,2},{6,4},{8,6},{10,8},{12,10},{14,12},{1,15},{3,1}... | collective-permute-start | bytes 393224 | tf_op jit(solution)/shard_map/ppermute | solution.py:145
  32.2 4.1 %collective-permute-start.3 = (bf16[256,256]{1,0:T(8,128)(2,1)}, bf16[256,256]{1,0:T(8,128)(2,1)S(1)}, u32[]{:S(2)}, u32[]{:S(2)}) collective-permute-start(bf16[256,256]{1,0:T(8,128)(2,1)} %cot_ref.1), channel_id=1, source_target_pairs={{0,12},{2,14},{4,0},{6,2},{8,4},{10,6},{12,8},{14,10},{1,13},{3,15... | collective-permute-start | bytes 393224 | tf_op jit(solution)/shard_map/ppermute | solution.py:145
  36.4 0.6 collective-permute-start.4
  37.0 4.4 %collective-permute-start.5 = (bf16[256,256]{1,0:T(8,128)(2,1)}, bf16[256,256]{1,0:T(8,128)(2,1)S(1)}, u32[]{:S(2)}, u32[]{:S(2)}) collective-permute-start(bf16[256,256]{1,0:T(8,128)(2,1)} %cot_ref.1), channel_id=1, source_target_pairs={{0,10},{2,12},{4,14},{6,0},{8,2},{10,4},{12,6},{14,8},{1,11},{3,13... | collective-permute-start | bytes 393224 | tf_op jit(solution)/shard_map/ppermute | solution.py:145
  41.4 4.5 %collective-permute-start.6 = (bf16[256,256]{1,0:T(8,128)(2,1)}, bf16[256,256]{1,0:T(8,128)(2,1)S(1)}, u32[]{:S(2)}, u32[]{:S(2)}) collective-permute-start(bf16[256,256]{1,0:T(8,128)(2,1)} %cot_ref.1), channel_id=1, source_target_pairs={{0,8},{2,10},{4,12},{6,14},{8,0},{10,2},{12,4},{14,6},{1,9},{3,11}... | collective-permute-start | bytes 393224 | tf_op jit(solution)/shard_map/ppermute | solution.py:145
  45.9 0.8 collective-permute-done.2.refs_3_
  46.7 2.1 collective-permute-done.3.refs_4_
  48.8 7.9 %collective-permute-done.4.refs_5_ = bf16[256,256]{1,0:T(8,128)(2,1)S(1)} collective-permute-done((bf16[256,256]{1,0:T(8,128)(2,1)}, bf16[256,256]{1,0:T(8,128)(2,1)S(1)}, u32[]{:S(2)}, u32[]{:S(2)}) %collective-permute-start.4) | collective-permute-done | bytes 131104 | tf_op jit(solution)/shard_map/ppermute | solution.py:145
  56.7 3.6 %collective-permute-done.5.refs_6_ = bf16[256,256]{1,0:T(8,128)(2,1)S(1)} collective-permute-done((bf16[256,256]{1,0:T(8,128)(2,1)}, bf16[256,256]{1,0:T(8,128)(2,1)S(1)}, u32[]{:S(2)}, u32[]{:S(2)}) %collective-permute-start.5) | collective-permute-done | bytes 131104 | tf_op jit(solution)/shard_map/ppermute | solution.py:145
  60.3 2.3 collective-permute-done.6.refs_7_
  62.6 0.6 copy-done.28
  63.2 4.3 %spread.1 = (bf16[1024,1024]{1,0:T(8,128)(2,1)}, bf16[1024,1024]{1,0:T(8,128)(2,1)}) custom-call(bf16[1024,256]{1,0:T(8,128)(2,1)} %get-tuple-element.25.pick_ref, f32[1024,128]{1,0:T(8,128)} %get-tuple-element.26.scale_ref, bf16[256,256]{1,0:T(8,128)(2,1)} %cot_ref.1, bf16[256,256]{1,0:T(8,128)(2,1)} %copy-done.22, bf16[256,256]{1,0:T(8,128)(2,1)} %copy-done.23, ...), custom_call_target="tpu_custom_call" | custom-call | flops 1073741824 | bytes 8388608 | tf_op jit(solution)/shard_map/spread/pallas_call | solution.py:200
  67.4 24.6 %all_to_all.26 = bf16[16,64,1024]{2,1,0:T(8,128)(2,1)S(1)} all-to-all(bf16[16,64,1024]{2,1,0:T(8,128)(2,1)} %bitcast.33), channel_id=1, replica_groups=mesh['sp'=16,'z'=8,'c'=2] {'sp'}, dimensions={0} | all-to-all | bytes 4194304 | tf_op jit(solution)/shard_map/all_to_all | solution.py:209
  92.0 6.7 %all-to-all-start.2 = ((bf16[16,64,1024]{2,1,0:T(8,128)(2,1)}), bf16[16,64,1024]{2,1,0:T(8,128)(2,1)}, u32[]{:S(2)}, u32[]{:S(2)}) async-start(bf16[16,64,1024]{2,1,0:T(8,128)(2,1)} %bitcast.32), calls=%async_computation.2 | async-start | bytes 4194304 | tf_op jit(solution)/shard_map/all_to_all | solution.py:209
  98.8 0.1 collective-permute-start.7
  98.9 20.6 %all-to-all-done.2 = bf16[16,64,1024]{2,1,0:T(8,128)(2,1)} async-done(((bf16[16,64,1024]{2,1,0:T(8,128)(2,1)}), bf16[16,64,1024]{2,1,0:T(8,128)(2,1)}, u32[]{:S(2)}, u32[]{:S(2)}) %all-to-all-start.2) | async-done | bytes 2097184 | tf_op jit(solution)/shard_map/all_to_all | solution.py:209
  119.5 0.6 pad_add_fusion.slab_ref
  120.1 3.9 %collective-permute-done.8.th_ref = bf16[1024,1024]{1,0:T(8,128)(2,1)} collective-permute-done((bf16[1024,1024]{1,0:T(8,128)(2,1)}, bf16[1024,1024]{1,0:T(8,128)(2,1)}, u32[]{:S(2)}, u32[]{:S(2)}) %collective-permute-start.8) | collective-permute-done | bytes 2097184 | tf_op jit(solution)/shard_map/ppermute | solution.py:212
  124.0 14.4 %expert.1 = (bf16[16,1024,256]{2,1,0:T(8,128)(2,1)}, bf16[1024,384]{1,0:T(8,128)(2,1)}) custom-call(s32[16]{0:T(128)} %pad_add_fusion.slab_ref, bf16[16,1024,256]{2,1,0:T(8,128)(2,1)} %all-gather.2.cloned.1.call-done.state_ref, bf16[1024,1024]{1,0:T(8,128)(2,1)} %bitcast.30, bf16[1024,1024]{1,0:T(8,128)(2,1)} %bitcast.7.mh_ref, ...), custom_call_target="tpu_custom_call" | custom-call | flops 5368709120 | bytes 25165824 | tf_op jit(solution)/shard_map/expert/pallas_call | solution.py:221
  138.4 19.4 %weight_grads.1 = (f32[128,4096]{1,0:T(8,128)}, f32[128,4096]{1,0:T(8,128)}, f32[128,4096]{1,0:T(8,128)}) custom-call(s32[16]{0:T(128)} %pad_add_fusion.slab_ref, bf16[1024,384]{1,0:T(8,128)(2,1)} %get-tuple-element.30.act_ref, bf16[16,1024,256]{2,1,0:T(8,128)(2,1)} %all-gather.2.cloned.1.call-done.state_ref, bf16[1024,1024]{1,0:T(8,128)(2,1)} %bitcast.31, ...), custom_call_target="tpu_custom_call" | custom-call | flops 3221225472 | bytes 25165824 | tf_op jit(solution)/shard_map/weight_grads/pallas_call | solution.py:252
  157.8 58.8 %reduce-scatter.2.cloned.1.call-done = bf16[1,1024,256]{2,1,0:T(8,128)(2,1)} async-done(((bf16[16,1024,256]{2,1,0:T(8,128)(2,1)}), bf16[1,1024,256]{2,1,0:T(8,128)(2,1)}) %reduce-scatter.2.cloned.1.call-update) | async-done | bytes 524304 | tf_op jit(solution)/shard_map/reduce_scatter | solution.py:242
  216.6 7.0 %all-to-all-start.3 = ((bf16[16,64,256]{2,1,0:T(8,128)(2,1)}), bf16[16,64,256]{2,1,0:T(8,128)(2,1)S(1)}, u32[]{:S(2)}, u32[]{:S(2)}) async-start(bf16[16,64,256]{2,1,0:T(8,128)(2,1)} %bitcast.39), calls=%async_computation.4 | async-start | bytes 1048576 | tf_op jit(solution)/shard_map/all_to_all | solution.py:272
  223.6 0.1 slice.44
  223.7 0.1 copy.25
  223.7 0.1 slice.43
  223.8 0.1 copy.24
  223.9 0.1 copy.23
  224.1 3.4 %collective-permute-start.9 = (bf16[2,128,2]{2,1,0:T(8,128)(2,1)S(1)}, bf16[2,128,2]{2,1,0:T(8,128)(2,1)S(1)}, u32[]{:S(2)}, u32[]{:S(2)}) collective-permute-start(bf16[2,128,2]{2,1,0:T(8,128)(2,1)S(1)} %copy.23), channel_id=1, source_target_pairs={{0,16},{16,32},{32,48},{48,64},{64,80},{80,96},{96,112},{112,128},... | collective-permute-start | bytes 3080 | tf_op jit(solution)/shard_map/ppermute | solution.py:152
  227.5 4.0 %all-to-all-done.3 = bf16[16,64,256]{2,1,0:T(8,128)(2,1)S(1)} async-done(((bf16[16,64,256]{2,1,0:T(8,128)(2,1)}), bf16[16,64,256]{2,1,0:T(8,128)(2,1)S(1)}, u32[]{:S(2)}, u32[]{:S(2)}) %all-to-all-start.3) | async-done | bytes 524320 | tf_op jit(solution)/shard_map/all_to_all | solution.py:272
  231.4 0.8 copy-done.1
  232.2 2.2 combine.1.refs_0_
  234.5 3.2 %collective-permute-start.11 = (bf16[256,256]{1,0:T(8,128)(2,1)}, bf16[256,256]{1,0:T(8,128)(2,1)S(1)}, u32[]{:S(2)}, u32[]{:S(2)}) collective-permute-start(bf16[256,256]{1,0:T(8,128)(2,1)} %combine.1.refs_0_), channel_id=1, source_target_pairs={{0,14},{2,0},{4,2},{6,4},{8,6},{10,8},{12,10},{14,12},{1,15},{3,1}... | collective-permute-start | bytes 393224 | tf_op jit(solution)/shard_map/ppermute | solution.py:145
  237.7 4.1 %collective-permute-start.13 = (bf16[256,256]{1,0:T(8,128)(2,1)}, bf16[256,256]{1,0:T(8,128)(2,1)S(1)}, u32[]{:S(2)}, u32[]{:S(2)}) collective-permute-start(bf16[256,256]{1,0:T(8,128)(2,1)} %combine.1.refs_0_), channel_id=1, source_target_pairs={{0,12},{2,14},{4,0},{6,2},{8,4},{10,6},{12,8},{14,10},{1,13},{3,15... | collective-permute-start | bytes 393224 | tf_op jit(solution)/shard_map/ppermute | solution.py:145
  241.8 0.6 collective-permute-start.14
  242.5 4.5 %collective-permute-start.15 = (bf16[256,256]{1,0:T(8,128)(2,1)}, bf16[256,256]{1,0:T(8,128)(2,1)S(1)}, u32[]{:S(2)}, u32[]{:S(2)}) collective-permute-start(bf16[256,256]{1,0:T(8,128)(2,1)} %combine.1.refs_0_), channel_id=1, source_target_pairs={{0,10},{2,12},{4,14},{6,0},{8,2},{10,4},{12,6},{14,8},{1,11},{3,13... | collective-permute-start | bytes 393224 | tf_op jit(solution)/shard_map/ppermute | solution.py:145
  247.0 4.5 %collective-permute-start.16 = (bf16[256,256]{1,0:T(8,128)(2,1)}, bf16[256,256]{1,0:T(8,128)(2,1)S(1)}, u32[]{:S(2)}, u32[]{:S(2)}) collective-permute-start(bf16[256,256]{1,0:T(8,128)(2,1)} %combine.1.refs_0_), channel_id=1, source_target_pairs={{0,8},{2,10},{4,12},{6,14},{8,0},{10,2},{12,4},{14,6},{1,9},{3,11}... | collective-permute-start | bytes 393224 | tf_op jit(solution)/shard_map/ppermute | solution.py:145
  251.5 0.5 collective-permute-start.18
  252.0 6.3 %collective-permute-done.14.refs_5_ = bf16[256,256]{1,0:T(8,128)(2,1)S(1)} collective-permute-done((bf16[256,256]{1,0:T(8,128)(2,1)}, bf16[256,256]{1,0:T(8,128)(2,1)S(1)}, u32[]{:S(2)}, u32[]{:S(2)}) %collective-permute-start.14) | collective-permute-done | bytes 131104 | tf_op jit(solution)/shard_map/ppermute | solution.py:145
  258.3 0.1 convert_multiply_fusion
  258.4 1.8 collective-permute-done.15.refs_6_
  260.2 0.5 collective-permute-start.21
  260.7 0.1 collective-permute-start.22
  260.8 0.4 collective-permute-start.23
  261.3 0.1 collective-permute-start.24
  261.4 0.9 multiply_convert_fusion.2
  262.3 0.3 collective-permute-done.24.refs_15_
  262.7 0.2 copy-done.12
  262.9 0.0 copy-done.13
  262.9 0.1 copy-done.14
  263.0 0.0 copy-done.15
  263.0 0.2 copy-done.16
  263.3 3.1 %proj.1 = bf16[16,128,256]{2,1,0:T(8,128)(2,1)} custom-call(s32[16]{0:T(128)} %pad_add_fusion.slab_ref, bf16[128,256]{1,0:T(8,128)(2,1)} %get-tuple-element.42.act_ref, bf16[256,256]{1,0:T(8,128)(2,1)} %combine.1.refs_0_, bf16[256,256]{1,0:T(8,128)(2,1)} %copy-done.2, bf16[256,256]{1,0:T(8,128)(2,1)} %copy-done.3, bf16[256,256]{1,0:T(8,128)(2,1)} %copy-done.4, ...), custom_call_target="tpu_custom_call" | custom-call | flops 268435456 | bytes 4194304 | tf_op jit(solution)/shard_map/proj/pallas_call | solution.py:303
  266.4 5.9 %all-to-all-start.4 = ((bf16[16,128,256]{2,1,0:T(8,128)(2,1)}), bf16[16,128,256]{2,1,0:T(8,128)(2,1)S(1)}, u32[]{:S(2)}, u32[]{:S(2)}) async-start(bf16[16,128,256]{2,1,0:T(8,128)(2,1)} %proj.1), calls=%async_computation.5 | async-start | bytes 2097152 | tf_op jit(solution)/shard_map/all_to_all | solution.py:310
  272.3 3.5 %mixer.1 = (bf16[128,256]{1,0:T(8,128)(2,1)}, f32[128,256]{1,0:T(8,128)}) custom-call(s32[16]{0:T(128)} %pad_add_fusion.slab_ref, bf16[128,4096]{1,0:T(8,128)(2,1)} %proj_ref.1, f32[128,256]{1,0:T(8,128)} %get-tuple-element.43.conv_ref, bf16[128,256]{1,0:T(8,128)(2,1)} %outer_ref.1, bf16[256,256]{1,0:T(8,128)(2,1)} %combine.1.refs_0_, ...), custom_call_target="tpu_custom_call" | custom-call | flops 268435456 | bytes 4194304 | tf_op jit(solution)/shard_map/mixer/pallas_call | solution.py:312
  275.8 0.8 slice.52
  276.6 4.9 %collective-permute-start.25 = (f32[128,2]{1,0:T(8,128)S(1)}, f32[128,2]{1,0:T(8,128)S(1)}, u32[]{:S(2)}, u32[]{:S(2)}) collective-permute-start(f32[128,2]{1,0:T(8,128)S(1)} %slice.52), channel_id=1, source_target_pairs={{16,0},{32,16},{48,32},{64,48},{80,64},{96,80},{112,96},{128,112},... | collective-permute-start | bytes 3080 | tf_op jit(solution)/shard_map/ppermute | solution.py:152
  281.5 0.9 constant_dynamic-update-slice_fusion.1
  282.4 5.1 %collective-permute-done.25 = f32[128,2]{1,0:T(8,128)S(1)} collective-permute-done((f32[128,2]{1,0:T(8,128)S(1)}, f32[128,2]{1,0:T(8,128)S(1)}, u32[]{:S(2)}, u32[]{:S(2)}) %collective-permute-start.25) | collective-permute-done | bytes 1056 | tf_op jit(solution)/shard_map/ppermute | solution.py:152
  287.5 1.7 multiply_convert_fusion
  289.2 0.6 multiply_convert_fusion.1
  289.9 0.8 convert_reduce_fusion
  (86 shorter events, 0.3 us)
Async XLA Ops:
  7.2 116.8 %all-gather.2.cloned.1.call-start = ((), (), s32[]{:S(2)}) async-start(), calls=%async_computation.6 | async-start | bytes 8912896 | tf_op jit(solution)/shard_map/all_gather | solution.py:197
  26.2 10.8 %collective-permute-start = (bf16[256,256]{1,0:T(8,128)(2,1)}, bf16[256,256]{1,0:T(8,128)(2,1)S(1)}, u32[]{:S(2)}, u32[]{:S(2)}) collective-permute-start(bf16[256,256]{1,0:T(8,128)(2,1)} %cot_ref.1), channel_id=1, source_target_pairs={{0,2},{2,4},{4,6},{6,8},{8,10},{10,12},{12,14},{14,0},{1,3},{3,5},... | collective-permute-start | bytes 393224 | tf_op jit(solution)/shard_map/ppermute | solution.py:145
  28.2 13.2 %collective-permute-start.1 = (bf16[256,256]{1,0:T(8,128)(2,1)}, bf16[256,256]{1,0:T(8,128)(2,1)S(1)}, u32[]{:S(2)}, u32[]{:S(2)}) collective-permute-start(bf16[256,256]{1,0:T(8,128)(2,1)} %cot_ref.1), channel_id=1, source_target_pairs={{0,14},{2,0},{4,2},{6,4},{8,6},{10,8},{12,10},{14,12},{1,15},{3,1}... | collective-permute-start | bytes 393224 | tf_op jit(solution)/shard_map/ppermute | solution.py:145
  32.2 14.4 %collective-permute-start.2 = (bf16[256,256]{1,0:T(8,128)(2,1)}, bf16[256,256]{1,0:T(8,128)(2,1)S(1)}, u32[]{:S(2)}, u32[]{:S(2)}) collective-permute-start(bf16[256,256]{1,0:T(8,128)(2,1)} %cot_ref.1), channel_id=1, source_target_pairs={{0,4},{2,6},{4,8},{6,10},{8,12},{10,14},{12,0},{14,2},{1,5},{3,7},... | collective-permute-start | bytes 393224 | tf_op jit(solution)/shard_map/ppermute | solution.py:145
  32.2 16.5 %collective-permute-start.3 = (bf16[256,256]{1,0:T(8,128)(2,1)}, bf16[256,256]{1,0:T(8,128)(2,1)S(1)}, u32[]{:S(2)}, u32[]{:S(2)}) collective-permute-start(bf16[256,256]{1,0:T(8,128)(2,1)} %cot_ref.1), channel_id=1, source_target_pairs={{0,12},{2,14},{4,0},{6,2},{8,4},{10,6},{12,8},{14,10},{1,13},{3,15... | collective-permute-start | bytes 393224 | tf_op jit(solution)/shard_map/ppermute | solution.py:145
  36.4 20.3 %collective-permute-start.4 = (bf16[256,256]{1,0:T(8,128)(2,1)}, bf16[256,256]{1,0:T(8,128)(2,1)S(1)}, u32[]{:S(2)}, u32[]{:S(2)}) collective-permute-start(bf16[256,256]{1,0:T(8,128)(2,1)} %cot_ref.1), channel_id=1, source_target_pairs={{0,6},{2,8},{4,10},{6,12},{8,14},{10,0},{12,2},{14,4},{1,7},{3,9},... | collective-permute-start | bytes 393224 | tf_op jit(solution)/shard_map/ppermute | solution.py:145
  37.0 25.6 %copy-start.22 = (bf16[256,256]{1,0:T(8,128)(2,1)}, bf16[256,256]{1,0:T(8,128)(2,1)S(1)}, u32[]{:S(2)}) copy-start(bf16[256,256]{1,0:T(8,128)(2,1)S(1)} %collective-permute-done.refs_1_) | copy-start | bytes 393220
  37.0 23.3 %collective-permute-start.5 = (bf16[256,256]{1,0:T(8,128)(2,1)}, bf16[256,256]{1,0:T(8,128)(2,1)S(1)}, u32[]{:S(2)}, u32[]{:S(2)}) collective-permute-start(bf16[256,256]{1,0:T(8,128)(2,1)} %cot_ref.1), channel_id=1, source_target_pairs={{0,10},{2,12},{4,14},{6,0},{8,2},{10,4},{12,6},{14,8},{1,11},{3,13... | collective-permute-start | bytes 393224 | tf_op jit(solution)/shard_map/ppermute | solution.py:145
  41.4 21.1 %copy-start.23 = (bf16[256,256]{1,0:T(8,128)(2,1)}, bf16[256,256]{1,0:T(8,128)(2,1)S(1)}, u32[]{:S(2)}) copy-start(bf16[256,256]{1,0:T(8,128)(2,1)S(1)} %collective-permute-done.1.refs_2_) | copy-start | bytes 393220
  41.4 21.1 %collective-permute-start.6 = (bf16[256,256]{1,0:T(8,128)(2,1)}, bf16[256,256]{1,0:T(8,128)(2,1)S(1)}, u32[]{:S(2)}, u32[]{:S(2)}) collective-permute-start(bf16[256,256]{1,0:T(8,128)(2,1)} %cot_ref.1), channel_id=1, source_target_pairs={{0,8},{2,10},{4,12},{6,14},{8,0},{10,2},{12,4},{14,6},{1,9},{3,11}... | collective-permute-start | bytes 393224 | tf_op jit(solution)/shard_map/ppermute | solution.py:145
  46.7 15.9 %copy-start.24 = (bf16[256,256]{1,0:T(8,128)(2,1)}, bf16[256,256]{1,0:T(8,128)(2,1)S(1)}, u32[]{:S(2)}) copy-start(bf16[256,256]{1,0:T(8,128)(2,1)S(1)} %collective-permute-done.2.refs_3_) | copy-start | bytes 393220
  48.8 13.8 %copy-start.25 = (bf16[256,256]{1,0:T(8,128)(2,1)}, bf16[256,256]{1,0:T(8,128)(2,1)S(1)}, u32[]{:S(2)}) copy-start(bf16[256,256]{1,0:T(8,128)(2,1)S(1)} %collective-permute-done.3.refs_4_) | copy-start | bytes 393220
  56.7 5.9 %copy-start.26 = (bf16[256,256]{1,0:T(8,128)(2,1)}, bf16[256,256]{1,0:T(8,128)(2,1)S(1)}, u32[]{:S(2)}) copy-start(bf16[256,256]{1,0:T(8,128)(2,1)S(1)} %collective-permute-done.4.refs_5_) | copy-start | bytes 393220
  60.3 2.3 copy-start.27
  62.5 0.7 copy-start.28
  92.0 6.7 %copy-start = (bf16[16,64,1024]{2,1,0:T(8,128)(2,1)}, bf16[16,64,1024]{2,1,0:T(8,128)(2,1)S(1)}, u32[]{:S(2)}) copy-start(bf16[16,64,1024]{2,1,0:T(8,128)(2,1)S(1)} %all_to_all.26) | copy-start | bytes 6291460
  92.0 27.4 %copy-start.21 = (s32[8]{0:T(128)S(1)}, s32[8]{0:T(128)}, u32[]{:S(2)}) copy-start(s32[8]{0:T(128)} %constant.35) | copy-start | bytes 100
  92.0 27.4 %all-to-all-start.2 = ((bf16[16,64,1024]{2,1,0:T(8,128)(2,1)}), bf16[16,64,1024]{2,1,0:T(8,128)(2,1)}, u32[]{:S(2)}, u32[]{:S(2)}) async-start(bf16[16,64,1024]{2,1,0:T(8,128)(2,1)} %bitcast.32), calls=%async_computation.2 | async-start | bytes 4194304 | tf_op jit(solution)/shard_map/all_to_all | solution.py:209
  98.7 117.8 %reduce-scatter.2.cloned.1.call-start = ((), (), s32[]{:S(2)}) async-start(), calls=%async_computation.7 | async-start | bytes 8912896 | tf_op jit(solution)/shard_map/reduce_scatter | solution.py:242
  98.8 21.3 %collective-permute-start.7 = (bf16[1024,1024]{1,0:T(8,128)(2,1)S(1)}, bf16[1024,1024]{1,0:T(8,128)(2,1)}, u32[]{:S(2)}, u32[]{:S(2)}) collective-permute-start(bf16[1024,1024]{1,0:T(8,128)(2,1)S(1)} %bitcast.29), channel_id=1, source_target_pairs={{0,1},{1,0},{2,3},{3,2},{4,5},{5,4},{6,7},{7,6},{8,9},{9,8},{10,11... | collective-permute-start | bytes 6291464 | tf_op jit(solution)/shard_map/ppermute | solution.py:212
  119.5 4.5 %collective-permute-start.8 = (bf16[1024,1024]{1,0:T(8,128)(2,1)}, bf16[1024,1024]{1,0:T(8,128)(2,1)}, u32[]{:S(2)}, u32[]{:S(2)}) collective-permute-start(bf16[1024,1024]{1,0:T(8,128)(2,1)} %bitcast.7.mh_ref), channel_id=1, source_target_pairs={{0,1},{1,0},{2,3},{3,2},{4,5},{5,4},{6,7},{7,6},{8,9},{9,8},{10,11... | collective-permute-start | bytes 6291464 | tf_op jit(solution)/shard_map/ppermute | solution.py:212
  138.4 85.2 %copy-start.18 = (bf16[128,256]{1,0:T(8,128)(2,1)S(1)}, bf16[128,256]{1,0:T(8,128)(2,1)}, u32[]{:S(2)}) copy-start(bf16[128,256]{1,0:T(8,128)(2,1)} %param.15) | copy-start | bytes 196612
  138.4 85.3 %copy-start.17 = (bf16[128,256]{1,0:T(8,128)(2,1)S(1)}, bf16[128,256]{1,0:T(8,128)(2,1)}, u32[]{:S(2)}) copy-start(bf16[128,256]{1,0:T(8,128)(2,1)} %param.14) | copy-start | bytes 196612
  157.8 84.7 %copy-start.20 = (f32[3,128]{1,0:T(4,128)S(1)}, f32[3,128]{1,0:T(4,128)}, u32[]{:S(2)}) copy-start(f32[3,128]{1,0:T(4,128)} %param.16) | copy-start | bytes 4612
  157.8 103.6 %copy-start.19 = (bf16[128,256]{1,0:T(8,128)(2,1)S(1)}, bf16[128,256]{1,0:T(8,128)(2,1)}, u32[]{:S(2)}) copy-start(bf16[128,256]{1,0:T(8,128)(2,1)} %outer_ref.1) | copy-start | bytes 196612
  216.6 14.9 %all-to-all-start.3 = ((bf16[16,64,256]{2,1,0:T(8,128)(2,1)}), bf16[16,64,256]{2,1,0:T(8,128)(2,1)S(1)}, u32[]{:S(2)}, u32[]{:S(2)}) async-start(bf16[16,64,256]{2,1,0:T(8,128)(2,1)} %bitcast.39), calls=%async_computation.4 | async-start | bytes 1048576 | tf_op jit(solution)/shard_map/all_to_all | solution.py:272
  224.1 17.7 %collective-permute-start.9 = (bf16[2,128,2]{2,1,0:T(8,128)(2,1)S(1)}, bf16[2,128,2]{2,1,0:T(8,128)(2,1)S(1)}, u32[]{:S(2)}, u32[]{:S(2)}) collective-permute-start(bf16[2,128,2]{2,1,0:T(8,128)(2,1)S(1)} %copy.23), channel_id=1, source_target_pairs={{0,16},{16,32},{32,48},{48,64},{64,80},{80,96},{96,112},{112,128},... | collective-permute-start | bytes 3080 | tf_op jit(solution)/shard_map/ppermute | solution.py:152
  231.4 0.8 copy-start.1
  234.5 8.0 %collective-permute-start.10 = (bf16[256,256]{1,0:T(8,128)(2,1)}, bf16[256,256]{1,0:T(8,128)(2,1)S(1)}, u32[]{:S(2)}, u32[]{:S(2)}) collective-permute-start(bf16[256,256]{1,0:T(8,128)(2,1)} %combine.1.refs_0_), channel_id=1, source_target_pairs={{0,2},{2,4},{4,6},{6,8},{8,10},{10,12},{12,14},{14,0},{1,3},{3,5},... | collective-permute-start | bytes 393224 | tf_op jit(solution)/shard_map/ppermute | solution.py:145
  234.5 12.5 %collective-permute-start.11 = (bf16[256,256]{1,0:T(8,128)(2,1)}, bf16[256,256]{1,0:T(8,128)(2,1)S(1)}, u32[]{:S(2)}, u32[]{:S(2)}) collective-permute-start(bf16[256,256]{1,0:T(8,128)(2,1)} %combine.1.refs_0_), channel_id=1, source_target_pairs={{0,14},{2,0},{4,2},{6,4},{8,6},{10,8},{12,10},{14,12},{1,15},{3,1}... | collective-permute-start | bytes 393224 | tf_op jit(solution)/shard_map/ppermute | solution.py:145
  237.7 13.8 %collective-permute-start.12 = (bf16[256,256]{1,0:T(8,128)(2,1)}, bf16[256,256]{1,0:T(8,128)(2,1)S(1)}, u32[]{:S(2)}, u32[]{:S(2)}) collective-permute-start(bf16[256,256]{1,0:T(8,128)(2,1)} %combine.1.refs_0_), channel_id=1, source_target_pairs={{0,4},{2,6},{4,8},{6,10},{8,12},{10,14},{12,0},{14,2},{1,5},{3,7},... | collective-permute-start | bytes 393224 | tf_op jit(solution)/shard_map/ppermute | solution.py:145
  237.7 13.8 %collective-permute-start.13 = (bf16[256,256]{1,0:T(8,128)(2,1)}, bf16[256,256]{1,0:T(8,128)(2,1)S(1)}, u32[]{:S(2)}, u32[]{:S(2)}) collective-permute-start(bf16[256,256]{1,0:T(8,128)(2,1)} %combine.1.refs_0_), channel_id=1, source_target_pairs={{0,12},{2,14},{4,0},{6,2},{8,4},{10,6},{12,8},{14,10},{1,13},{3,15... | collective-permute-start | bytes 393224 | tf_op jit(solution)/shard_map/ppermute | solution.py:145
  241.8 16.5 %collective-permute-start.14 = (bf16[256,256]{1,0:T(8,128)(2,1)}, bf16[256,256]{1,0:T(8,128)(2,1)S(1)}, u32[]{:S(2)}, u32[]{:S(2)}) collective-permute-start(bf16[256,256]{1,0:T(8,128)(2,1)} %combine.1.refs_0_), channel_id=1, source_target_pairs={{0,6},{2,8},{4,10},{6,12},{8,14},{10,0},{12,2},{14,4},{1,7},{3,9},... | collective-permute-start | bytes 393224 | tf_op jit(solution)/shard_map/ppermute | solution.py:145
  242.5 20.1 %copy-start.2 = (bf16[256,256]{1,0:T(8,128)(2,1)}, bf16[256,256]{1,0:T(8,128)(2,1)S(1)}, u32[]{:S(2)}) copy-start(bf16[256,256]{1,0:T(8,128)(2,1)S(1)} %collective-permute-done.10.refs_1_) | copy-start | bytes 393220
  242.5 17.7 %collective-permute-start.15 = (bf16[256,256]{1,0:T(8,128)(2,1)}, bf16[256,256]{1,0:T(8,128)(2,1)S(1)}, u32[]{:S(2)}, u32[]{:S(2)}) collective-permute-start(bf16[256,256]{1,0:T(8,128)(2,1)} %combine.1.refs_0_), channel_id=1, source_target_pairs={{0,10},{2,12},{4,14},{6,0},{8,2},{10,4},{12,6},{14,8},{1,11},{3,13... | collective-permute-start | bytes 393224 | tf_op jit(solution)/shard_map/ppermute | solution.py:145
  247.0 15.6 %copy-start.3 = (bf16[256,256]{1,0:T(8,128)(2,1)}, bf16[256,256]{1,0:T(8,128)(2,1)S(1)}, u32[]{:S(2)}) copy-start(bf16[256,256]{1,0:T(8,128)(2,1)S(1)} %collective-permute-done.11.refs_2_) | copy-start | bytes 393220
  247.0 13.2 %collective-permute-start.16 = (bf16[256,256]{1,0:T(8,128)(2,1)}, bf16[256,256]{1,0:T(8,128)(2,1)S(1)}, u32[]{:S(2)}, u32[]{:S(2)}) collective-permute-start(bf16[256,256]{1,0:T(8,128)(2,1)} %combine.1.refs_0_), channel_id=1, source_target_pairs={{0,8},{2,10},{4,12},{6,14},{8,0},{10,2},{12,4},{14,6},{1,9},{3,11}... | collective-permute-start | bytes 393224 | tf_op jit(solution)/shard_map/ppermute | solution.py:145
  251.5 11.1 %copy-start.4 = (bf16[256,256]{1,0:T(8,128)(2,1)}, bf16[256,256]{1,0:T(8,128)(2,1)S(1)}, u32[]{:S(2)}) copy-start(bf16[256,256]{1,0:T(8,128)(2,1)S(1)} %collective-permute-done.12.refs_3_) | copy-start | bytes 393220
  251.5 9.2 %collective-permute-start.17 = (bf16[256,256]{1,0:T(8,128)(2,1)}, bf16[256,256]{1,0:T(8,128)(2,1)S(1)}, u32[]{:S(2)}, u32[]{:S(2)}) collective-permute-start(bf16[256,256]{1,0:T(8,128)(2,1)} %combine.1.refs_0_), channel_id=1, source_target_pairs={{0,1},{1,0},{2,3},{3,2},{4,5},{5,4},{6,7},{7,6},{8,9},{9,8},{10,11... | collective-permute-start | bytes 393224 | tf_op jit(solution)/shard_map/ppermute | solution.py:282
  251.5 11.1 %copy-start.5 = (bf16[256,256]{1,0:T(8,128)(2,1)}, bf16[256,256]{1,0:T(8,128)(2,1)S(1)}, u32[]{:S(2)}) copy-start(bf16[256,256]{1,0:T(8,128)(2,1)S(1)} %collective-permute-done.13.refs_4_) | copy-start | bytes 393220
  251.5 9.3 %collective-permute-start.18 = (bf16[256,256]{1,0:T(8,128)(2,1)S(1)}, bf16[256,256]{1,0:T(8,128)(2,1)S(1)}, u32[]{:S(2)}, u32[]{:S(2)}) collective-permute-start(bf16[256,256]{1,0:T(8,128)(2,1)S(1)} %collective-permute-done.10.refs_1_), channel_id=1, source_target_pairs={{0,1},{1,0},{2,3},{3,2},{4,5},{5,4},{6,7},{7,6},{8,9},{9,8},{10,11... | collective-permute-start | bytes 393224 | tf_op jit(solution)/shard_map/ppermute | solution.py:282
  258.3 4.3 %copy-start.6 = (bf16[256,256]{1,0:T(8,128)(2,1)}, bf16[256,256]{1,0:T(8,128)(2,1)S(1)}, u32[]{:S(2)}) copy-start(bf16[256,256]{1,0:T(8,128)(2,1)S(1)} %collective-permute-done.14.refs_5_) | copy-start | bytes 393220
  258.3 2.9 collective-permute-start.19
  260.2 2.4 copy-start.7
  260.2 2.0 collective-permute-start.20
  260.2 2.4 copy-start.8
  260.2 2.0 collective-permute-start.21
  260.7 1.9 copy-start.9
  260.7 1.5 collective-permute-start.22
  260.8 1.8 copy-start.10
  260.8 1.4 collective-permute-start.23
  261.3 1.4 copy-start.11
  261.3 1.3 collective-permute-start.24
  262.2 0.6 copy-start.12
  262.2 0.7 copy-start.13
  262.3 0.7 copy-start.14
  262.3 0.7 copy-start.15
  262.6 0.7 copy-start.16
  266.4 23.5 %all-to-all-start.4 = ((bf16[16,128,256]{2,1,0:T(8,128)(2,1)}), bf16[16,128,256]{2,1,0:T(8,128)(2,1)S(1)}, u32[]{:S(2)}, u32[]{:S(2)}) async-start(bf16[16,128,256]{2,1,0:T(8,128)(2,1)} %proj.1), calls=%async_computation.5 | async-start | bytes 2097152 | tf_op jit(solution)/shard_map/all_to_all | solution.py:310
  276.6 10.9 %collective-permute-start.25 = (f32[128,2]{1,0:T(8,128)S(1)}, f32[128,2]{1,0:T(8,128)S(1)}, u32[]{:S(2)}, u32[]{:S(2)}) collective-permute-start(f32[128,2]{1,0:T(8,128)S(1)} %slice.52), channel_id=1, source_target_pairs={{16,0},{32,16},{48,32},{64,48},{80,64},{96,80},{112,96},{128,112},... | collective-permute-start | bytes 3080 | tf_op jit(solution)/shard_map/ppermute | solution.py:152
Sparse Core Ops, SparseCore 0:
  26.3 69.6 all-gather.1
  138.5 78.0 reduce-scatter.1

commit v2 on v1

--- a/solution.py
+++ b/solution.py
@@ -26,11 +26,17 @@
     return lax.dot_general(a, b, (((0,), (0,)), ((), ())), preferred_element_type=F32)
 
 
+def grant(mib):
+    return pltpu.CompilerParams(vmem_limit_bytes=mib << 20)
+
+
 def cost(flops, nbytes):
     return pl.CostEstimate(flops=int(flops), bytes_accessed=int(nbytes), transcendentals=0)
 
 
-def route_kernel(experts, cap, ids_ref, wts_ref, state_ref, sent_ref, pick_ref, scale_ref):
+def route_kernel(
+    experts, cap, early, ids_ref, wts_ref, state_ref, cot_ref, sent_ref, pick_ref, late_ref, scale_ref
+):
     tokens = ids_ref.shape[1]
     first, second = ids_ref[0:1, :], ids_ref[1:2, :]
     expert = lax.broadcasted_iota(jnp.int32, (experts, tokens), 0)
@@ -43,70 +49,149 @@
     slot = jnp.where(named, earlier.astype(jnp.int32), -1)
     weight = jnp.where(is_first, wts_ref[0:1, :], jnp.where(is_second, wts_ref[1:2, :], 0.0))
     place = lax.broadcasted_iota(jnp.int32, (cap, tokens), 0)
+    hits, scales = [], []
     for e in range(experts):
         hit = slot[e : e + 1, :] == place
-        pick_ref[e * cap : (e + 1) * cap, :] = hit.astype(F32).astype(BF16)
-        taken = jnp.sum(jnp.where(hit, weight[e : e + 1, :], 0.0), axis=1, keepdims=True)
-        scale_ref[e * cap : (e + 1) * cap, :] = jnp.broadcast_to(taken, (cap, 128))
-    sent_ref[...] = dot_nn(pick_ref[...], state_ref[...]).astype(BF16)
-
-
-def spread_kernel(pick_ref, scale_ref, *refs):
-    pieces, (low_ref, high_ref) = refs[:-2], refs[-2:]
+        hits.append(hit.astype(F32))
+        scales.append(jnp.sum(jnp.where(hit, weight[e : e + 1, :], 0.0), axis=1, keepdims=True))
+    pick = jnp.concatenate(hits, axis=0).astype(BF16)
+    pick_ref[...] = pick
+    late_ref[...] = jnp.concatenate([hit[early:] for hit in hits], axis=0).astype(BF16)
+    late_scale = jnp.concatenate([taken[early:] for taken in scales], axis=0)
+    scale_ref[...] = jnp.broadcast_to(late_scale, scale_ref.shape)
+    state_rows = dot_nn(pick, state_ref[...])
+    soon = jnp.concatenate([hit[:early] for hit in hits], axis=0).astype(BF16)
+    soon_rows = dot_nn(soon, cot_ref[...]) * jnp.concatenate(
+        [taken[:early] for taken in scales], axis=0
+    )
+    both = []
+    for e in range(experts):
+        both += [state_rows[e * cap : (e + 1) * cap], soon_rows[e * early : (e + 1) * early]]
+    sent_ref[...] = jnp.concatenate(both, axis=0).astype(BF16)
+
+
+def spread_kernel(late_ref, scale_ref, *refs):
+    pieces, out_ref = refs[:-1], refs[-1]
     width = pieces[0].shape[1]
-    half = len(pieces) // 2
     scale = scale_ref[:, 0:1]
     for j, piece in enumerate(pieces):
-        rows = (dot_nn(pick_ref[...], piece[...]) * scale).astype(BF16)
-        out = low_ref if j < half else high_ref
-        out[:, (j % half) * width : (j % half + 1) * width] = rows
-
-
-def expert_kernel(
-    slab_ref, state_ref, ml_ref, mh_ref, tl_ref, th_ref, wg_ref, wu_ref, wd_ref, part_ref, act_ref, wgu_ref
+        rows = (dot_nn(late_ref[...], piece[...]) * scale).astype(BF16)
+        out_ref[:, j * width : (j + 1) * width] = rows
+
+
+def down_columns(slab_ref, base, wd_ref, count, width):
+    pieces = [
+        wd_ref[:, pl.ds(pl.multiple_of(slab_ref[base + j] * width, width), width)]
+        for j in range(count)
+    ]
+    return jnp.concatenate(pieces, axis=1)
+
+
+def expert_first_kernel(
+    cap,
+    early,
+    slab_ref,
+    state_ref,
+    mine_ref,
+    their_ref,
+    wg_ref,
+    wu_ref,
+    wdk_ref,
+    wd_ref,
+    pre_ref,
+    acc_ref,
+    late_ref,
 ):
     slabs, width = state_ref.shape[0], state_ref.shape[2]
     hidden_n = wd_ref.shape[0]
+    step, steps = pl.program_id(0), pl.num_programs(0)
+    rows = jnp.concatenate([state_ref[s] for s in range(slabs)], axis=1)
+    weights = jnp.concatenate([wg_ref[...], wu_ref[...], wdk_ref[...]], axis=0)
+    acc = dot_nt(rows, weights)
+
+    def down(base):
+        at = pl.multiple_of(slab_ref[base + step] * width, width)
+        return wd_ref[:, pl.ds(at, width)]
+
+    late = dot_nt(mine_ref[...], down(0)) + dot_nt(their_ref[...], down(2 * steps))
+
+    @pl.when(step == 0)
+    def _():
+        acc_ref[...] = acc
+        late_ref[...] = late
+
+    @pl.when(step > 0)
+    def _():
+        acc_ref[...] += acc
+        late_ref[...] += late
+
+    @pl.when(step == steps - 1)
+    def _():
+        late_n, own = cap - early, cap + early
+        for i in range(acc_ref.shape[0] // own):
+            at, to, few = i * own, i * cap, i * late_n
+            pre_ref[to : to + cap, : 2 * hidden_n] = acc_ref[at : at + cap, : 2 * hidden_n]
+            pre_ref[to : to + early, 2 * hidden_n :] = acc_ref[at + cap : at + own, 2 * hidden_n :]
+            pre_ref[to + early : to + cap, 2 * hidden_n :] = late_ref[few : few + late_n]
+
+
+def expert_second_kernel(
+    cap, early, slab_ref, pre_ref, mine_ref, their_ref, wg_ref, wu_ref, wd_ref, part_ref, act_ref, late_ref, w_ref
+):
+    slabs, width = part_ref.shape[0], part_ref.shape[2]
+    hidden_n = wd_ref.shape[0]
 
     @pl.when(pl.program_id(0) == 0)
     def _():
-        wgu_ref[:hidden_n] = wg_ref[...]
-        wgu_ref[hidden_n:] = wu_ref[...]
-
-    rows = jnp.concatenate([state_ref[s] for s in range(slabs)], axis=1)
-    pre = dot_nt(rows, wgu_ref[...])
-    gate_pre, up_pre = pre[:, :hidden_n], pre[:, hidden_n:]
-    back_hidden = jnp.zeros(gate_pre.shape, F32)
-    per = ml_ref.shape[1] // width
-    for q, ref in enumerate((ml_ref, mh_ref, tl_ref, th_ref)):
-        pieces = [
-            wd_ref[:, pl.ds(pl.multiple_of(slab_ref[q * per + j] * width, width), width)]
-            for j in range(per)
-        ]
-        back_hidden = back_hidden + dot_nt(ref[...], jnp.concatenate(pieces, axis=1))
+        w_ref[:hidden_n] = wg_ref[...]
+        w_ref[hidden_n:] = wu_ref[...]
+
+    per = mine_ref.shape[1] // width
+    late = dot_nt(mine_ref[...], down_columns(slab_ref, per, wd_ref, per, width))
+    late = late + dot_nt(their_ref[...], down_columns(slab_ref, 3 * per, wd_ref, per, width))
+    late_n = cap - early
+    groups = range(pre_ref.shape[0] // cap)
+    none = jnp.zeros((early, hidden_n), F32)
+    more = jnp.concatenate(
+        [x for i in groups for x in (none, late[i * late_n : (i + 1) * late_n])], axis=0
+    )
+    gate_pre, up_pre = pre_ref[:, :hidden_n], pre_ref[:, hidden_n : 2 * hidden_n]
+    back_hidden = pre_ref[:, 2 * hidden_n :] + more
     sig_gate = jax.nn.sigmoid(gate_pre)
     silu_gate = gate_pre * sig_gate
-    hidden = (silu_gate * up_pre).astype(BF16)
-    back_gate = (back_hidden * up_pre * sig_gate * (1.0 + gate_pre * (1.0 - sig_gate))).astype(BF16)
-    back_up = (back_hidden * silu_gate).astype(BF16)
+    hidden = silu_gate * up_pre
+    back_gate = back_hidden * up_pre * sig_gate * (1.0 + gate_pre * (1.0 - sig_gate))
+    back_up = back_hidden * silu_gate
     back = jnp.concatenate([back_gate, back_up], axis=1)
-    act_ref[:, : 2 * hidden_n] = back
-    act_ref[:, 2 * hidden_n :] = hidden
+    rounded = back.astype(BF16)
     for s in range(slabs):
-        part_ref[s] = dot_nn(back, wgu_ref[:, s * width : (s + 1) * width]).astype(BF16)
-
-
-def weight_grad_kernel(slab_ref, act_ref, state_ref, ml_ref, mh_ref, tl_ref, th_ref, gg_ref, gu_ref, gd_ref):
+        part_ref[s] = dot_nn(rounded, w_ref[:, s * width : (s + 1) * width]).astype(BF16)
+    nothing = jnp.zeros((cap, hidden_n), F32)
+    wide = jnp.zeros((early, 2 * hidden_n), F32)
+    act_ref[:, : 2 * hidden_n] = jnp.concatenate(
+        [x for i in groups for x in (back[i * cap : (i + 1) * cap], wide)], axis=0
+    ).astype(BF16)
+    act_ref[:, 2 * hidden_n :] = jnp.concatenate(
+        [x for i in groups for x in (nothing, hidden[i * cap : i * cap + early])], axis=0
+    ).astype(BF16)
+    late_ref[...] = jnp.concatenate(
+        [hidden[i * cap + early : (i + 1) * cap] for i in groups], axis=0
+    ).astype(BF16)
+
+
+def weight_grad_kernel(
+    slab_ref, act_ref, late_ref, state_ref, ml_ref, mh_ref, tl_ref, th_ref, gg_ref, gu_ref, gd_ref
+):
     hidden_n = gg_ref.shape[0]
     step, per = pl.program_id(0), pl.num_programs(0) // 4
-    both = dot_tn(act_ref[:, : 2 * hidden_n], state_ref[0])
-    gg_ref[...] = both[:hidden_n]
-    gu_ref[...] = both[hidden_n:]
+    every = dot_tn(act_ref[...], state_ref[0])
+    gg_ref[...] = every[:hidden_n]
+    gu_ref[...] = every[hidden_n : 2 * hidden_n]
     for q, ref in enumerate((ml_ref, mh_ref, tl_ref, th_ref)):
 
         @pl.when(step // per == q)
         def _(ref=ref):
-            gd_ref[...] = dot_tn(act_ref[:, 2 * hidden_n :], ref[...])
+            gd_ref[...] = every[2 * hidden_n :] + dot_tn(late_ref[...], ref[...])
 
 
 def combine_kernel(pick_ref, rows_ref, cot_ref, out_ref):
@@ -181,63 +266,99 @@
 
     cot_pieces = gathered(cotangent, "z")
 
-    sent_state, pick, scale = pl.pallas_call(
-        functools.partial(route_kernel, experts, cap),
+    early = cap // 8
+    late_n = cap - early
+    own, late_rows = experts * (cap + early), experts * late_n
+    sent_rows, pick, late_pick, late_scale = pl.pallas_call(
+        functools.partial(route_kernel, experts, cap, early),
         out_shape=(
-            shape((slots, width), BF16),
+            shape((own, width), BF16),
             shape((slots, tok_count), BF16),
-            shape((slots, 128), F32),
+            shape((late_rows, tok_count), BF16),
+            shape((late_rows, 128), F32),
         ),
         cost_estimate=cost(2 * slots * tok_count * width, 4 * slots * width),
         name="route",
-    )(route_ids.T, route_weights.T, mixed_state)
-    recv_state = lax.all_to_all(
-        sent_state.reshape(experts, cap, width), "sp", split_axis=0, concat_axis=0, tiled=True
-    )
-    state_all = lax.all_gather(recv_state.reshape(slots, width), TP, axis=0, tiled=False)
+    compiler_params=grant(20),
+    )(route_ids.T, route_weights.T, mixed_state, cotangent)
+    recv_rows = lax.all_to_all(
+        sent_rows.reshape(experts, cap + early, width), "sp", split_axis=0, concat_axis=0, tiled=True
+    )
+    state_all = lax.all_gather(recv_rows.reshape(own, width), TP, axis=0, tiled=False)
 
     half = z_size // 2 * width
-    cot_low, cot_high = pl.pallas_call(
-        spread_kernel,
-        out_shape=(shape((slots, half), BF16),) * 2,
-        cost_estimate=cost(4 * slots * tok_count * half, 8 * slots * half),
-        name="spread",
-    )(pick, scale, *cot_pieces)
     swap = [(0, 1), (1, 0)]
+
+    def spread(pieces):
+      return pl.pallas_call(
+          spread_kernel,
+          out_shape=shape((late_rows, half), BF16),
+          cost_estimate=cost(2 * late_rows * tok_count * half, 4 * late_rows * half),
+          compiler_params=grant(12),
+      )(late_pick, late_scale, *pieces)
 
     def exchanged(part):
         got = lax.all_to_all(
-            part.reshape(experts, cap, half), "sp", split_axis=0, concat_axis=0, tiled=True
-        ).reshape(slots, half)
+            part.reshape(experts, late_n, half), "sp", split_axis=0, concat_axis=0, tiled=True
+        ).reshape(late_rows, half)
         return got, lax.ppermute(got, "c", swap)
 
-    my_low, their_low = exchanged(cot_low)
-    my_high, their_high = exchanged(cot_high)
+    my_low, their_low = exchanged(spread(cot_pieces[: z_size // 2]))
+    my_high, their_high = exchanged(spread(cot_pieces[z_size // 2 :]))
     cots = (my_low, my_high, their_low, their_high)
 
-    block = 256
+    steps = 4
     whole = lambda *dims: pl.BlockSpec(dims, lambda *_: (0,) * len(dims))
-    cot_rows = pl.BlockSpec((block, half), lambda r, core: (r, 0))
-    partial_value, acts = pl.pallas_call(
-        expert_kernel,
+    by_rows = lambda *dims: pl.BlockSpec(dims, lambda r, slab: (r, 0))
+    weights = (w_gate[0], w_up[0], w_down[0])
+    pre = pl.pallas_call(
+        functools.partial(expert_first_kernel, cap, early),
         grid_spec=pltpu.PrefetchScalarGridSpec(
             num_scalar_prefetch=1,
-            grid=(slots // block,),
+            grid=(steps,),
             in_specs=[
-                pl.BlockSpec((slabs, block, width), lambda r, core: (0, r, 0)),
-                *[cot_rows] * 4,
+                pl.BlockSpec((slabs // steps, own, width), lambda k, slab: (k, 0, 0)),
+                *[pl.BlockSpec((late_rows, width), lambda k, slab: (0, k))] * 2,
+                *[pl.BlockSpec((hidden_n, features // steps), lambda k, slab: (0, k))] * 3,
+                whole(hidden_n, features),
+            ],
+            out_specs=whole(slots, 3 * hidden_n),
+            scratch_shapes=[
+                pltpu.VMEM((own, 3 * hidden_n), F32),
+                pltpu.VMEM((late_rows, hidden_n), F32),
+            ],
+        ),
+        out_shape=shape((slots, 3 * hidden_n), F32),
+        cost_estimate=cost(6 * slots * hidden_n * features, 3 * slots * features),
+        name="expert_first",
+    compiler_params=grant(57),
+    )(slab_of, state_all, my_low, their_low, *weights, w_down[0])
+    partial_value, acts, late_acts = pl.pallas_call(
+        functools.partial(expert_second_kernel, cap, early),
+        grid_spec=pltpu.PrefetchScalarGridSpec(
+            num_scalar_prefetch=1,
+            grid=(steps,),
+            in_specs=[
+                by_rows(slots // steps, 3 * hidden_n),
+                *[by_rows(late_rows // steps, half)] * 2,
                 *[whole(hidden_n, features)] * 3,
             ],
             out_specs=[
-                pl.BlockSpec((slabs, block, width), lambda r, core: (0, r, 0)),
-                pl.BlockSpec((block, 3 * hidden_n), lambda r, core: (r, 0)),
+                pl.BlockSpec((slabs, slots // steps, width), lambda r, slab: (0, r, 0)),
+                by_rows(own // steps, 3 * hidden_n),
+                by_rows(late_rows // steps, hidden_n),
             ],
             scratch_shapes=[pltpu.VMEM((2 * hidden_n, features), BF16)],
         ),
-        out_shape=(shape((slabs, slots, width), BF16), shape((slots, 3 * hidden_n), BF16)),
-        cost_estimate=cost(10 * slots * hidden_n * features, 6 * slots * features),
-        name="expert",
-    )(slab_of, state_all, *cots, w_gate[0], w_up[0], w_down[0])
+        out_shape=(
+            shape((slabs, slots, width), BF16),
+            shape((own, 3 * hidden_n), BF16),
+            shape((late_rows, hidden_n), BF16),
+        ),
+        cost_estimate=cost(5 * slots * hidden_n * features, 4 * slots * features),
+        name="expert_second",
+        compiler_params=grant(57),
+    )(slab_of, pre, my_high, their_high, *weights)
 
     row_back = lax.psum_scatter(partial_value, TP, scatter_dimension=0, tiled=False)
 
@@ -245,7 +366,7 @@
 
     def cot_piece(q):
         return pl.BlockSpec(
-            (slots, width), lambda s, core: (0, jnp.clip(s - q * quarter, 0, quarter - 1))
+            (late_rows, width), lambda s, slab: (0, jnp.clip(s - q * quarter, 0, quarter - 1))
         )
 
     grad_out = pl.BlockSpec((hidden_n, width), lambda s, slab: (0, slab[s]))
@@ -255,8 +376,9 @@
             num_scalar_prefetch=1,
             grid=(slabs,),
             in_specs=[
-                whole(slots, 3 * hidden_n),
-                pl.BlockSpec((1, slots, width), lambda s, slab: (slab[s], 0, 0)),
+                whole(own, 3 * hidden_n),
+                whole(late_rows, hidden_n),
+                pl.BlockSpec((1, own, width), lambda s, slab: (slab[s], 0, 0)),
                 *[cot_piece(q) for q in range(4)],
             ],
             out_specs=[grad_out] * 3,
@@ -264,7 +386,8 @@
         out_shape=(shape((hidden_n, features), F32),) * 3,
         cost_estimate=cost(6 * slots * hidden_n * features, 6 * slots * features),
         name="weight_grads",
-    )(slab_of, acts, state_all, *cots)
+        compiler_params=grant(57),
+    )(slab_of, acts, late_acts, state_all, *cots)
     row_back, grad_gate, grad_up, grad_down = lax.optimization_barrier(
         (row_back, grad_gate, grad_up, grad_down)
     )
@@ -277,6 +400,7 @@
         out_shape=shape((tok_count, width), BF16),
         cost_estimate=cost(2 * slots * tok_count * width, 4 * slots * width),
         name="combine",
+        compiler_params=grant(16),
     )(pick, arrived, cotangent)
     near = gathered(grad_mixed, "z")
     full_back = near + [lax.ppermute(piece, "c", swap) for piece in near]
@@ -306,6 +430,7 @@
         out_shape=shape((slabs, channels, width), BF16),
         cost_estimate=cost(2 * channels * tok_count * features, 4 * tok_count * features),
         name="proj",
+        compiler_params=grant(14),
     )(slab_of, mixer_act, *full_back)
     landed = lax.all_to_all(proj_term, "sp", split_axis=0, concat_axis=0, tiled=True)
     grad_proj = jnp.sum(landed.astype(F32), axis=0)
@@ -315,6 +440,7 @@
         out_shape=(shape((channels, tok_count), BF16), shape((channels, tok_count), F32)),
         cost_estimate=cost(2 * channels * tok_count * features, 4 * tok_count * features),
         name="mixer",
+        compiler_params=grant(14),
     )(slab_of, out_proj, conv_out, conv_outer, *full_back)
     tail_back = from_behind(back_conv[:, :rim_width], "sp", -1)
     back_ext = jnp.concatenate([back_conv, tail_back], axis=1)

time: 303 us -> 289 us (0.954)
  the two profiles are of different devices: /device:TPU:24 before, /device:TPU:32 now
where the time goes in v2:
time: 289 us; the launch traced here: 288 us
  waiting for transfers between devices  130 us (45%)
  starting transfers between devices  63.3 us (22%)
  Pallas kernels  52.4 us (18%)
  blocking collectives  19.2 us (7%)
  between operations  14.3 us (5%)
  local copies, waits for them, and re-layouts  4.62 us (2%)
  other arithmetic  4.43 us (2%)
    ppermute x14, waiting for transfers between devices, gathered(): lax.ppermute(value, axis, [(i, (i + k) % size) for i in range(size)])  42.5 us
    reduce_scatter x1, waiting for transfers between devices, shards(): lax.psum_scatter(partial_value, TP, scatter_dimension=0, tiled=False)  41.1 us
    ppermute x14, starting transfers between devices, gathered(): lax.ppermute(value, axis, [(i, (i + k) % size) for i in range(size)])  34.3 us
    all_to_all x2, waiting for transfers between devices, exchanged(): lax.all_to_all(part.reshape(experts, late_n, half), 'sp', split_axis=0, c...  24 us
    pallas_call x1, Pallas kernels, shards(): pl.pallas_call(weight_grad_kernel, grid_spec=pltpu.PrefetchScalarGridSpec...  20.6 us
    all_to_all x1, blocking collectives, shards(): lax.all_to_all(sent_rows.reshape(experts, cap + early, width), 'sp', spli...  19.2 us
    pallas_call x1, Pallas kernels, shards(): pl.pallas_call(functools.partial(expert_first_kernel, cap, early), grid_s...  12.3 us
    ppermute x2, waiting for transfers between devices, from_behind(): lax.ppermute(value, axis, [(source, source + steps) for source in range(f...  12.1 us
  transfers between devices with their start and end apart: 32, of which 17 were waited for; matrix products, arithmetic and copies ran while one was open for 1% of the time, Pallas kernels for 14%

profile of v2, /device:TPU:32, one launch (start us, length us, event | category | flops | bytes accessed | tf_op | source)
XLA Modules:
  0.0 287.8 jit_solution(6946655224394293561)
XLA Ops:
  7.2 0.9 copy-done.3
  8.1 0.9 copy-done.7
  9.0 0.7 copy-done.8
  9.7 0.7 copy-done.9
  10.4 0.7 route.1
  11.0 19.2 %all_to_all.25 = bf16[16,72,256]{2,1,0:T(8,128)(2,1)} all-to-all(bf16[16,72,256]{2,1,0:T(8,128)(2,1)S(1)} %bitcast.30), channel_id=1, replica_groups=mesh['sp'=16,'z'=8,'c'=2] {'sp'}, dimensions={0} | all-to-all | bytes 1179648 | tf_op jit(solution)/shard_map/all_to_all | solution.py:284
  30.3 2.0 collective-permute-start
  32.3 0.1 collective-permute-start.1
  32.4 4.4 %collective-permute-start.2 = (bf16[256,256]{1,0:T(8,128)(2,1)S(1)}, bf16[256,256]{1,0:T(8,128)(2,1)S(1)}, u32[]{:S(2)}, u32[]{:S(2)}) collective-permute-start(bf16[256,256]{1,0:T(8,128)(2,1)S(1)} %copy-done.4), channel_id=1, source_target_pairs={{0,4},{2,6},{4,8},{6,10},{8,12},{10,14},{12,0},{14,2},{1,5},{3,7},... | collective-permute-start | bytes 393224 | tf_op jit(solution)/shard_map/ppermute | solution.py:230
  36.8 0.5 collective-permute-done.1.refs_2_
  37.3 4.5 %collective-permute-done.2.refs_3_ = bf16[256,256]{1,0:T(8,128)(2,1)S(1)} collective-permute-done((bf16[256,256]{1,0:T(8,128)(2,1)S(1)}, bf16[256,256]{1,0:T(8,128)(2,1)S(1)}, u32[]{:S(2)}, u32[]{:S(2)}) %collective-permute-start.2) | collective-permute-done | bytes 131104 | tf_op jit(solution)/shard_map/ppermute | solution.py:230
  41.8 1.9 shard_map.188
  43.7 3.7 %all-to-all-start.1 = ((bf16[16,56,1024]{2,1,0:T(8,128)(2,1)}), bf16[16,56,1024]{2,1,0:T(8,128)(2,1)S(1)}, u32[]{:S(2)}, u32[]{:S(2)}) async-start(bf16[16,56,1024]{2,1,0:T(8,128)(2,1)} %bitcast.4), calls=%async_computation.1 | async-start | bytes 3670016 | tf_op jit(solution)/shard_map/all_to_all | solution.py:301
  47.4 4.7 %collective-permute-start.4 = (bf16[256,256]{1,0:T(8,128)(2,1)S(1)}, bf16[256,256]{1,0:T(8,128)(2,1)S(1)}, u32[]{:S(2)}, u32[]{:S(2)}) collective-permute-start(bf16[256,256]{1,0:T(8,128)(2,1)S(1)} %copy-done.4), channel_id=1, source_target_pairs={{0,12},{2,14},{4,0},{6,2},{8,4},{10,6},{12,8},{14,10},{1,13},{3,15... | collective-permute-start | bytes 393224 | tf_op jit(solution)/shard_map/ppermute | solution.py:230
  52.1 3.4 %collective-permute-start.5 = (bf16[256,256]{1,0:T(8,128)(2,1)S(1)}, bf16[256,256]{1,0:T(8,128)(2,1)S(1)}, u32[]{:S(2)}, u32[]{:S(2)}) collective-permute-start(bf16[256,256]{1,0:T(8,128)(2,1)S(1)} %copy-done.4), channel_id=1, source_target_pairs={{0,6},{2,8},{4,10},{6,12},{8,14},{10,0},{12,2},{14,4},{1,7},{3,9},... | collective-permute-start | bytes 393224 | tf_op jit(solution)/shard_map/ppermute | solution.py:230
  55.5 1.7 collective-permute-start.6
  57.2 1.8 collective-permute-start.7
  58.9 4.3 %collective-permute-done.4.refs_0_ = bf16[256,256]{1,0:T(8,128)(2,1)S(1)} collective-permute-done((bf16[256,256]{1,0:T(8,128)(2,1)S(1)}, bf16[256,256]{1,0:T(8,128)(2,1)S(1)}, u32[]{:S(2)}, u32[]{:S(2)}) %collective-permute-start.4) | collective-permute-done | bytes 131104 | tf_op jit(solution)/shard_map/ppermute | solution.py:230
  63.2 5.9 %collective-permute-done.5.refs_1_ = bf16[256,256]{1,0:T(8,128)(2,1)S(1)} collective-permute-done((bf16[256,256]{1,0:T(8,128)(2,1)S(1)}, bf16[256,256]{1,0:T(8,128)(2,1)S(1)}, u32[]{:S(2)}, u32[]{:S(2)}) %collective-permute-start.5) | collective-permute-done | bytes 131104 | tf_op jit(solution)/shard_map/ppermute | solution.py:230
  69.1 6.0 %collective-permute-done.6.refs_2_ = bf16[256,256]{1,0:T(8,128)(2,1)S(1)} collective-permute-done((bf16[256,256]{1,0:T(8,128)(2,1)S(1)}, bf16[256,256]{1,0:T(8,128)(2,1)S(1)}, u32[]{:S(2)}, u32[]{:S(2)}) %collective-permute-start.6) | collective-permute-done | bytes 131104 | tf_op jit(solution)/shard_map/ppermute | solution.py:230
  75.1 6.8 %collective-permute-done.7.refs_3_ = bf16[256,256]{1,0:T(8,128)(2,1)S(1)} collective-permute-done((bf16[256,256]{1,0:T(8,128)(2,1)S(1)}, bf16[256,256]{1,0:T(8,128)(2,1)S(1)}, u32[]{:S(2)}, u32[]{:S(2)}) %collective-permute-start.7) | collective-permute-done | bytes 131104 | tf_op jit(solution)/shard_map/ppermute | solution.py:230
  81.9 1.9 shard_map.189
  83.8 7.2 %all-to-all-start.2 = ((bf16[16,56,1024]{2,1,0:T(8,128)(2,1)}), bf16[16,56,1024]{2,1,0:T(8,128)(2,1)}, u32[]{:S(2)}, u32[]{:S(2)}) async-start(bf16[16,56,1024]{2,1,0:T(8,128)(2,1)} %bitcast.9), calls=%async_computation.2 | async-start | bytes 3670016 | tf_op jit(solution)/shard_map/all_to_all | solution.py:301
  91.0 0.1 collective-permute-start.3
  91.2 24.0 %all-to-all-done.2 = bf16[16,56,1024]{2,1,0:T(8,128)(2,1)} async-done(((bf16[16,56,1024]{2,1,0:T(8,128)(2,1)}), bf16[16,56,1024]{2,1,0:T(8,128)(2,1)}, u32[]{:S(2)}, u32[]{:S(2)}) %all-to-all-start.2) | async-done | bytes 1835040 | tf_op jit(solution)/shard_map/all_to_all | solution.py:301
  115.2 0.6 pad_add_fusion.slab_ref
  115.8 12.3 %expert_first.1.pre_ref = f32[1024,384]{1,0:T(8,128)} custom-call(s32[16]{0:T(128)} %pad_add_fusion.slab_ref, bf16[16,1152,256]{2,1,0:T(8,128)(2,1)} %all-gather.2.cloned.1.call-done.state_ref, bf16[896,1024]{1,0:T(8,128)(2,1)} %bitcast.34, bf16[896,1024]{1,0:T(8,128)(2,1)} %collective-permute-done.3.their_ref.tl_ref, bf16[128,4096]{1,0:T(8,128)(2,1)} %bitcast.40, ...), custom_call_target="tpu_custom_call" | custom-call | flops 3221225472 | bytes 12582912 | tf_op jit(solution)/shard_map/expert_first/pallas_call | solution.py:314
  128.1 10.2 %expert_second.1 = (bf16[16,1024,256]{2,1,0:T(8,128)(2,1)}, bf16[1152,384]{1,0:T(8,128)(2,1)}, bf16[896,128]{1,0:T(8,128)(2,1)}) custom-call(s32[16]{0:T(128)} %pad_add_fusion.slab_ref, f32[1024,384]{1,0:T(8,128)} %expert_first.1.pre_ref, bf16[896,1024]{1,0:T(8,128)(2,1)} %bitcast.10.mine_ref.mh_ref, ...), custom_call_target="tpu_custom_call" | custom-call | flops 2684354560 | bytes 16777216 | tf_op jit(solution)/shard_map/expert_second/pallas_call | solution.py:336
  138.3 20.6 %weight_grads.1 = (f32[128,4096]{1,0:T(8,128)}, f32[128,4096]{1,0:T(8,128)}, f32[128,4096]{1,0:T(8,128)}) custom-call(s32[16]{0:T(128)} %pad_add_fusion.slab_ref, bf16[1152,384]{1,0:T(8,128)(2,1)} %get-tuple-element.28.act_ref, bf16[896,128]{1,0:T(8,128)(2,1)} %get-tuple-element.29.late_ref, bf16[16,1152,256]{2,1,0:T(8,128)(2,1)} %all-gather.2.cloned.1.call-done.state_ref, ...), custom_call_target="tpu_custom_call" | custom-call | flops 3221225472 | bytes 25165824 | tf_op jit(solution)/shard_map/weight_grads/pallas_call | solution.py:373
  158.9 41.1 %reduce-scatter.2.cloned.1.call-done = bf16[1,1024,256]{2,1,0:T(8,128)(2,1)} async-done(((bf16[16,1024,256]{2,1,0:T(8,128)(2,1)}), bf16[1,1024,256]{2,1,0:T(8,128)(2,1)}) %reduce-scatter.2.cloned.1.call-update) | async-done | bytes 524304 | tf_op jit(solution)/shard_map/reduce_scatter | solution.py:363
  200.0 6.7 %all-to-all-start.3 = ((bf16[16,64,256]{2,1,0:T(8,128)(2,1)}), bf16[16,64,256]{2,1,0:T(8,128)(2,1)S(1)}, u32[]{:S(2)}, u32[]{:S(2)}) async-start(bf16[16,64,256]{2,1,0:T(8,128)(2,1)} %bitcast.44), calls=%async_computation.4 | async-start | bytes 1048576 | tf_op jit(solution)/shard_map/all_to_all | solution.py:395
  206.9 0.1 slice.43
  207.1 0.2 copy.23
  207.3 3.8 %collective-permute-start.9 = (bf16[2,128,2]{2,1,0:T(8,128)(2,1)S(1)}, bf16[2,128,2]{2,1,0:T(8,128)(2,1)S(1)}, u32[]{:S(2)}, u32[]{:S(2)}) collective-permute-start(bf16[2,128,2]{2,1,0:T(8,128)(2,1)S(1)} %copy.23), channel_id=1, source_target_pairs={{0,16},{16,32},{32,48},{48,64},{64,80},{80,96},{96,112},{112,128},... | collective-permute-start | bytes 3080 | tf_op jit(solution)/shard_map/ppermute | solution.py:237
  211.1 7.2 %all-to-all-done.3 = bf16[16,64,256]{2,1,0:T(8,128)(2,1)S(1)} async-done(((bf16[16,64,256]{2,1,0:T(8,128)(2,1)}), bf16[16,64,256]{2,1,0:T(8,128)(2,1)S(1)}, u32[]{:S(2)}, u32[]{:S(2)}) %all-to-all-start.3) | async-done | bytes 524320 | tf_op jit(solution)/shard_map/all_to_all | solution.py:395
  218.3 1.0 combine.1.refs_0_
  219.3 2.7 collective-permute-start.11
  222.0 3.5 %collective-permute-start.12 = (bf16[256,256]{1,0:T(8,128)(2,1)}, bf16[256,256]{1,0:T(8,128)(2,1)S(1)}, u32[]{:S(2)}, u32[]{:S(2)}) collective-permute-start(bf16[256,256]{1,0:T(8,128)(2,1)} %combine.1.refs_0_), channel_id=1, source_target_pairs={{0,4},{2,6},{4,8},{6,10},{8,12},{10,14},{12,0},{14,2},{1,5},{3,7},... | collective-permute-start | bytes 393224 | tf_op jit(solution)/shard_map/ppermute | solution.py:230
  225.5 0.6 collective-permute-start.13
  226.1 6.2 %collective-permute-start.14 = (bf16[256,256]{1,0:T(8,128)(2,1)}, bf16[256,256]{1,0:T(8,128)(2,1)S(1)}, u32[]{:S(2)}, u32[]{:S(2)}) collective-permute-start(bf16[256,256]{1,0:T(8,128)(2,1)} %combine.1.refs_0_), channel_id=1, source_target_pairs={{0,6},{2,8},{4,10},{6,12},{8,14},{10,0},{12,2},{14,4},{1,7},{3,9},... | collective-permute-start | bytes 393224 | tf_op jit(solution)/shard_map/ppermute | solution.py:230
  232.4 3.2 %collective-permute-start.16 = (bf16[256,256]{1,0:T(8,128)(2,1)}, bf16[256,256]{1,0:T(8,128)(2,1)S(1)}, u32[]{:S(2)}, u32[]{:S(2)}) collective-permute-start(bf16[256,256]{1,0:T(8,128)(2,1)} %combine.1.refs_0_), channel_id=1, source_target_pairs={{0,8},{2,10},{4,12},{6,14},{8,0},{10,2},{12,4},{14,6},{1,9},{3,11}... | collective-permute-start | bytes 393224 | tf_op jit(solution)/shard_map/ppermute | solution.py:230
  235.6 0.5 collective-permute-start.18
  236.1 9.6 %collective-permute-done.14.refs_5_ = bf16[256,256]{1,0:T(8,128)(2,1)S(1)} collective-permute-done((bf16[256,256]{1,0:T(8,128)(2,1)}, bf16[256,256]{1,0:T(8,128)(2,1)S(1)}, u32[]{:S(2)}, u32[]{:S(2)}) %collective-permute-start.14) | collective-permute-done | bytes 131104 | tf_op jit(solution)/shard_map/ppermute | solution.py:230
  245.8 0.1 convert_multiply_fusion
  245.9 4.8 %collective-permute-done.15.refs_6_ = bf16[256,256]{1,0:T(8,128)(2,1)S(1)} collective-permute-done((bf16[256,256]{1,0:T(8,128)(2,1)}, bf16[256,256]{1,0:T(8,128)(2,1)S(1)}, u32[]{:S(2)}, u32[]{:S(2)}) %collective-permute-start.15) | collective-permute-done | bytes 131104 | tf_op jit(solution)/shard_map/ppermute | solution.py:230
  250.7 0.5 collective-permute-start.21
  251.2 0.1 collective-permute-start.22
  251.3 0.4 collective-permute-start.23
  251.8 0.1 collective-permute-start.24
  251.8 0.2 multiply_convert_fusion.2
  252.1 0.2 collective-permute-done.21.refs_12_
  252.3 0.3 collective-permute-done.22.refs_13_
  252.6 0.2 collective-permute-done.23.refs_14_
  252.8 0.3 collective-permute-done.24.refs_15_
  253.1 0.9 copy-done
  254.0 2.0 proj.1
  256.0 4.5 %all-to-all-start.4 = ((bf16[16,128,256]{2,1,0:T(8,128)(2,1)}), bf16[16,128,256]{2,1,0:T(8,128)(2,1)}, u32[]{:S(2)}, u32[]{:S(2)}) async-start(bf16[16,128,256]{2,1,0:T(8,128)(2,1)} %proj.1), calls=%async_computation.5 | async-start | bytes 2097152 | tf_op jit(solution)/shard_map/all_to_all | solution.py:435
  260.5 2.0 mixer.1
  262.5 1.3 collective-permute-start.25
  263.8 12.1 %collective-permute-done.25 = f32[128,2]{1,0:T(8,128)S(1)} collective-permute-done((f32[128,2]{1,0:T(8,128)S(1)}, f32[128,2]{1,0:T(8,128)S(1)}, u32[]{:S(2)}, u32[]{:S(2)}) %collective-permute-start.25) | collective-permute-done | bytes 1056 | tf_op jit(solution)/shard_map/ppermute | solution.py:237
  275.9 0.8 multiply_convert_fusion
  276.7 0.6 multiply_convert_fusion.1
  277.4 1.6 all-to-all-done.4
  279.0 2.0 convert_reduce_fusion
  (61 shorter events, 0.6 us)
Async XLA Ops:
  7.2 108.6 %all-gather.2.cloned.1.call-start = ((), (), s32[]{:S(2)}) async-start(), calls=%async_computation.6 | async-start | bytes 10027008 | tf_op jit(solution)/shard_map/all_gather | solution.py:287
  7.2 0.9 copy-start.3
  8.1 0.9 copy-start.7
  9.0 0.7 copy-start.8
  9.7 0.7 copy-start.9
  10.4 19.9 %copy-start.4 = (bf16[256,256]{1,0:T(8,128)(2,1)S(1)}, bf16[256,256]{1,0:T(8,128)(2,1)}, u32[]{:S(2)}) copy-start(bf16[256,256]{1,0:T(8,128)(2,1)} %cot_ref.3) | copy-start | bytes 393220
  30.3 6.5 %collective-permute-start = (bf16[256,256]{1,0:T(8,128)(2,1)S(1)}, bf16[256,256]{1,0:T(8,128)(2,1)S(1)}, u32[]{:S(2)}, u32[]{:S(2)}) collective-permute-start(bf16[256,256]{1,0:T(8,128)(2,1)S(1)} %copy-done.4), channel_id=1, source_target_pairs={{0,2},{2,4},{4,6},{6,8},{8,10},{10,12},{12,14},{14,0},{1,3},{3,5},... | collective-permute-start | bytes 393224 | tf_op jit(solution)/shard_map/ppermute | solution.py:230
  32.3 5.0 %collective-permute-start.1 = (bf16[256,256]{1,0:T(8,128)(2,1)S(1)}, bf16[256,256]{1,0:T(8,128)(2,1)S(1)}, u32[]{:S(2)}, u32[]{:S(2)}) collective-permute-start(bf16[256,256]{1,0:T(8,128)(2,1)S(1)} %copy-done.4), channel_id=1, source_target_pairs={{0,14},{2,0},{4,2},{6,4},{8,6},{10,8},{12,10},{14,12},{1,15},{3,1}... | collective-permute-start | bytes 393224 | tf_op jit(solution)/shard_map/ppermute | solution.py:230
  32.4 9.4 %collective-permute-start.2 = (bf16[256,256]{1,0:T(8,128)(2,1)S(1)}, bf16[256,256]{1,0:T(8,128)(2,1)S(1)}, u32[]{:S(2)}, u32[]{:S(2)}) collective-permute-start(bf16[256,256]{1,0:T(8,128)(2,1)S(1)} %copy-done.4), channel_id=1, source_target_pairs={{0,4},{2,6},{4,8},{6,10},{8,12},{10,14},{12,0},{14,2},{1,5},{3,7},... | collective-permute-start | bytes 393224 | tf_op jit(solution)/shard_map/ppermute | solution.py:230
  43.7 40.1 %all-to-all-start.1 = ((bf16[16,56,1024]{2,1,0:T(8,128)(2,1)}), bf16[16,56,1024]{2,1,0:T(8,128)(2,1)S(1)}, u32[]{:S(2)}, u32[]{:S(2)}) async-start(bf16[16,56,1024]{2,1,0:T(8,128)(2,1)} %bitcast.4), calls=%async_computation.1 | async-start | bytes 3670016 | tf_op jit(solution)/shard_map/all_to_all | solution.py:301
  47.4 15.8 %collective-permute-start.4 = (bf16[256,256]{1,0:T(8,128)(2,1)S(1)}, bf16[256,256]{1,0:T(8,128)(2,1)S(1)}, u32[]{:S(2)}, u32[]{:S(2)}) collective-permute-start(bf16[256,256]{1,0:T(8,128)(2,1)S(1)} %copy-done.4), channel_id=1, source_target_pairs={{0,12},{2,14},{4,0},{6,2},{8,4},{10,6},{12,8},{14,10},{1,13},{3,15... | collective-permute-start | bytes 393224 | tf_op jit(solution)/shard_map/ppermute | solution.py:230
  52.1 17.0 %collective-permute-start.5 = (bf16[256,256]{1,0:T(8,128)(2,1)S(1)}, bf16[256,256]{1,0:T(8,128)(2,1)S(1)}, u32[]{:S(2)}, u32[]{:S(2)}) collective-permute-start(bf16[256,256]{1,0:T(8,128)(2,1)S(1)} %copy-done.4), channel_id=1, source_target_pairs={{0,6},{2,8},{4,10},{6,12},{8,14},{10,0},{12,2},{14,4},{1,7},{3,9},... | collective-permute-start | bytes 393224 | tf_op jit(solution)/shard_map/ppermute | solution.py:230
  55.5 19.6 %collective-permute-start.6 = (bf16[256,256]{1,0:T(8,128)(2,1)S(1)}, bf16[256,256]{1,0:T(8,128)(2,1)S(1)}, u32[]{:S(2)}, u32[]{:S(2)}) collective-permute-start(bf16[256,256]{1,0:T(8,128)(2,1)S(1)} %copy-done.4), channel_id=1, source_target_pairs={{0,10},{2,12},{4,14},{6,0},{8,2},{10,4},{12,6},{14,8},{1,11},{3,13... | collective-permute-start | bytes 393224 | tf_op jit(solution)/shard_map/ppermute | solution.py:230
  57.2 24.8 %collective-permute-start.7 = (bf16[256,256]{1,0:T(8,128)(2,1)S(1)}, bf16[256,256]{1,0:T(8,128)(2,1)S(1)}, u32[]{:S(2)}, u32[]{:S(2)}) collective-permute-start(bf16[256,256]{1,0:T(8,128)(2,1)S(1)} %copy-done.4), channel_id=1, source_target_pairs={{0,8},{2,10},{4,12},{6,14},{8,0},{10,2},{12,4},{14,6},{1,9},{3,11}... | collective-permute-start | bytes 393224 | tf_op jit(solution)/shard_map/ppermute | solution.py:230
  83.8 7.2 %copy-start.10 = (bf16[16,56,1024]{2,1,0:T(8,128)(2,1)}, bf16[16,56,1024]{2,1,0:T(8,128)(2,1)S(1)}, u32[]{:S(2)}) copy-start(bf16[16,56,1024]{2,1,0:T(8,128)(2,1)S(1)} %all-to-all-done.1) | copy-start | bytes 5505028
  83.8 31.4 %copy-start.14 = (s32[8]{0:T(128)S(1)}, s32[8]{0:T(128)}, u32[]{:S(2)}) copy-start(s32[8]{0:T(128)} %constant.35) | copy-start | bytes 100
  83.8 31.4 %all-to-all-start.2 = ((bf16[16,56,1024]{2,1,0:T(8,128)(2,1)}), bf16[16,56,1024]{2,1,0:T(8,128)(2,1)}, u32[]{:S(2)}, u32[]{:S(2)}) async-start(bf16[16,56,1024]{2,1,0:T(8,128)(2,1)} %bitcast.9), calls=%async_computation.2 | async-start | bytes 3670016 | tf_op jit(solution)/shard_map/all_to_all | solution.py:301
  91.0 109.0 %reduce-scatter.2.cloned.1.call-start = ((), (), s32[]{:S(2)}) async-start(), calls=%async_computation.7 | async-start | bytes 8912896 | tf_op jit(solution)/shard_map/reduce_scatter | solution.py:363
  91.0 24.7 %collective-permute-start.3 = (bf16[896,1024]{1,0:T(8,128)(2,1)S(1)}, bf16[896,1024]{1,0:T(8,128)(2,1)}, u32[]{:S(2)}, u32[]{:S(2)}) collective-permute-start(bf16[896,1024]{1,0:T(8,128)(2,1)S(1)} %bitcast.33), channel_id=1, source_target_pairs={{0,1},{1,0},{2,3},{3,2},{4,5},{5,4},{6,7},{7,6},{8,9},{9,8},{10,11... | collective-permute-start | bytes 5505032 | tf_op jit(solution)/shard_map/ppermute | solution.py:304
  115.2 12.9 %collective-permute-start.8 = (bf16[896,1024]{1,0:T(8,128)(2,1)}, bf16[896,1024]{1,0:T(8,128)(2,1)}, u32[]{:S(2)}, u32[]{:S(2)}) collective-permute-start(bf16[896,1024]{1,0:T(8,128)(2,1)} %bitcast.10.mine_ref.mh_ref), channel_id=1, source_target_pairs={{0,1},{1,0},{2,3},{3,2},{4,5},{5,4},{6,7},{7,6},{8,9},{9,8},{10,11... | collective-permute-start | bytes 5505032 | tf_op jit(solution)/shard_map/ppermute | solution.py:304
  138.3 68.5 %copy-start.12 = (bf16[128,256]{1,0:T(8,128)(2,1)S(1)}, bf16[128,256]{1,0:T(8,128)(2,1)}, u32[]{:S(2)}) copy-start(bf16[128,256]{1,0:T(8,128)(2,1)} %param.15) | copy-start | bytes 196612
  138.3 68.6 %copy-start.11 = (bf16[128,256]{1,0:T(8,128)(2,1)S(1)}, bf16[128,256]{1,0:T(8,128)(2,1)}, u32[]{:S(2)}) copy-start(bf16[128,256]{1,0:T(8,128)(2,1)} %param.14) | copy-start | bytes 196612
  158.9 73.4 %copy-start.13 = (f32[3,128]{1,0:T(4,128)S(1)}, f32[3,128]{1,0:T(4,128)}, u32[]{:S(2)}) copy-start(f32[3,128]{1,0:T(4,128)} %param.16) | copy-start | bytes 4612
  158.9 92.9 %copy-start.5 = (bf16[128,256]{1,0:T(8,128)(2,1)S(1)}, bf16[128,256]{1,0:T(8,128)(2,1)}, u32[]{:S(2)}) copy-start(bf16[128,256]{1,0:T(8,128)(2,1)} %outer_ref.1) | copy-start | bytes 196612
  200.0 53.1 %copy-start.6 = (s32[16]{0:T(128)S(1)}, s32[16]{0:T(128)}, u32[]{:S(2)}) copy-start(s32[16]{0:T(128)} %pad_add_fusion.slab_ref) | copy-start | bytes 196
  200.0 18.3 %all-to-all-start.3 = ((bf16[16,64,256]{2,1,0:T(8,128)(2,1)}), bf16[16,64,256]{2,1,0:T(8,128)(2,1)S(1)}, u32[]{:S(2)}, u32[]{:S(2)}) async-start(bf16[16,64,256]{2,1,0:T(8,128)(2,1)} %bitcast.44), calls=%async_computation.4 | async-start | bytes 1048576 | tf_op jit(solution)/shard_map/all_to_all | solution.py:395
  207.3 18.8 %collective-permute-start.9 = (bf16[2,128,2]{2,1,0:T(8,128)(2,1)S(1)}, bf16[2,128,2]{2,1,0:T(8,128)(2,1)S(1)}, u32[]{:S(2)}, u32[]{:S(2)}) collective-permute-start(bf16[2,128,2]{2,1,0:T(8,128)(2,1)S(1)} %copy.23), channel_id=1, source_target_pairs={{0,16},{16,32},{32,48},{48,64},{64,80},{80,96},{96,112},{112,128},... | collective-permute-start | bytes 3080 | tf_op jit(solution)/shard_map/ppermute | solution.py:237
  219.3 13.0 %collective-permute-start.10 = (bf16[256,256]{1,0:T(8,128)(2,1)}, bf16[256,256]{1,0:T(8,128)(2,1)S(1)}, u32[]{:S(2)}, u32[]{:S(2)}) collective-permute-start(bf16[256,256]{1,0:T(8,128)(2,1)} %combine.1.refs_0_), channel_id=1, source_target_pairs={{0,2},{2,4},{4,6},{6,8},{8,10},{10,12},{12,14},{14,0},{1,3},{3,5},... | collective-permute-start | bytes 393224 | tf_op jit(solution)/shard_map/ppermute | solution.py:230
  219.3 13.1 %collective-permute-start.11 = (bf16[256,256]{1,0:T(8,128)(2,1)}, bf16[256,256]{1,0:T(8,128)(2,1)S(1)}, u32[]{:S(2)}, u32[]{:S(2)}) collective-permute-start(bf16[256,256]{1,0:T(8,128)(2,1)} %combine.1.refs_0_), channel_id=1, source_target_pairs={{0,14},{2,0},{4,2},{6,4},{8,6},{10,8},{12,10},{14,12},{1,15},{3,1}... | collective-permute-start | bytes 393224 | tf_op jit(solution)/shard_map/ppermute | solution.py:230
  222.0 13.7 %collective-permute-start.12 = (bf16[256,256]{1,0:T(8,128)(2,1)}, bf16[256,256]{1,0:T(8,128)(2,1)S(1)}, u32[]{:S(2)}, u32[]{:S(2)}) collective-permute-start(bf16[256,256]{1,0:T(8,128)(2,1)} %combine.1.refs_0_), channel_id=1, source_target_pairs={{0,4},{2,6},{4,8},{6,10},{8,12},{10,14},{12,0},{14,2},{1,5},{3,7},... | collective-permute-start | bytes 393224 | tf_op jit(solution)/shard_map/ppermute | solution.py:230
  225.5 10.2 %collective-permute-start.13 = (bf16[256,256]{1,0:T(8,128)(2,1)}, bf16[256,256]{1,0:T(8,128)(2,1)S(1)}, u32[]{:S(2)}, u32[]{:S(2)}) collective-permute-start(bf16[256,256]{1,0:T(8,128)(2,1)} %combine.1.refs_0_), channel_id=1, source_target_pairs={{0,12},{2,14},{4,0},{6,2},{8,4},{10,6},{12,8},{14,10},{1,13},{3,15... | collective-permute-start | bytes 393224 | tf_op jit(solution)/shard_map/ppermute | solution.py:230
  226.1 19.7 %collective-permute-start.14 = (bf16[256,256]{1,0:T(8,128)(2,1)}, bf16[256,256]{1,0:T(8,128)(2,1)S(1)}, u32[]{:S(2)}, u32[]{:S(2)}) collective-permute-start(bf16[256,256]{1,0:T(8,128)(2,1)} %combine.1.refs_0_), channel_id=1, source_target_pairs={{0,6},{2,8},{4,10},{6,12},{8,14},{10,0},{12,2},{14,4},{1,7},{3,9},... | collective-permute-start | bytes 393224 | tf_op jit(solution)/shard_map/ppermute | solution.py:230
  232.3 18.4 %collective-permute-start.15 = (bf16[256,256]{1,0:T(8,128)(2,1)}, bf16[256,256]{1,0:T(8,128)(2,1)S(1)}, u32[]{:S(2)}, u32[]{:S(2)}) collective-permute-start(bf16[256,256]{1,0:T(8,128)(2,1)} %combine.1.refs_0_), channel_id=1, source_target_pairs={{0,10},{2,12},{4,14},{6,0},{8,2},{10,4},{12,6},{14,8},{1,11},{3,13... | collective-permute-start | bytes 393224 | tf_op jit(solution)/shard_map/ppermute | solution.py:230
  232.4 18.3 %collective-permute-start.16 = (bf16[256,256]{1,0:T(8,128)(2,1)}, bf16[256,256]{1,0:T(8,128)(2,1)S(1)}, u32[]{:S(2)}, u32[]{:S(2)}) collective-permute-start(bf16[256,256]{1,0:T(8,128)(2,1)} %combine.1.refs_0_), channel_id=1, source_target_pairs={{0,8},{2,10},{4,12},{6,14},{8,0},{10,2},{12,4},{14,6},{1,9},{3,11}... | collective-permute-start | bytes 393224 | tf_op jit(solution)/shard_map/ppermute | solution.py:230
  235.6 15.6 %collective-permute-start.17 = (bf16[256,256]{1,0:T(8,128)(2,1)}, bf16[256,256]{1,0:T(8,128)(2,1)S(1)}, u32[]{:S(2)}, u32[]{:S(2)}) collective-permute-start(bf16[256,256]{1,0:T(8,128)(2,1)} %combine.1.refs_0_), channel_id=1, source_target_pairs={{0,1},{1,0},{2,3},{3,2},{4,5},{5,4},{6,7},{7,6},{8,9},{9,8},{10,11... | collective-permute-start | bytes 393224 | tf_op jit(solution)/shard_map/ppermute | solution.py:406
  235.6 15.7 %collective-permute-start.18 = (bf16[256,256]{1,0:T(8,128)(2,1)S(1)}, bf16[256,256]{1,0:T(8,128)(2,1)S(1)}, u32[]{:S(2)}, u32[]{:S(2)}) collective-permute-start(bf16[256,256]{1,0:T(8,128)(2,1)S(1)} %collective-permute-done.10.refs_1_), channel_id=1, source_target_pairs={{0,1},{1,0},{2,3},{3,2},{4,5},{5,4},{6,7},{7,6},{8,9},{9,8},{10,11... | collective-permute-start | bytes 393224 | tf_op jit(solution)/shard_map/ppermute | solution.py:406
  245.8 6.0 %collective-permute-start.19 = (bf16[256,256]{1,0:T(8,128)(2,1)S(1)}, bf16[256,256]{1,0:T(8,128)(2,1)S(1)}, u32[]{:S(2)}, u32[]{:S(2)}) collective-permute-start(bf16[256,256]{1,0:T(8,128)(2,1)S(1)} %collective-permute-done.11.refs_2_), channel_id=1, source_target_pairs={{0,1},{1,0},{2,3},{3,2},{4,5},{5,4},{6,7},{7,6},{8,9},{9,8},{10,11... | collective-permute-start | bytes 393224 | tf_op jit(solution)/shard_map/ppermute | solution.py:406
  250.7 1.3 collective-permute-start.20
  250.7 1.5 collective-permute-start.21
  251.2 1.3 collective-permute-start.22
  251.3 1.4 collective-permute-start.23
  251.8 1.3 collective-permute-start.24
  253.1 0.9 copy-start
  256.0 4.5 %copy-start.1 = (bf16[256,256]{1,0:T(8,128)(2,1)S(1)}, bf16[256,256]{1,0:T(8,128)(2,1)}, u32[]{:S(2)}) copy-start(bf16[256,256]{1,0:T(8,128)(2,1)} %combine.1.refs_0_) | copy-start | bytes 393220
  256.0 4.5 %copy-start.2 = (bf16[128,4096]{1,0:T(8,128)(2,1)S(1)}, bf16[128,4096]{1,0:T(8,128)(2,1)}, u32[]{:S(2)}) copy-start(bf16[128,4096]{1,0:T(8,128)(2,1)} %proj_ref.1) | copy-start | bytes 3145732
  256.0 23.0 %all-to-all-start.4 = ((bf16[16,128,256]{2,1,0:T(8,128)(2,1)}), bf16[16,128,256]{2,1,0:T(8,128)(2,1)}, u32[]{:S(2)}, u32[]{:S(2)}) async-start(bf16[16,128,256]{2,1,0:T(8,128)(2,1)} %proj.1), calls=%async_computation.5 | async-start | bytes 2097152 | tf_op jit(solution)/shard_map/all_to_all | solution.py:435
  262.5 13.4 %collective-permute-start.25 = (f32[128,2]{1,0:T(8,128)S(1)}, f32[128,2]{1,0:T(8,128)S(1)}, u32[]{:S(2)}, u32[]{:S(2)}) collective-permute-start(f32[128,2]{1,0:T(8,128)S(1)} %slice.52), channel_id=1, source_target_pairs={{16,0},{32,16},{48,32},{64,48},{80,64},{96,80},{112,96},{128,112},... | collective-permute-start | bytes 3080 | tf_op jit(solution)/shard_map/ppermute | solution.py:237
Sparse Core Ops, SparseCore 0:
  30.4 77.4 all-gather.1
  138.4 61.5 reduce-scatter.1

commit v3 on v1

--- a/solution.py
+++ b/solution.py
@@ -24,6 +24,10 @@
 
 def dot_tn(a, b):
     return lax.dot_general(a, b, (((0,), (0,)), ((), ())), preferred_element_type=F32)
+
+
+def grant(mib):
+    return pltpu.CompilerParams(vmem_limit_bytes=mib << 20)
 
 
 def cost(flops, nbytes):
@@ -51,52 +55,83 @@
     sent_ref[...] = dot_nn(pick_ref[...], state_ref[...]).astype(BF16)
 
 
-def spread_kernel(pick_ref, scale_ref, *refs):
-    pieces, (low_ref, high_ref) = refs[:-2], refs[-2:]
+def spread_kernel(late_ref, scale_ref, *refs):
+    pieces, out_ref = refs[:-1], refs[-1]
     width = pieces[0].shape[1]
-    half = len(pieces) // 2
     scale = scale_ref[:, 0:1]
     for j, piece in enumerate(pieces):
-        rows = (dot_nn(pick_ref[...], piece[...]) * scale).astype(BF16)
-        out = low_ref if j < half else high_ref
-        out[:, (j % half) * width : (j % half + 1) * width] = rows
-
-
-def expert_kernel(
-    slab_ref, state_ref, ml_ref, mh_ref, tl_ref, th_ref, wg_ref, wu_ref, wd_ref, part_ref, act_ref, wgu_ref
+        rows = (dot_nn(late_ref[...], piece[...]) * scale).astype(BF16)
+        out_ref[:, j * width : (j + 1) * width] = rows
+
+
+def down_columns(slab_ref, base, wd_ref, count, width):
+    pieces = [
+        wd_ref[:, pl.ds(pl.multiple_of(slab_ref[base + j] * width, width), width)]
+        for j in range(count)
+    ]
+    return jnp.concatenate(pieces, axis=1)
+
+
+def expert_first_kernel(
+    slab_ref, state_ref, mine_ref, their_ref, wg_ref, wu_ref, wd_ref, pre_ref
 ):
     slabs, width = state_ref.shape[0], state_ref.shape[2]
     hidden_n = wd_ref.shape[0]
+    step, steps = pl.program_id(0), pl.num_programs(0)
+    rows = jnp.concatenate([state_ref[s] for s in range(slabs)], axis=1)
+    both = dot_nt(rows, jnp.concatenate([wg_ref[...], wu_ref[...]], axis=0))
+
+    def down(base):
+        at = pl.multiple_of(slab_ref[base + step] * width, width)
+        return wd_ref[:, pl.ds(at, width)]
+
+    cots = jnp.concatenate([mine_ref[...], their_ref[...]], axis=1)
+    back = dot_nt(cots, jnp.concatenate([down(0), down(2 * steps)], axis=1))
+
+    @pl.when(step == 0)
+    def _():
+        pre_ref[:, : 2 * hidden_n] = both
+        pre_ref[:, 2 * hidden_n :] = back
+
+    @pl.when(step > 0)
+    def _():
+        pre_ref[:, : 2 * hidden_n] += both
+        pre_ref[:, 2 * hidden_n :] += back
+
+
+def expert_second_kernel(
+    slab_ref, pre_ref, mine_ref, their_ref, wg_ref, wu_ref, wd_ref, part_ref, act_ref, w_ref
+):
+    slabs, width = part_ref.shape[0], part_ref.shape[2]
+    hidden_n = wd_ref.shape[0]
 
     @pl.when(pl.program_id(0) == 0)
     def _():
-        wgu_ref[:hidden_n] = wg_ref[...]
-        wgu_ref[hidden_n:] = wu_ref[...]
-
-    rows = jnp.concatenate([state_ref[s] for s in range(slabs)], axis=1)
-    pre = dot_nt(rows, wgu_ref[...])
-    gate_pre, up_pre = pre[:, :hidden_n], pre[:, hidden_n:]
-    back_hidden = jnp.zeros(gate_pre.shape, F32)
-    per = ml_ref.shape[1] // width
-    for q, ref in enumerate((ml_ref, mh_ref, tl_ref, th_ref)):
-        pieces = [
-            wd_ref[:, pl.ds(pl.multiple_of(slab_ref[q * per + j] * width, width), width)]
-            for j in range(per)
-        ]
-        back_hidden = back_hidden + dot_nt(ref[...], jnp.concatenate(pieces, axis=1))
+        w_ref[:hidden_n] = wg_ref[...]
+        w_ref[hidden_n:] = wu_ref[...]
+
+    per = mine_ref.shape[1] // width
+    gate_pre, up_pre = pre_ref[:, :hidden_n], pre_ref[:, hidden_n : 2 * hidden_n]
+    back_hidden = pre_ref[:, 2 * hidden_n :]
+    back_hidden = back_hidden + dot_nt(mine_ref[...], down_columns(slab_ref, per, wd_ref, per, width))
+    back_hidden = back_hidden + dot_nt(
+        their_ref[...], down_columns(slab_ref, 3 * per, wd_ref, per, width)
+    )
     sig_gate = jax.nn.sigmoid(gate_pre)
     silu_gate = gate_pre * sig_gate
     hidden = (silu_gate * up_pre).astype(BF16)
     back_gate = (back_hidden * up_pre * sig_gate * (1.0 + gate_pre * (1.0 - sig_gate))).astype(BF16)
     back_up = (back_hidden * silu_gate).astype(BF16)
     back = jnp.concatenate([back_gate, back_up], axis=1)
+    for s in range(slabs):
+        part_ref[s] = dot_nn(back, w_ref[:, s * width : (s + 1) * width]).astype(BF16)
     act_ref[:, : 2 * hidden_n] = back
     act_ref[:, 2 * hidden_n :] = hidden
-    for s in range(slabs):
-        part_ref[s] = dot_nn(back, wgu_ref[:, s * width : (s + 1) * width]).astype(BF16)
-
-
-def weight_grad_kernel(slab_ref, act_ref, state_ref, ml_ref, mh_ref, tl_ref, th_ref, gg_ref, gu_ref, gd_ref):
+
+
+def weight_grad_kernel(
+    slab_ref, act_ref, state_ref, ml_ref, mh_ref, tl_ref, th_ref, gg_ref, gu_ref, gd_ref
+):
     hidden_n = gg_ref.shape[0]
     step, per = pl.program_id(0), pl.num_programs(0) // 4
     both = dot_tn(act_ref[:, : 2 * hidden_n], state_ref[0])
@@ -181,7 +216,7 @@
 
     cot_pieces = gathered(cotangent, "z")
 
-    sent_state, pick, scale = pl.pallas_call(
+    sent_rows, pick, scale = pl.pallas_call(
         functools.partial(route_kernel, experts, cap),
         out_shape=(
             shape((slots, width), BF16),
@@ -191,19 +226,21 @@
         cost_estimate=cost(2 * slots * tok_count * width, 4 * slots * width),
         name="route",
     )(route_ids.T, route_weights.T, mixed_state)
-    recv_state = lax.all_to_all(
-        sent_state.reshape(experts, cap, width), "sp", split_axis=0, concat_axis=0, tiled=True
-    )
-    state_all = lax.all_gather(recv_state.reshape(slots, width), TP, axis=0, tiled=False)
+    recv_rows = lax.all_to_all(
+        sent_rows.reshape(experts, cap, width), "sp", split_axis=0, concat_axis=0, tiled=True
+    )
+    state_all = lax.all_gather(recv_rows.reshape(slots, width), TP, axis=0, tiled=False)
 
     half = z_size // 2 * width
-    cot_low, cot_high = pl.pallas_call(
-        spread_kernel,
-        out_shape=(shape((slots, half), BF16),) * 2,
-        cost_estimate=cost(4 * slots * tok_count * half, 8 * slots * half),
-        name="spread",
-    )(pick, scale, *cot_pieces)
     swap = [(0, 1), (1, 0)]
+
+    def spread(pieces):
+        return pl.pallas_call(
+            spread_kernel,
+            out_shape=shape((slots, half), BF16),
+            cost_estimate=cost(2 * slots * tok_count * half, 4 * slots * half),
+            compiler_params=grant(16),
+        )(pick, scale, *pieces)
 
     def exchanged(part):
         got = lax.all_to_all(
@@ -211,33 +248,51 @@
         ).reshape(slots, half)
         return got, lax.ppermute(got, "c", swap)
 
-    my_low, their_low = exchanged(cot_low)
-    my_high, their_high = exchanged(cot_high)
+    my_low, their_low = exchanged(spread(cot_pieces[: z_size // 2]))
+    my_high, their_high = exchanged(spread(cot_pieces[z_size // 2 :]))
     cots = (my_low, my_high, their_low, their_high)
 
-    block = 256
+    steps = 4
     whole = lambda *dims: pl.BlockSpec(dims, lambda *_: (0,) * len(dims))
-    cot_rows = pl.BlockSpec((block, half), lambda r, core: (r, 0))
-    partial_value, acts = pl.pallas_call(
-        expert_kernel,
+    by_rows = lambda *dims: pl.BlockSpec(dims, lambda r, slab: (r, 0))
+    weights = (w_gate[0], w_up[0], w_down[0])
+    pre = pl.pallas_call(
+        expert_first_kernel,
         grid_spec=pltpu.PrefetchScalarGridSpec(
             num_scalar_prefetch=1,
-            grid=(slots // block,),
+            grid=(steps,),
             in_specs=[
-                pl.BlockSpec((slabs, block, width), lambda r, core: (0, r, 0)),
-                *[cot_rows] * 4,
+                pl.BlockSpec((slabs // steps, slots, width), lambda k, slab: (k, 0, 0)),
+                *[pl.BlockSpec((slots, width), lambda k, slab: (0, k))] * 2,
+                *[pl.BlockSpec((hidden_n, features // steps), lambda k, slab: (0, k))] * 2,
+                whole(hidden_n, features),
+            ],
+            out_specs=whole(slots, 3 * hidden_n),
+        ),
+        out_shape=shape((slots, 3 * hidden_n), F32),
+        cost_estimate=cost(5 * slots * hidden_n * features, 3 * slots * features),
+        name="expert_first",
+    )(slab_of, state_all, my_low, their_low, *weights)
+    partial_value, acts = pl.pallas_call(
+        expert_second_kernel,
+        grid_spec=pltpu.PrefetchScalarGridSpec(
+            num_scalar_prefetch=1,
+            grid=(steps,),
+            in_specs=[
+                by_rows(slots // steps, 3 * hidden_n),
+                *[by_rows(slots // steps, half)] * 2,
                 *[whole(hidden_n, features)] * 3,
             ],
             out_specs=[
-                pl.BlockSpec((slabs, block, width), lambda r, core: (0, r, 0)),
-                pl.BlockSpec((block, 3 * hidden_n), lambda r, core: (r, 0)),
+                pl.BlockSpec((slabs, slots // steps, width), lambda r, slab: (0, r, 0)),
+                by_rows(slots // steps, 3 * hidden_n),
             ],
             scratch_shapes=[pltpu.VMEM((2 * hidden_n, features), BF16)],
         ),
         out_shape=(shape((slabs, slots, width), BF16), shape((slots, 3 * hidden_n), BF16)),
-        cost_estimate=cost(10 * slots * hidden_n * features, 6 * slots * features),
-        name="expert",
-    )(slab_of, state_all, *cots, w_gate[0], w_up[0], w_down[0])
+        cost_estimate=cost(5 * slots * hidden_n * features, 4 * slots * features),
+        name="expert_second",
+    )(slab_of, pre, my_high, their_high, *weights)
 
     row_back = lax.psum_scatter(partial_value, TP, scatter_dimension=0, tiled=False)
 
@@ -245,7 +300,7 @@
 
     def cot_piece(q):
         return pl.BlockSpec(
-            (slots, width), lambda s, core: (0, jnp.clip(s - q * quarter, 0, quarter - 1))
+            (slots, width), lambda s, slab: (0, jnp.clip(s - q * quarter, 0, quarter - 1))
         )
 
     grad_out = pl.BlockSpec((hidden_n, width), lambda s, slab: (0, slab[s]))
@@ -277,6 +332,7 @@
         out_shape=shape((tok_count, width), BF16),
         cost_estimate=cost(2 * slots * tok_count * width, 4 * slots * width),
         name="combine",
+        compiler_params=grant(16),
     )(pick, arrived, cotangent)
     near = gathered(grad_mixed, "z")
     full_back = near + [lax.ppermute(piece, "c", swap) for piece in near]
@@ -306,6 +362,7 @@
         out_shape=shape((slabs, channels, width), BF16),
         cost_estimate=cost(2 * channels * tok_count * features, 4 * tok_count * features),
         name="proj",
+        compiler_params=grant(14),
     )(slab_of, mixer_act, *full_back)
     landed = lax.all_to_all(proj_term, "sp", split_axis=0, concat_axis=0, tiled=True)
     grad_proj = jnp.sum(landed.astype(F32), axis=0)
@@ -315,6 +372,7 @@
         out_shape=(shape((channels, tok_count), BF16), shape((channels, tok_count), F32)),
         cost_estimate=cost(2 * channels * tok_count * features, 4 * tok_count * features),
         name="mixer",
+        compiler_params=grant(14),
     )(slab_of, out_proj, conv_out, conv_outer, *full_back)
     tail_back = from_behind(back_conv[:, :rim_width], "sp", -1)
     back_ext = jnp.concatenate([back_conv, tail_back], axis=1)

time: 303 us -> 292 us (0.964)
  the two profiles are of different devices: /device:TPU:24 before, /device:TPU:32 now
where the time goes in v3:
time: 292 us; the launch traced here: 291 us
  waiting for transfers between devices  134 us (46%)
  starting transfers between devices  63.6 us (22%)
  Pallas kernels  52.9 us (18%)
  blocking collectives  18.7 us (6%)
  between operations  14.3 us (5%)
  other arithmetic  4.43 us (2%)
  local copies, waits for them, and re-layouts  3.55 us (1%)
    ppermute x14, waiting for transfers between devices, gathered(): lax.ppermute(value, axis, [(i, (i + k) % size) for i in range(size)])  42.6 us
    reduce_scatter x1, waiting for transfers between devices, shards(): lax.psum_scatter(partial_value, TP, scatter_dimension=0, tiled=False)  42.4 us
    ppermute x14, starting transfers between devices, gathered(): lax.ppermute(value, axis, [(i, (i + k) % size) for i in range(size)])  34.1 us
    all_to_all x2, waiting for transfers between devices, exchanged(): lax.all_to_all(part.reshape(experts, cap, half), 'sp', split_axis=0, conc...  26.8 us
    pallas_call x1, Pallas kernels, shards(): pl.pallas_call(weight_grad_kernel, grid_spec=pltpu.PrefetchScalarGridSpec...  19.5 us
    all_to_all x1, blocking collectives, shards(): lax.all_to_all(sent_rows.reshape(experts, cap, width), 'sp', split_axis=0...  18.7 us
    ppermute x2, waiting for transfers between devices, from_behind(): lax.ppermute(value, axis, [(source, source + steps) for source in range(f...  12.1 us
    pallas_call x1, Pallas kernels, shards(): pl.pallas_call(expert_second_kernel, grid_spec=pltpu.PrefetchScalarGridSp...  11.7 us
  transfers between devices with their start and end apart: 32, of which 17 were waited for; matrix products, arithmetic and copies ran while one was open for 1% of the time, Pallas kernels for 13%

profile of v3, /device:TPU:32, one launch (start us, length us, event | category | flops | bytes accessed | tf_op | source)
XLA Modules:
  0.0 291.1 jit_solution(1584668412543627210)
XLA Ops:
  7.2 2.5 route.1
  9.7 18.7 %all_to_all.25 = bf16[16,64,256]{2,1,0:T(8,128)(2,1)} all-to-all(bf16[16,64,256]{2,1,0:T(8,128)(2,1)} %bitcast.41), channel_id=1, replica_groups=mesh['sp'=16,'z'=8,'c'=2] {'sp'}, dimensions={0} | all-to-all | bytes 1048576 | tf_op jit(solution)/shard_map/all_to_all | solution.py:229
  28.4 2.0 collective-permute-start
  30.4 0.1 collective-permute-start.1
  30.5 4.4 %collective-permute-start.2 = (bf16[256,256]{1,0:T(8,128)(2,1)}, bf16[256,256]{1,0:T(8,128)(2,1)S(1)}, u32[]{:S(2)}, u32[]{:S(2)}) collective-permute-start(bf16[256,256]{1,0:T(8,128)(2,1)} %cot_ref.1), channel_id=1, source_target_pairs={{0,4},{2,6},{4,8},{6,10},{8,12},{10,14},{12,0},{14,2},{1,5},{3,7},... | collective-permute-start | bytes 393224 | tf_op jit(solution)/shard_map/ppermute | solution.py:180
  34.9 0.7 collective-permute-done.1.refs_2_
  35.6 4.4 %collective-permute-done.2.refs_3_ = bf16[256,256]{1,0:T(8,128)(2,1)S(1)} collective-permute-done((bf16[256,256]{1,0:T(8,128)(2,1)}, bf16[256,256]{1,0:T(8,128)(2,1)S(1)}, u32[]{:S(2)}, u32[]{:S(2)}) %collective-permute-start.2) | collective-permute-done | bytes 131104 | tf_op jit(solution)/shard_map/ppermute | solution.py:180
  40.0 1.0 copy-done
  41.1 1.0 copy-done.2
  42.1 2.0 shard_map.188
  44.1 4.4 %all-to-all-start.1 = ((bf16[16,64,1024]{2,1,0:T(8,128)(2,1)}), bf16[16,64,1024]{2,1,0:T(8,128)(2,1)S(1)}, u32[]{:S(2)}, u32[]{:S(2)}) async-start(bf16[16,64,1024]{2,1,0:T(8,128)(2,1)} %bitcast.4), calls=%async_computation.1 | async-start | bytes 4194304 | tf_op jit(solution)/shard_map/all_to_all | solution.py:246
  48.5 4.6 %collective-permute-start.4 = (bf16[256,256]{1,0:T(8,128)(2,1)S(1)}, bf16[256,256]{1,0:T(8,128)(2,1)S(1)}, u32[]{:S(2)}, u32[]{:S(2)}) collective-permute-start(bf16[256,256]{1,0:T(8,128)(2,1)S(1)} %copy-done.7), channel_id=1, source_target_pairs={{0,12},{2,14},{4,0},{6,2},{8,4},{10,6},{12,8},{14,10},{1,13},{3,15... | collective-permute-start | bytes 393224 | tf_op jit(solution)/shard_map/ppermute | solution.py:180
  53.1 3.4 %collective-permute-start.5 = (bf16[256,256]{1,0:T(8,128)(2,1)S(1)}, bf16[256,256]{1,0:T(8,128)(2,1)S(1)}, u32[]{:S(2)}, u32[]{:S(2)}) collective-permute-start(bf16[256,256]{1,0:T(8,128)(2,1)S(1)} %copy-done.7), channel_id=1, source_target_pairs={{0,6},{2,8},{4,10},{6,12},{8,14},{10,0},{12,2},{14,4},{1,7},{3,9},... | collective-permute-start | bytes 393224 | tf_op jit(solution)/shard_map/ppermute | solution.py:180
  56.5 1.7 collective-permute-start.6
  58.1 1.7 collective-permute-start.7
  59.9 5.0 %collective-permute-done.4.refs_0_ = bf16[256,256]{1,0:T(8,128)(2,1)S(1)} collective-permute-done((bf16[256,256]{1,0:T(8,128)(2,1)S(1)}, bf16[256,256]{1,0:T(8,128)(2,1)S(1)}, u32[]{:S(2)}, u32[]{:S(2)}) %collective-permute-start.4) | collective-permute-done | bytes 131104 | tf_op jit(solution)/shard_map/ppermute | solution.py:180
  64.8 5.0 %collective-permute-done.5.refs_1_ = bf16[256,256]{1,0:T(8,128)(2,1)S(1)} collective-permute-done((bf16[256,256]{1,0:T(8,128)(2,1)S(1)}, bf16[256,256]{1,0:T(8,128)(2,1)S(1)}, u32[]{:S(2)}, u32[]{:S(2)}) %collective-permute-start.5) | collective-permute-done | bytes 131104 | tf_op jit(solution)/shard_map/ppermute | solution.py:180
  69.8 6.5 %collective-permute-done.6.refs_2_ = bf16[256,256]{1,0:T(8,128)(2,1)S(1)} collective-permute-done((bf16[256,256]{1,0:T(8,128)(2,1)S(1)}, bf16[256,256]{1,0:T(8,128)(2,1)S(1)}, u32[]{:S(2)}, u32[]{:S(2)}) %collective-permute-start.6) | collective-permute-done | bytes 131104 | tf_op jit(solution)/shard_map/ppermute | solution.py:180
  76.3 6.7 %collective-permute-done.7.refs_3_ = bf16[256,256]{1,0:T(8,128)(2,1)S(1)} collective-permute-done((bf16[256,256]{1,0:T(8,128)(2,1)S(1)}, bf16[256,256]{1,0:T(8,128)(2,1)S(1)}, u32[]{:S(2)}, u32[]{:S(2)}) %collective-permute-start.7) | collective-permute-done | bytes 131104 | tf_op jit(solution)/shard_map/ppermute | solution.py:180
  82.9 2.0 shard_map.189
  85.0 7.1 %all-to-all-start.2 = ((bf16[16,64,1024]{2,1,0:T(8,128)(2,1)}), bf16[16,64,1024]{2,1,0:T(8,128)(2,1)}, u32[]{:S(2)}, u32[]{:S(2)}) async-start(bf16[16,64,1024]{2,1,0:T(8,128)(2,1)} %bitcast.9), calls=%async_computation.2 | async-start | bytes 4194304 | tf_op jit(solution)/shard_map/all_to_all | solution.py:246
  92.2 0.1 collective-permute-start.3
  92.3 26.8 %all-to-all-done.2 = bf16[16,64,1024]{2,1,0:T(8,128)(2,1)} async-done(((bf16[16,64,1024]{2,1,0:T(8,128)(2,1)}), bf16[16,64,1024]{2,1,0:T(8,128)(2,1)}, u32[]{:S(2)}, u32[]{:S(2)}) %all-to-all-start.2) | async-done | bytes 2097184 | tf_op jit(solution)/shard_map/all_to_all | solution.py:246
  119.1 0.6 pad_add_fusion.slab_ref
  119.7 10.1 %expert_first.1.pre_ref = f32[1024,384]{1,0:T(8,128)} custom-call(s32[16]{0:T(128)} %pad_add_fusion.slab_ref, bf16[16,1024,256]{2,1,0:T(8,128)(2,1)} %all-gather.2.cloned.1.call-done.state_ref, bf16[1024,1024]{1,0:T(8,128)(2,1)} %bitcast.31, bf16[1024,1024]{1,0:T(8,128)(2,1)} %collective-permute-done.3.their_ref.tl_ref, bf16[128,4096]{1,0:T(8,128)(2,1)} %bitcast.34, ...), custom_call_target="tpu_custom_call" | custom-call | flops 2684354560 | bytes 12582912 | tf_op jit(solution)/shard_map/expert_first/pallas_call | solution.py:259
  129.8 11.7 %expert_second.1 = (bf16[16,1024,256]{2,1,0:T(8,128)(2,1)}, bf16[1024,384]{1,0:T(8,128)(2,1)}) custom-call(s32[16]{0:T(128)} %pad_add_fusion.slab_ref, f32[1024,384]{1,0:T(8,128)} %expert_first.1.pre_ref, bf16[1024,1024]{1,0:T(8,128)(2,1)} %bitcast.10.mine_ref.mh_ref, bf16[1024,1024]{1,0:T(8,128)(2,1)} %collective-permute-done.8.their_ref.th_ref, ...), custom_call_target="tpu_custom_call" | custom-call | flops 2684354560 | bytes 16777216 | tf_op jit(solution)/shard_map/expert_second/pallas_call | solution.py:276
  141.6 19.5 %weight_grads.1 = (f32[128,4096]{1,0:T(8,128)}, f32[128,4096]{1,0:T(8,128)}, f32[128,4096]{1,0:T(8,128)}) custom-call(s32[16]{0:T(128)} %pad_add_fusion.slab_ref, bf16[1024,384]{1,0:T(8,128)(2,1)} %get-tuple-element.26.act_ref, bf16[16,1024,256]{2,1,0:T(8,128)(2,1)} %all-gather.2.cloned.1.call-done.state_ref, bf16[1024,1024]{1,0:T(8,128)(2,1)} %bitcast.32, ...), custom_call_target="tpu_custom_call" | custom-call | flops 3221225472 | bytes 25165824 | tf_op jit(solution)/shard_map/weight_grads/pallas_call | solution.py:307
  161.2 42.4 %reduce-scatter.2.cloned.1.call-done = bf16[1,1024,256]{2,1,0:T(8,128)(2,1)} async-done(((bf16[16,1024,256]{2,1,0:T(8,128)(2,1)}), bf16[1,1024,256]{2,1,0:T(8,128)(2,1)}) %reduce-scatter.2.cloned.1.call-update) | async-done | bytes 524304 | tf_op jit(solution)/shard_map/reduce_scatter | solution.py:297
  203.6 6.7 %all-to-all-start.3 = ((bf16[16,64,256]{2,1,0:T(8,128)(2,1)}), bf16[16,64,256]{2,1,0:T(8,128)(2,1)S(1)}, u32[]{:S(2)}, u32[]{:S(2)}) async-start(bf16[16,64,256]{2,1,0:T(8,128)(2,1)} %bitcast.40), calls=%async_computation.4 | async-start | bytes 1048576 | tf_op jit(solution)/shard_map/all_to_all | solution.py:327
  210.3 0.1 slice.44
  210.5 0.1 slice.43
  210.7 0.2 copy.23
  210.8 3.8 %collective-permute-start.9 = (bf16[2,128,2]{2,1,0:T(8,128)(2,1)S(1)}, bf16[2,128,2]{2,1,0:T(8,128)(2,1)S(1)}, u32[]{:S(2)}, u32[]{:S(2)}) collective-permute-start(bf16[2,128,2]{2,1,0:T(8,128)(2,1)S(1)} %copy.23), channel_id=1, source_target_pairs={{0,16},{16,32},{32,48},{48,64},{64,80},{80,96},{96,112},{112,128},... | collective-permute-start | bytes 3080 | tf_op jit(solution)/shard_map/ppermute | solution.py:187
  214.7 7.1 %all-to-all-done.3 = bf16[16,64,256]{2,1,0:T(8,128)(2,1)S(1)} async-done(((bf16[16,64,256]{2,1,0:T(8,128)(2,1)}), bf16[16,64,256]{2,1,0:T(8,128)(2,1)S(1)}, u32[]{:S(2)}, u32[]{:S(2)}) %all-to-all-start.3) | async-done | bytes 524320 | tf_op jit(solution)/shard_map/all_to_all | solution.py:327
  221.7 1.0 combine.1.refs_0_
  222.8 2.8 collective-permute-start.11
  225.5 3.4 %collective-permute-start.12 = (bf16[256,256]{1,0:T(8,128)(2,1)}, bf16[256,256]{1,0:T(8,128)(2,1)S(1)}, u32[]{:S(2)}, u32[]{:S(2)}) collective-permute-start(bf16[256,256]{1,0:T(8,128)(2,1)} %combine.1.refs_0_), channel_id=1, source_target_pairs={{0,4},{2,6},{4,8},{6,10},{8,12},{10,14},{12,0},{14,2},{1,5},{3,7},... | collective-permute-start | bytes 393224 | tf_op jit(solution)/shard_map/ppermute | solution.py:180
  228.9 0.8 collective-permute-start.13
  229.7 6.0 %collective-permute-start.14 = (bf16[256,256]{1,0:T(8,128)(2,1)}, bf16[256,256]{1,0:T(8,128)(2,1)S(1)}, u32[]{:S(2)}, u32[]{:S(2)}) collective-permute-start(bf16[256,256]{1,0:T(8,128)(2,1)} %combine.1.refs_0_), channel_id=1, source_target_pairs={{0,6},{2,8},{4,10},{6,12},{8,14},{10,0},{12,2},{14,4},{1,7},{3,9},... | collective-permute-start | bytes 393224 | tf_op jit(solution)/shard_map/ppermute | solution.py:180
  235.7 0.1 collective-permute-start.15
  235.8 3.2 %collective-permute-start.16 = (bf16[256,256]{1,0:T(8,128)(2,1)}, bf16[256,256]{1,0:T(8,128)(2,1)S(1)}, u32[]{:S(2)}, u32[]{:S(2)}) collective-permute-start(bf16[256,256]{1,0:T(8,128)(2,1)} %combine.1.refs_0_), channel_id=1, source_target_pairs={{0,8},{2,10},{4,12},{6,14},{8,0},{10,2},{12,4},{14,6},{1,9},{3,11}... | collective-permute-start | bytes 393224 | tf_op jit(solution)/shard_map/ppermute | solution.py:180
  239.1 0.5 collective-permute-start.18
  239.6 9.7 %collective-permute-done.14.refs_5_ = bf16[256,256]{1,0:T(8,128)(2,1)S(1)} collective-permute-done((bf16[256,256]{1,0:T(8,128)(2,1)}, bf16[256,256]{1,0:T(8,128)(2,1)S(1)}, u32[]{:S(2)}, u32[]{:S(2)}) %collective-permute-start.14) | collective-permute-done | bytes 131104 | tf_op jit(solution)/shard_map/ppermute | solution.py:180
  249.3 0.1 convert_multiply_fusion
  249.5 4.7 %collective-permute-done.15.refs_6_ = bf16[256,256]{1,0:T(8,128)(2,1)S(1)} collective-permute-done((bf16[256,256]{1,0:T(8,128)(2,1)}, bf16[256,256]{1,0:T(8,128)(2,1)S(1)}, u32[]{:S(2)}, u32[]{:S(2)}) %collective-permute-start.15) | collective-permute-done | bytes 131104 | tf_op jit(solution)/shard_map/ppermute | solution.py:180
  254.1 0.5 collective-permute-start.21
  254.7 0.1 collective-permute-start.22
  254.8 0.4 collective-permute-start.23
  255.2 0.1 collective-permute-start.24
  255.3 0.2 multiply_convert_fusion.2
  255.5 0.2 collective-permute-done.21.refs_12_
  255.7 0.3 collective-permute-done.22.refs_13_
  256.0 0.2 collective-permute-done.23.refs_14_
  256.2 0.3 collective-permute-done.24.refs_15_
  256.5 0.9 copy-done.4
  257.4 2.0 proj.1
  259.4 4.4 %all-to-all-start.4 = ((bf16[16,128,256]{2,1,0:T(8,128)(2,1)}), bf16[16,128,256]{2,1,0:T(8,128)(2,1)}, u32[]{:S(2)}, u32[]{:S(2)}) async-start(bf16[16,128,256]{2,1,0:T(8,128)(2,1)} %proj.1), calls=%async_computation.5 | async-start | bytes 2097152 | tf_op jit(solution)/shard_map/all_to_all | solution.py:367
  263.8 2.0 mixer.1
  265.8 1.3 collective-permute-start.25
  267.1 12.1 %collective-permute-done.25 = f32[128,2]{1,0:T(8,128)S(1)} collective-permute-done((f32[128,2]{1,0:T(8,128)S(1)}, f32[128,2]{1,0:T(8,128)S(1)}, u32[]{:S(2)}, u32[]{:S(2)}) %collective-permute-start.25) | collective-permute-done | bytes 1056 | tf_op jit(solution)/shard_map/ppermute | solution.py:187
  279.2 0.8 multiply_convert_fusion
  280.0 0.6 multiply_convert_fusion.1
  280.7 1.6 all-to-all-done.4
  282.3 2.0 convert_reduce_fusion
  (61 shorter events, 0.5 us)
Async XLA Ops:
  7.2 32.9 %copy-start.7 = (bf16[256,256]{1,0:T(8,128)(2,1)S(1)}, bf16[256,256]{1,0:T(8,128)(2,1)}, u32[]{:S(2)}) copy-start(bf16[256,256]{1,0:T(8,128)(2,1)} %cot_ref.1) | copy-start | bytes 393220
  7.2 112.6 %all-gather.2.cloned.1.call-start = ((), (), s32[]{:S(2)}) async-start(), calls=%async_computation.6 | async-start | bytes 8912896 | tf_op jit(solution)/shard_map/all_gather | solution.py:232
  28.4 6.5 %collective-permute-start = (bf16[256,256]{1,0:T(8,128)(2,1)}, bf16[256,256]{1,0:T(8,128)(2,1)S(1)}, u32[]{:S(2)}, u32[]{:S(2)}) collective-permute-start(bf16[256,256]{1,0:T(8,128)(2,1)} %cot_ref.1), channel_id=1, source_target_pairs={{0,2},{2,4},{4,6},{6,8},{8,10},{10,12},{12,14},{14,0},{1,3},{3,5},... | collective-permute-start | bytes 393224 | tf_op jit(solution)/shard_map/ppermute | solution.py:180
  30.4 5.2 %collective-permute-start.1 = (bf16[256,256]{1,0:T(8,128)(2,1)}, bf16[256,256]{1,0:T(8,128)(2,1)S(1)}, u32[]{:S(2)}, u32[]{:S(2)}) collective-permute-start(bf16[256,256]{1,0:T(8,128)(2,1)} %cot_ref.1), channel_id=1, source_target_pairs={{0,14},{2,0},{4,2},{6,4},{8,6},{10,8},{12,10},{14,12},{1,15},{3,1}... | collective-permute-start | bytes 393224 | tf_op jit(solution)/shard_map/ppermute | solution.py:180
  30.5 9.5 %collective-permute-start.2 = (bf16[256,256]{1,0:T(8,128)(2,1)}, bf16[256,256]{1,0:T(8,128)(2,1)S(1)}, u32[]{:S(2)}, u32[]{:S(2)}) collective-permute-start(bf16[256,256]{1,0:T(8,128)(2,1)} %cot_ref.1), channel_id=1, source_target_pairs={{0,4},{2,6},{4,8},{6,10},{8,12},{10,14},{12,0},{14,2},{1,5},{3,7},... | collective-permute-start | bytes 393224 | tf_op jit(solution)/shard_map/ppermute | solution.py:180
  40.0 1.0 copy-start
  41.1 1.0 copy-start.2
  44.1 38.8 %copy-start.1 = (bf16[1024,256]{1,0:T(8,128)(2,1)S(1)}, bf16[1024,256]{1,0:T(8,128)(2,1)}, u32[]{:S(2)}) copy-start(bf16[1024,256]{1,0:T(8,128)(2,1)} %get-tuple-element.23.late_ref.pick_ref) | copy-start | bytes 1572868
  44.1 38.8 %copy-start.3 = (f32[1024,128]{1,0:T(8,128)S(1)}, f32[1024,128]{1,0:T(8,128)}, u32[]{:S(2)}) copy-start(f32[1024,128]{1,0:T(8,128)} %get-tuple-element.24.scale_ref) | copy-start | bytes 1572868
  44.1 40.8 %all-to-all-start.1 = ((bf16[16,64,1024]{2,1,0:T(8,128)(2,1)}), bf16[16,64,1024]{2,1,0:T(8,128)(2,1)S(1)}, u32[]{:S(2)}, u32[]{:S(2)}) async-start(bf16[16,64,1024]{2,1,0:T(8,128)(2,1)} %bitcast.4), calls=%async_computation.1 | async-start | bytes 4194304 | tf_op jit(solution)/shard_map/all_to_all | solution.py:246
  48.5 16.3 %collective-permute-start.4 = (bf16[256,256]{1,0:T(8,128)(2,1)S(1)}, bf16[256,256]{1,0:T(8,128)(2,1)S(1)}, u32[]{:S(2)}, u32[]{:S(2)}) collective-permute-start(bf16[256,256]{1,0:T(8,128)(2,1)S(1)} %copy-done.7), channel_id=1, source_target_pairs={{0,12},{2,14},{4,0},{6,2},{8,4},{10,6},{12,8},{14,10},{1,13},{3,15... | collective-permute-start | bytes 393224 | tf_op jit(solution)/shard_map/ppermute | solution.py:180
  53.1 16.7 %collective-permute-start.5 = (bf16[256,256]{1,0:T(8,128)(2,1)S(1)}, bf16[256,256]{1,0:T(8,128)(2,1)S(1)}, u32[]{:S(2)}, u32[]{:S(2)}) collective-permute-start(bf16[256,256]{1,0:T(8,128)(2,1)S(1)} %copy-done.7), channel_id=1, source_target_pairs={{0,6},{2,8},{4,10},{6,12},{8,14},{10,0},{12,2},{14,4},{1,7},{3,9},... | collective-permute-start | bytes 393224 | tf_op jit(solution)/shard_map/ppermute | solution.py:180
  56.5 19.8 %collective-permute-start.6 = (bf16[256,256]{1,0:T(8,128)(2,1)S(1)}, bf16[256,256]{1,0:T(8,128)(2,1)S(1)}, u32[]{:S(2)}, u32[]{:S(2)}) collective-permute-start(bf16[256,256]{1,0:T(8,128)(2,1)S(1)} %copy-done.7), channel_id=1, source_target_pairs={{0,10},{2,12},{4,14},{6,0},{8,2},{10,4},{12,6},{14,8},{1,11},{3,13... | collective-permute-start | bytes 393224 | tf_op jit(solution)/shard_map/ppermute | solution.py:180
  58.1 24.8 %collective-permute-start.7 = (bf16[256,256]{1,0:T(8,128)(2,1)S(1)}, bf16[256,256]{1,0:T(8,128)(2,1)S(1)}, u32[]{:S(2)}, u32[]{:S(2)}) collective-permute-start(bf16[256,256]{1,0:T(8,128)(2,1)S(1)} %copy-done.7), channel_id=1, source_target_pairs={{0,8},{2,10},{4,12},{6,14},{8,0},{10,2},{12,4},{14,6},{1,9},{3,11}... | collective-permute-start | bytes 393224 | tf_op jit(solution)/shard_map/ppermute | solution.py:180
  85.0 7.2 %copy-start.10 = (bf16[16,64,1024]{2,1,0:T(8,128)(2,1)}, bf16[16,64,1024]{2,1,0:T(8,128)(2,1)S(1)}, u32[]{:S(2)}) copy-start(bf16[16,64,1024]{2,1,0:T(8,128)(2,1)S(1)} %all-to-all-done.1) | copy-start | bytes 6291460
  85.0 34.1 %copy-start.14 = (s32[8]{0:T(128)S(1)}, s32[8]{0:T(128)}, u32[]{:S(2)}) copy-start(s32[8]{0:T(128)} %constant.35) | copy-start | bytes 100
  85.0 34.1 %all-to-all-start.2 = ((bf16[16,64,1024]{2,1,0:T(8,128)(2,1)}), bf16[16,64,1024]{2,1,0:T(8,128)(2,1)}, u32[]{:S(2)}, u32[]{:S(2)}) async-start(bf16[16,64,1024]{2,1,0:T(8,128)(2,1)} %bitcast.9), calls=%async_computation.2 | async-start | bytes 4194304 | tf_op jit(solution)/shard_map/all_to_all | solution.py:246
  92.1 111.4 %reduce-scatter.2.cloned.1.call-start = ((), (), s32[]{:S(2)}) async-start(), calls=%async_computation.7 | async-start | bytes 8912896 | tf_op jit(solution)/shard_map/reduce_scatter | solution.py:297
  92.2 27.5 %collective-permute-start.3 = (bf16[1024,1024]{1,0:T(8,128)(2,1)S(1)}, bf16[1024,1024]{1,0:T(8,128)(2,1)}, u32[]{:S(2)}, u32[]{:S(2)}) collective-permute-start(bf16[1024,1024]{1,0:T(8,128)(2,1)S(1)} %bitcast.30), channel_id=1, source_target_pairs={{0,1},{1,0},{2,3},{3,2},{4,5},{5,4},{6,7},{7,6},{8,9},{9,8},{10,11... | collective-permute-start | bytes 6291464 | tf_op jit(solution)/shard_map/ppermute | solution.py:249
  119.1 10.7 %collective-permute-start.8 = (bf16[1024,1024]{1,0:T(8,128)(2,1)}, bf16[1024,1024]{1,0:T(8,128)(2,1)}, u32[]{:S(2)}, u32[]{:S(2)}) collective-permute-start(bf16[1024,1024]{1,0:T(8,128)(2,1)} %bitcast.10.mine_ref.mh_ref), channel_id=1, source_target_pairs={{0,1},{1,0},{2,3},{3,2},{4,5},{5,4},{6,7},{7,6},{8,9},{9,8},{10,11... | collective-permute-start | bytes 6291464 | tf_op jit(solution)/shard_map/ppermute | solution.py:249
  141.6 68.7 %copy-start.12 = (bf16[128,256]{1,0:T(8,128)(2,1)S(1)}, bf16[128,256]{1,0:T(8,128)(2,1)}, u32[]{:S(2)}) copy-start(bf16[128,256]{1,0:T(8,128)(2,1)} %param.15) | copy-start | bytes 196612
  141.6 68.9 %copy-start.11 = (bf16[128,256]{1,0:T(8,128)(2,1)S(1)}, bf16[128,256]{1,0:T(8,128)(2,1)}, u32[]{:S(2)}) copy-start(bf16[128,256]{1,0:T(8,128)(2,1)} %param.14) | copy-start | bytes 196612
  161.1 74.6 %copy-start.13 = (f32[3,128]{1,0:T(4,128)S(1)}, f32[3,128]{1,0:T(4,128)}, u32[]{:S(2)}) copy-start(f32[3,128]{1,0:T(4,128)} %param.16) | copy-start | bytes 4612
  161.2 94.1 %copy-start.8 = (bf16[128,256]{1,0:T(8,128)(2,1)S(1)}, bf16[128,256]{1,0:T(8,128)(2,1)}, u32[]{:S(2)}) copy-start(bf16[128,256]{1,0:T(8,128)(2,1)} %outer_ref.1) | copy-start | bytes 196612
  161.2 95.4 %copy-start.9 = (s32[16]{0:T(128)S(1)}, s32[16]{0:T(128)}, u32[]{:S(2)}) copy-start(s32[16]{0:T(128)} %pad_add_fusion.slab_ref) | copy-start | bytes 196
  203.6 18.2 %all-to-all-start.3 = ((bf16[16,64,256]{2,1,0:T(8,128)(2,1)}), bf16[16,64,256]{2,1,0:T(8,128)(2,1)S(1)}, u32[]{:S(2)}, u32[]{:S(2)}) async-start(bf16[16,64,256]{2,1,0:T(8,128)(2,1)} %bitcast.40), calls=%async_computation.4 | async-start | bytes 1048576 | tf_op jit(solution)/shard_map/all_to_all | solution.py:327
  210.8 18.8 %collective-permute-start.9 = (bf16[2,128,2]{2,1,0:T(8,128)(2,1)S(1)}, bf16[2,128,2]{2,1,0:T(8,128)(2,1)S(1)}, u32[]{:S(2)}, u32[]{:S(2)}) collective-permute-start(bf16[2,128,2]{2,1,0:T(8,128)(2,1)S(1)} %copy.23), channel_id=1, source_target_pairs={{0,16},{16,32},{32,48},{48,64},{64,80},{80,96},{96,112},{112,128},... | collective-permute-start | bytes 3080 | tf_op jit(solution)/shard_map/ppermute | solution.py:187
  222.8 13.0 %collective-permute-start.10 = (bf16[256,256]{1,0:T(8,128)(2,1)}, bf16[256,256]{1,0:T(8,128)(2,1)S(1)}, u32[]{:S(2)}, u32[]{:S(2)}) collective-permute-start(bf16[256,256]{1,0:T(8,128)(2,1)} %combine.1.refs_0_), channel_id=1, source_target_pairs={{0,2},{2,4},{4,6},{6,8},{8,10},{10,12},{12,14},{14,0},{1,3},{3,5},... | collective-permute-start | bytes 393224 | tf_op jit(solution)/shard_map/ppermute | solution.py:180
  222.8 13.1 %collective-permute-start.11 = (bf16[256,256]{1,0:T(8,128)(2,1)}, bf16[256,256]{1,0:T(8,128)(2,1)S(1)}, u32[]{:S(2)}, u32[]{:S(2)}) collective-permute-start(bf16[256,256]{1,0:T(8,128)(2,1)} %combine.1.refs_0_), channel_id=1, source_target_pairs={{0,14},{2,0},{4,2},{6,4},{8,6},{10,8},{12,10},{14,12},{1,15},{3,1}... | collective-permute-start | bytes 393224 | tf_op jit(solution)/shard_map/ppermute | solution.py:180
  225.5 13.5 %collective-permute-start.12 = (bf16[256,256]{1,0:T(8,128)(2,1)}, bf16[256,256]{1,0:T(8,128)(2,1)S(1)}, u32[]{:S(2)}, u32[]{:S(2)}) collective-permute-start(bf16[256,256]{1,0:T(8,128)(2,1)} %combine.1.refs_0_), channel_id=1, source_target_pairs={{0,4},{2,6},{4,8},{6,10},{8,12},{10,14},{12,0},{14,2},{1,5},{3,7},... | collective-permute-start | bytes 393224 | tf_op jit(solution)/shard_map/ppermute | solution.py:180
  228.9 10.2 %collective-permute-start.13 = (bf16[256,256]{1,0:T(8,128)(2,1)}, bf16[256,256]{1,0:T(8,128)(2,1)S(1)}, u32[]{:S(2)}, u32[]{:S(2)}) collective-permute-start(bf16[256,256]{1,0:T(8,128)(2,1)} %combine.1.refs_0_), channel_id=1, source_target_pairs={{0,12},{2,14},{4,0},{6,2},{8,4},{10,6},{12,8},{14,10},{1,13},{3,15... | collective-permute-start | bytes 393224 | tf_op jit(solution)/shard_map/ppermute | solution.py:180
  229.7 19.6 %collective-permute-start.14 = (bf16[256,256]{1,0:T(8,128)(2,1)}, bf16[256,256]{1,0:T(8,128)(2,1)S(1)}, u32[]{:S(2)}, u32[]{:S(2)}) collective-permute-start(bf16[256,256]{1,0:T(8,128)(2,1)} %combine.1.refs_0_), channel_id=1, source_target_pairs={{0,6},{2,8},{4,10},{6,12},{8,14},{10,0},{12,2},{14,4},{1,7},{3,9},... | collective-permute-start | bytes 393224 | tf_op jit(solution)/shard_map/ppermute | solution.py:180
  235.7 18.4 %collective-permute-start.15 = (bf16[256,256]{1,0:T(8,128)(2,1)}, bf16[256,256]{1,0:T(8,128)(2,1)S(1)}, u32[]{:S(2)}, u32[]{:S(2)}) collective-permute-start(bf16[256,256]{1,0:T(8,128)(2,1)} %combine.1.refs_0_), channel_id=1, source_target_pairs={{0,10},{2,12},{4,14},{6,0},{8,2},{10,4},{12,6},{14,8},{1,11},{3,13... | collective-permute-start | bytes 393224 | tf_op jit(solution)/shard_map/ppermute | solution.py:180
  235.8 18.3 %collective-permute-start.16 = (bf16[256,256]{1,0:T(8,128)(2,1)}, bf16[256,256]{1,0:T(8,128)(2,1)S(1)}, u32[]{:S(2)}, u32[]{:S(2)}) collective-permute-start(bf16[256,256]{1,0:T(8,128)(2,1)} %combine.1.refs_0_), channel_id=1, source_target_pairs={{0,8},{2,10},{4,12},{6,14},{8,0},{10,2},{12,4},{14,6},{1,9},{3,11}... | collective-permute-start | bytes 393224 | tf_op jit(solution)/shard_map/ppermute | solution.py:180
  239.1 15.6 %collective-permute-start.17 = (bf16[256,256]{1,0:T(8,128)(2,1)}, bf16[256,256]{1,0:T(8,128)(2,1)S(1)}, u32[]{:S(2)}, u32[]{:S(2)}) collective-permute-start(bf16[256,256]{1,0:T(8,128)(2,1)} %combine.1.refs_0_), channel_id=1, source_target_pairs={{0,1},{1,0},{2,3},{3,2},{4,5},{5,4},{6,7},{7,6},{8,9},{9,8},{10,11... | collective-permute-start | bytes 393224 | tf_op jit(solution)/shard_map/ppermute | solution.py:338
  239.1 15.7 %collective-permute-start.18 = (bf16[256,256]{1,0:T(8,128)(2,1)S(1)}, bf16[256,256]{1,0:T(8,128)(2,1)S(1)}, u32[]{:S(2)}, u32[]{:S(2)}) collective-permute-start(bf16[256,256]{1,0:T(8,128)(2,1)S(1)} %collective-permute-done.10.refs_1_), channel_id=1, source_target_pairs={{0,1},{1,0},{2,3},{3,2},{4,5},{5,4},{6,7},{7,6},{8,9},{9,8},{10,11... | collective-permute-start | bytes 393224 | tf_op jit(solution)/shard_map/ppermute | solution.py:338
  249.3 5.8 %collective-permute-start.19 = (bf16[256,256]{1,0:T(8,128)(2,1)S(1)}, bf16[256,256]{1,0:T(8,128)(2,1)S(1)}, u32[]{:S(2)}, u32[]{:S(2)}) collective-permute-start(bf16[256,256]{1,0:T(8,128)(2,1)S(1)} %collective-permute-done.11.refs_2_), channel_id=1, source_target_pairs={{0,1},{1,0},{2,3},{3,2},{4,5},{5,4},{6,7},{7,6},{8,9},{9,8},{10,11... | collective-permute-start | bytes 393224 | tf_op jit(solution)/shard_map/ppermute | solution.py:338
  254.1 1.3 collective-permute-start.20
  254.1 1.5 collective-permute-start.21
  254.7 1.3 collective-permute-start.22
  254.8 1.4 collective-permute-start.23
  255.2 1.3 collective-permute-start.24
  256.5 0.9 copy-start.4
  257.4 6.3 %copy-start.5 = (bf16[256,256]{1,0:T(8,128)(2,1)S(1)}, bf16[256,256]{1,0:T(8,128)(2,1)}, u32[]{:S(2)}) copy-start(bf16[256,256]{1,0:T(8,128)(2,1)} %combine.1.refs_0_) | copy-start | bytes 393220
  257.4 6.3 %copy-start.6 = (bf16[128,4096]{1,0:T(8,128)(2,1)S(1)}, bf16[128,4096]{1,0:T(8,128)(2,1)}, u32[]{:S(2)}) copy-start(bf16[128,4096]{1,0:T(8,128)(2,1)} %proj_ref.1) | copy-start | bytes 3145732
  259.4 22.9 %all-to-all-start.4 = ((bf16[16,128,256]{2,1,0:T(8,128)(2,1)}), bf16[16,128,256]{2,1,0:T(8,128)(2,1)}, u32[]{:S(2)}, u32[]{:S(2)}) async-start(bf16[16,128,256]{2,1,0:T(8,128)(2,1)} %proj.1), calls=%async_computation.5 | async-start | bytes 2097152 | tf_op jit(solution)/shard_map/all_to_all | solution.py:367
  265.8 13.4 %collective-permute-start.25 = (f32[128,2]{1,0:T(8,128)S(1)}, f32[128,2]{1,0:T(8,128)S(1)}, u32[]{:S(2)}, u32[]{:S(2)}) collective-permute-start(f32[128,2]{1,0:T(8,128)S(1)} %slice.52), channel_id=1, source_target_pairs={{16,0},{32,16},{48,32},{64,48},{80,64},{96,80},{112,96},{128,112},... | collective-permute-start | bytes 3080 | tf_op jit(solution)/shard_map/ppermute | solution.py:187
Sparse Core Ops, SparseCore 0:
  28.5 72.3 all-gather.1
  141.7 61.8 reduce-scatter.1

commit v4 on v1

--- a/solution.py
+++ b/solution.py
@@ -24,6 +24,10 @@
 
 def dot_tn(a, b):
     return lax.dot_general(a, b, (((0,), (0,)), ((), ())), preferred_element_type=F32)
+
+
+def grant(mib):
+    return pltpu.CompilerParams(vmem_limit_bytes=mib << 20)
 
 
 def cost(flops, nbytes):
@@ -52,14 +56,12 @@
 
 
 def spread_kernel(pick_ref, scale_ref, *refs):
-    pieces, (low_ref, high_ref) = refs[:-2], refs[-2:]
+    pieces, out_ref = refs[:-1], refs[-1]
     width = pieces[0].shape[1]
-    half = len(pieces) // 2
     scale = scale_ref[:, 0:1]
     for j, piece in enumerate(pieces):
         rows = (dot_nn(pick_ref[...], piece[...]) * scale).astype(BF16)
-        out = low_ref if j < half else high_ref
-        out[:, (j % half) * width : (j % half + 1) * width] = rows
+        out_ref[:, j * width : (j + 1) * width] = rows
 
 
 def expert_kernel(
@@ -197,13 +199,14 @@
     state_all = lax.all_gather(recv_state.reshape(slots, width), TP, axis=0, tiled=False)
 
     half = z_size // 2 * width
-    cot_low, cot_high = pl.pallas_call(
-        spread_kernel,
-        out_shape=(shape((slots, half), BF16),) * 2,
-        cost_estimate=cost(4 * slots * tok_count * half, 8 * slots * half),
-        name="spread",
-    )(pick, scale, *cot_pieces)
     swap = [(0, 1), (1, 0)]
+
+    def spread(pieces):
+        return pl.pallas_call(
+            spread_kernel,
+            out_shape=shape((slots, half), BF16),
+            cost_estimate=cost(2 * slots * tok_count * half, 4 * slots * half),
+        )(pick, scale, *pieces)
 
     def exchanged(part):
         got = lax.all_to_all(
@@ -211,8 +214,8 @@
         ).reshape(slots, half)
         return got, lax.ppermute(got, "c", swap)
 
-    my_low, their_low = exchanged(cot_low)
-    my_high, their_high = exchanged(cot_high)
+    my_low, their_low = exchanged(spread(cot_pieces[: z_size // 2]))
+    my_high, their_high = exchanged(spread(cot_pieces[z_size // 2 :]))
     cots = (my_low, my_high, their_low, their_high)
 
     block = 256
@@ -277,6 +280,7 @@
         out_shape=shape((tok_count, width), BF16),
         cost_estimate=cost(2 * slots * tok_count * width, 4 * slots * width),
         name="combine",
+        compiler_params=grant(16),
     )(pick, arrived, cotangent)
     near = gathered(grad_mixed, "z")
     full_back = near + [lax.ppermute(piece, "c", swap) for piece in near]

time: 303 us -> 290 us (0.957)
  blocking collectives: 41.1 us -> 16.5 us
  waiting for transfers between devices: 117 us -> 123 us
  starting transfers between devices: 66.3 us -> 70.8 us
    all_to_all x1 -> x0, blocking collectives: 24.6 us -> none  [exchanged(): lax.all_to_all(part.reshape(experts, cap, half), 'sp', split_axis=0, conc...]
    ppermute x14, waiting for transfers between devices: 24.7 us -> 32.6 us  [gathered(): lax.ppermute(value, axis, [(i, (i + k) % size) for i in range(size)])]
    all_to_all x1 -> x2, starting transfers between devices: 6.68 us -> 14.6 us  [exchanged(): lax.all_to_all(part.reshape(experts, cap, half), 'sp', split_axis=0, conc...]
    reduce_scatter x1, waiting for transfers between devices: 58.8 us -> 54.9 us  [shards(): lax.psum_scatter(partial_value, TP, scatter_dimension=0, tiled=False)]
    ppermute x14, starting transfers between devices: 36.7 us -> 32.9 us  [gathered(): lax.ppermute(value, axis, [(i, (i + k) % size) for i in range(size)])]
    pallas_call x1 -> x2, Pallas kernels: 4.25 us -> 6.82 us  [spread(): pl.pallas_call(spread_kernel, out_shape=shape((slots, half), BF16), cost_...]
    all_to_all x1 -> x2, waiting for transfers between devices: 20.6 us -> 22.7 us  [exchanged(): lax.all_to_all(part.reshape(experts, cap, half), 'sp', split_axis=0, conc...]
  transfers between devices with their start and end apart: 31 -> 32, of which waited for: 13 -> 14; matrix products, arithmetic and copies ran while one was open for 2% -> 2% of each run, Pallas kernels for 10% -> 11%
where the time goes in v4:
time: 290 us; the launch traced here: 285 us
  waiting for transfers between devices  123 us (42%)
  starting transfers between devices  70.8 us (24%)
  Pallas kernels  50.7 us (17%)
  blocking collectives  16.5 us (6%)
  between operations  14.4 us (5%)
  other arithmetic  4.77 us (2%)
  local copies, waits for them, and re-layouts  4.25 us (1%)
    reduce_scatter x1, waiting for transfers between devices, shards(): lax.psum_scatter(partial_value, TP, scatter_dimension=0, tiled=False)  54.9 us
    ppermute x14, starting transfers between devices, gathered(): lax.ppermute(value, axis, [(i, (i + k) % size) for i in range(size)])  32.9 us
    ppermute x14, waiting for transfers between devices, gathered(): lax.ppermute(value, axis, [(i, (i + k) % size) for i in range(size)])  32.6 us
    all_to_all x2, waiting for transfers between devices, exchanged(): lax.all_to_all(part.reshape(experts, cap, half), 'sp', split_axis=0, conc...  22.7 us
    pallas_call x1, Pallas kernels, shards(): pl.pallas_call(weight_grad_kernel, grid_spec=pltpu.PrefetchScalarGridSpec...  19.4 us
    all_to_all x1, blocking collectives, shards(): lax.all_to_all(sent_state.reshape(experts, cap, width), 'sp', split_axis=...  16.5 us
    all_to_all x2, starting transfers between devices, exchanged(): lax.all_to_all(part.reshape(experts, cap, half), 'sp', split_axis=0, conc...  14.6 us
    pallas_call x1, Pallas kernels, shards(): pl.pallas_call(expert_kernel, grid_spec=pltpu.PrefetchScalarGridSpec(num_...  14.4 us
  transfers between devices with their start and end apart: 32, of which 14 were waited for; matrix products, arithmetic and copies ran while one was open for 2% of the time, Pallas kernels for 11%

profile of v4, /device:TPU:24, one launch (start us, length us, event | category | flops | bytes accessed | tf_op | source)
XLA Modules:
  0.0 284.7 jit_solution(7790125207100827435)
XLA Ops:
  7.2 2.5 route.1
  9.7 16.5 %all_to_all.25 = bf16[16,64,256]{2,1,0:T(8,128)(2,1)} all-to-all(bf16[16,64,256]{2,1,0:T(8,128)(2,1)} %bitcast.40), channel_id=1, replica_groups=mesh['sp'=16,'z'=8,'c'=2] {'sp'}, dimensions={0} | all-to-all | bytes 1048576 | tf_op jit(solution)/shard_map/all_to_all | solution.py:196
  26.2 2.0 collective-permute-start
  28.2 4.0 %collective-permute-start.1 = (bf16[256,256]{1,0:T(8,128)(2,1)}, bf16[256,256]{1,0:T(8,128)(2,1)S(1)}, u32[]{:S(2)}, u32[]{:S(2)}) collective-permute-start(bf16[256,256]{1,0:T(8,128)(2,1)} %cot_ref.1), channel_id=1, source_target_pairs={{0,14},{2,0},{4,2},{6,4},{8,6},{10,8},{12,10},{14,12},{1,15},{3,1}... | collective-permute-start | bytes 393224 | tf_op jit(solution)/shard_map/ppermute | solution.py:147
  32.2 4.2 %collective-permute-done.refs_1_ = bf16[256,256]{1,0:T(8,128)(2,1)S(1)} collective-permute-done((bf16[256,256]{1,0:T(8,128)(2,1)}, bf16[256,256]{1,0:T(8,128)(2,1)S(1)}, u32[]{:S(2)}, u32[]{:S(2)}) %collective-permute-start) | collective-permute-done | bytes 131104 | tf_op jit(solution)/shard_map/ppermute | solution.py:147
  36.5 5.0 %collective-permute-done.2.refs_3_ = bf16[256,256]{1,0:T(8,128)(2,1)S(1)} collective-permute-done((bf16[256,256]{1,0:T(8,128)(2,1)}, bf16[256,256]{1,0:T(8,128)(2,1)S(1)}, u32[]{:S(2)}, u32[]{:S(2)}) %collective-permute-start.2) | collective-permute-done | bytes 131104 | tf_op jit(solution)/shard_map/ppermute | solution.py:147
  41.5 0.6 copy-done.27
  42.1 3.4 %shard_map.188 = bf16[1024,1024]{1,0:T(8,128)(2,1)} custom-call(bf16[1024,256]{1,0:T(8,128)(2,1)} %get-tuple-element.23.pick_ref, f32[1024,128]{1,0:T(8,128)} %get-tuple-element.24.scale_ref, bf16[256,256]{1,0:T(8,128)(2,1)} %cot_ref.1, bf16[256,256]{1,0:T(8,128)(2,1)} %copy-done.24, bf16[256,256]{1,0:T(8,128)(2,1)} %copy-done.26, bf16[256,256]{1,0:T(8,128)(2,1)} %copy-done.27), custom_call_target="tpu_custom_call" | custom-call | flops 536870912 | bytes 4194304 | tf_op jit(solution)/shard_map/pallas_call | solution.py:205
  45.5 7.3 %all-to-all-start.1 = ((bf16[16,64,1024]{2,1,0:T(8,128)(2,1)}), bf16[16,64,1024]{2,1,0:T(8,128)(2,1)S(1)}, u32[]{:S(2)}, u32[]{:S(2)}) async-start(bf16[16,64,1024]{2,1,0:T(8,128)(2,1)} %bitcast.33), calls=%async_computation.1 | async-start | bytes 4194304 | tf_op jit(solution)/shard_map/all_to_all | solution.py:212
  52.8 0.1 collective-permute-start.3
  52.9 0.1 collective-permute-start.4
  53.0 5.0 %collective-permute-start.5 = (bf16[256,256]{1,0:T(8,128)(2,1)S(1)}, bf16[256,256]{1,0:T(8,128)(2,1)S(1)}, u32[]{:S(2)}, u32[]{:S(2)}) collective-permute-start(bf16[256,256]{1,0:T(8,128)(2,1)S(1)} %copy-done.1), channel_id=1, source_target_pairs={{0,10},{2,12},{4,14},{6,0},{8,2},{10,4},{12,6},{14,8},{1,11},{3,13... | collective-permute-start | bytes 393224 | tf_op jit(solution)/shard_map/ppermute | solution.py:147
  58.0 4.8 %collective-permute-start.6 = (bf16[256,256]{1,0:T(8,128)(2,1)S(1)}, bf16[256,256]{1,0:T(8,128)(2,1)S(1)}, u32[]{:S(2)}, u32[]{:S(2)}) collective-permute-start(bf16[256,256]{1,0:T(8,128)(2,1)S(1)} %copy-done.1), channel_id=1, source_target_pairs={{0,8},{2,10},{4,12},{6,14},{8,0},{10,2},{12,4},{14,6},{1,9},{3,11}... | collective-permute-start | bytes 393224 | tf_op jit(solution)/shard_map/ppermute | solution.py:147
  62.9 3.8 %collective-permute-done.3.refs_0_ = bf16[256,256]{1,0:T(8,128)(2,1)S(1)} collective-permute-done((bf16[256,256]{1,0:T(8,128)(2,1)S(1)}, bf16[256,256]{1,0:T(8,128)(2,1)S(1)}, u32[]{:S(2)}, u32[]{:S(2)}) %collective-permute-start.3) | collective-permute-done | bytes 131104 | tf_op jit(solution)/shard_map/ppermute | solution.py:147
  66.7 1.6 collective-permute-done.4.refs_1_
  68.3 5.0 %collective-permute-done.5.refs_2_ = bf16[256,256]{1,0:T(8,128)(2,1)S(1)} collective-permute-done((bf16[256,256]{1,0:T(8,128)(2,1)S(1)}, bf16[256,256]{1,0:T(8,128)(2,1)S(1)}, u32[]{:S(2)}, u32[]{:S(2)}) %collective-permute-start.5) | collective-permute-done | bytes 131104 | tf_op jit(solution)/shard_map/ppermute | solution.py:147
  73.4 4.7 %collective-permute-done.6.refs_3_ = bf16[256,256]{1,0:T(8,128)(2,1)S(1)} collective-permute-done((bf16[256,256]{1,0:T(8,128)(2,1)S(1)}, bf16[256,256]{1,0:T(8,128)(2,1)S(1)}, u32[]{:S(2)}, u32[]{:S(2)}) %collective-permute-start.6) | collective-permute-done | bytes 131104 | tf_op jit(solution)/shard_map/ppermute | solution.py:147
  78.1 0.6 copy-done.25
  78.7 3.4 %shard_map.189 = bf16[1024,1024]{1,0:T(8,128)(2,1)} custom-call(bf16[1024,256]{1,0:T(8,128)(2,1)} %get-tuple-element.23.pick_ref, f32[1024,128]{1,0:T(8,128)} %get-tuple-element.24.scale_ref, bf16[256,256]{1,0:T(8,128)(2,1)} %copy-done.21, bf16[256,256]{1,0:T(8,128)(2,1)} %copy-done.22, bf16[256,256]{1,0:T(8,128)(2,1)} %copy-done.23, bf16[256,256]{1,0:T(8,128)(2,1)} %copy-done.25), custom_call_target="tpu_custom_call" | custom-call | flops 536870912 | bytes 4194304 | tf_op jit(solution)/shard_map/pallas_call | solution.py:205
  82.2 7.2 %all-to-all-start.2 = ((bf16[16,64,1024]{2,1,0:T(8,128)(2,1)}), bf16[16,64,1024]{2,1,0:T(8,128)(2,1)}, u32[]{:S(2)}, u32[]{:S(2)}) async-start(bf16[16,64,1024]{2,1,0:T(8,128)(2,1)} %bitcast.34), calls=%async_computation.2 | async-start | bytes 4194304 | tf_op jit(solution)/shard_map/all_to_all | solution.py:212
  89.5 0.1 collective-permute-start.7
  89.6 22.7 %all-to-all-done.2 = bf16[16,64,1024]{2,1,0:T(8,128)(2,1)} async-done(((bf16[16,64,1024]{2,1,0:T(8,128)(2,1)}), bf16[16,64,1024]{2,1,0:T(8,128)(2,1)}, u32[]{:S(2)}, u32[]{:S(2)}) %all-to-all-start.2) | async-done | bytes 2097184 | tf_op jit(solution)/shard_map/all_to_all | solution.py:212
  112.3 0.6 pad_add_fusion.slab_ref
  112.9 3.9 %collective-permute-done.8.th_ref = bf16[1024,1024]{1,0:T(8,128)(2,1)} collective-permute-done((bf16[1024,1024]{1,0:T(8,128)(2,1)}, bf16[1024,1024]{1,0:T(8,128)(2,1)}, u32[]{:S(2)}, u32[]{:S(2)}) %collective-permute-start.8) | collective-permute-done | bytes 2097184 | tf_op jit(solution)/shard_map/ppermute | solution.py:215
  116.7 14.4 %expert.1 = (bf16[16,1024,256]{2,1,0:T(8,128)(2,1)}, bf16[1024,384]{1,0:T(8,128)(2,1)}) custom-call(s32[16]{0:T(128)} %pad_add_fusion.slab_ref, bf16[16,1024,256]{2,1,0:T(8,128)(2,1)} %all-gather.2.cloned.1.call-done.state_ref, bf16[1024,1024]{1,0:T(8,128)(2,1)} %bitcast.31, bf16[1024,1024]{1,0:T(8,128)(2,1)} %bitcast.7.mh_ref, ...), custom_call_target="tpu_custom_call" | custom-call | flops 5368709120 | bytes 25165824 | tf_op jit(solution)/shard_map/expert/pallas_call | solution.py:224
  131.2 19.4 %weight_grads.1 = (f32[128,4096]{1,0:T(8,128)}, f32[128,4096]{1,0:T(8,128)}, f32[128,4096]{1,0:T(8,128)}) custom-call(s32[16]{0:T(128)} %pad_add_fusion.slab_ref, bf16[1024,384]{1,0:T(8,128)(2,1)} %get-tuple-element.26.act_ref, bf16[16,1024,256]{2,1,0:T(8,128)(2,1)} %all-gather.2.cloned.1.call-done.state_ref, bf16[1024,1024]{1,0:T(8,128)(2,1)} %bitcast.32, ...), custom_call_target="tpu_custom_call" | custom-call | flops 3221225472 | bytes 25165824 | tf_op jit(solution)/shard_map/weight_grads/pallas_call | solution.py:255
  150.6 54.9 %reduce-scatter.2.cloned.1.call-done = bf16[1,1024,256]{2,1,0:T(8,128)(2,1)} async-done(((bf16[16,1024,256]{2,1,0:T(8,128)(2,1)}), bf16[1,1024,256]{2,1,0:T(8,128)(2,1)}) %reduce-scatter.2.cloned.1.call-update) | async-done | bytes 524304 | tf_op jit(solution)/shard_map/reduce_scatter | solution.py:245
  205.5 7.2 %all-to-all-start.3 = ((bf16[16,64,256]{2,1,0:T(8,128)(2,1)}), bf16[16,64,256]{2,1,0:T(8,128)(2,1)S(1)}, u32[]{:S(2)}, u32[]{:S(2)}) async-start(bf16[16,64,256]{2,1,0:T(8,128)(2,1)} %bitcast.39), calls=%async_computation.4 | async-start | bytes 1048576 | tf_op jit(solution)/shard_map/all_to_all | solution.py:275
  212.7 0.1 slice.44
  212.7 0.1 copy.25
  212.8 0.1 slice.43
  212.9 0.1 copy.24
  213.0 0.1 copy.23
  213.2 3.4 %collective-permute-start.9 = (bf16[2,128,2]{2,1,0:T(8,128)(2,1)S(1)}, bf16[2,128,2]{2,1,0:T(8,128)(2,1)S(1)}, u32[]{:S(2)}, u32[]{:S(2)}) collective-permute-start(bf16[2,128,2]{2,1,0:T(8,128)(2,1)S(1)} %copy.23), channel_id=1, source_target_pairs={{0,16},{16,32},{32,48},{48,64},{64,80},{80,96},{96,112},{112,128},... | collective-permute-start | bytes 3080 | tf_op jit(solution)/shard_map/ppermute | solution.py:154
  216.6 4.0 %all-to-all-done.3 = bf16[16,64,256]{2,1,0:T(8,128)(2,1)S(1)} async-done(((bf16[16,64,256]{2,1,0:T(8,128)(2,1)}), bf16[16,64,256]{2,1,0:T(8,128)(2,1)S(1)}, u32[]{:S(2)}, u32[]{:S(2)}) %all-to-all-start.3) | async-done | bytes 524320 | tf_op jit(solution)/shard_map/all_to_all | solution.py:275
  220.5 1.0 combine.1.refs_0_
  221.5 3.2 %collective-permute-start.11 = (bf16[256,256]{1,0:T(8,128)(2,1)}, bf16[256,256]{1,0:T(8,128)(2,1)S(1)}, u32[]{:S(2)}, u32[]{:S(2)}) collective-permute-start(bf16[256,256]{1,0:T(8,128)(2,1)} %combine.1.refs_0_), channel_id=1, source_target_pairs={{0,14},{2,0},{4,2},{6,4},{8,6},{10,8},{12,10},{14,12},{1,15},{3,1}... | collective-permute-start | bytes 393224 | tf_op jit(solution)/shard_map/ppermute | solution.py:147
  224.8 4.1 %collective-permute-start.13 = (bf16[256,256]{1,0:T(8,128)(2,1)}, bf16[256,256]{1,0:T(8,128)(2,1)S(1)}, u32[]{:S(2)}, u32[]{:S(2)}) collective-permute-start(bf16[256,256]{1,0:T(8,128)(2,1)} %combine.1.refs_0_), channel_id=1, source_target_pairs={{0,12},{2,14},{4,0},{6,2},{8,4},{10,6},{12,8},{14,10},{1,13},{3,15... | collective-permute-start | bytes 393224 | tf_op jit(solution)/shard_map/ppermute | solution.py:147
  228.9 0.5 collective-permute-start.14
  229.4 4.6 %collective-permute-start.15 = (bf16[256,256]{1,0:T(8,128)(2,1)}, bf16[256,256]{1,0:T(8,128)(2,1)S(1)}, u32[]{:S(2)}, u32[]{:S(2)}) collective-permute-start(bf16[256,256]{1,0:T(8,128)(2,1)} %combine.1.refs_0_), channel_id=1, source_target_pairs={{0,10},{2,12},{4,14},{6,0},{8,2},{10,4},{12,6},{14,8},{1,11},{3,13... | collective-permute-start | bytes 393224 | tf_op jit(solution)/shard_map/ppermute | solution.py:147
  234.0 4.4 %collective-permute-start.16 = (bf16[256,256]{1,0:T(8,128)(2,1)}, bf16[256,256]{1,0:T(8,128)(2,1)S(1)}, u32[]{:S(2)}, u32[]{:S(2)}) collective-permute-start(bf16[256,256]{1,0:T(8,128)(2,1)} %combine.1.refs_0_), channel_id=1, source_target_pairs={{0,8},{2,10},{4,12},{6,14},{8,0},{10,2},{12,4},{14,6},{1,9},{3,11}... | collective-permute-start | bytes 393224 | tf_op jit(solution)/shard_map/ppermute | solution.py:147
  238.4 0.5 collective-permute-start.18
  238.9 6.9 %collective-permute-done.14.refs_5_ = bf16[256,256]{1,0:T(8,128)(2,1)S(1)} collective-permute-done((bf16[256,256]{1,0:T(8,128)(2,1)}, bf16[256,256]{1,0:T(8,128)(2,1)S(1)}, u32[]{:S(2)}, u32[]{:S(2)}) %collective-permute-start.14) | collective-permute-done | bytes 131104 | tf_op jit(solution)/shard_map/ppermute | solution.py:147
  245.9 0.1 convert_multiply_fusion
  246.0 1.3 collective-permute-done.15.refs_6_
  247.3 0.5 collective-permute-start.21
  247.8 0.3 collective-permute-start.22
  248.1 0.2 collective-permute-start.23
  248.3 0.3 collective-permute-start.24
  248.6 0.9 multiply_convert_fusion.2
  249.6 0.1 collective-permute-done.24.refs_15_
  249.7 0.4 copy-done.13
  250.1 0.1 copy-done.14
  250.3 0.1 copy-done.17
  250.3 3.1 %proj.1 = bf16[16,128,256]{2,1,0:T(8,128)(2,1)} custom-call(s32[16]{0:T(128)} %pad_add_fusion.slab_ref, bf16[128,256]{1,0:T(8,128)(2,1)} %get-tuple-element.38.act_ref, bf16[256,256]{1,0:T(8,128)(2,1)} %combine.1.refs_0_, bf16[256,256]{1,0:T(8,128)(2,1)} %copy-done.3, bf16[256,256]{1,0:T(8,128)(2,1)} %copy-done.4, bf16[256,256]{1,0:T(8,128)(2,1)} %copy-done.5, ...), custom_call_target="tpu_custom_call" | custom-call | flops 268435456 | bytes 4194304 | tf_op jit(solution)/shard_map/proj/pallas_call | solution.py:307
  253.4 5.9 %all-to-all-start.4 = ((bf16[16,128,256]{2,1,0:T(8,128)(2,1)}), bf16[16,128,256]{2,1,0:T(8,128)(2,1)S(1)}, u32[]{:S(2)}, u32[]{:S(2)}) async-start(bf16[16,128,256]{2,1,0:T(8,128)(2,1)} %proj.1), calls=%async_computation.5 | async-start | bytes 2097152 | tf_op jit(solution)/shard_map/all_to_all | solution.py:314
  259.3 3.5 %mixer.1 = (bf16[128,256]{1,0:T(8,128)(2,1)}, f32[128,256]{1,0:T(8,128)}) custom-call(s32[16]{0:T(128)} %pad_add_fusion.slab_ref, bf16[128,4096]{1,0:T(8,128)(2,1)} %proj_ref.1, f32[128,256]{1,0:T(8,128)} %get-tuple-element.39.conv_ref, bf16[128,256]{1,0:T(8,128)(2,1)} %outer_ref.1, bf16[256,256]{1,0:T(8,128)(2,1)} %combine.1.refs_0_, ...), custom_call_target="tpu_custom_call" | custom-call | flops 268435456 | bytes 4194304 | tf_op jit(solution)/shard_map/mixer/pallas_call | solution.py:316
  262.8 0.8 slice.52
  263.7 4.9 %collective-permute-start.25 = (f32[128,2]{1,0:T(8,128)S(1)}, f32[128,2]{1,0:T(8,128)S(1)}, u32[]{:S(2)}, u32[]{:S(2)}) collective-permute-start(f32[128,2]{1,0:T(8,128)S(1)} %slice.52), channel_id=1, source_target_pairs={{16,0},{32,16},{48,32},{64,48},{80,64},{96,80},{112,96},{128,112},... | collective-permute-start | bytes 3080 | tf_op jit(solution)/shard_map/ppermute | solution.py:154
  268.5 0.9 constant_dynamic-update-slice_fusion.1
  269.4 5.2 %collective-permute-done.25 = f32[128,2]{1,0:T(8,128)S(1)} collective-permute-done((f32[128,2]{1,0:T(8,128)S(1)}, f32[128,2]{1,0:T(8,128)S(1)}, u32[]{:S(2)}, u32[]{:S(2)}) %collective-permute-start.25) | collective-permute-done | bytes 1056 | tf_op jit(solution)/shard_map/ppermute | solution.py:154
  274.7 1.7 multiply_convert_fusion
  276.4 0.6 multiply_convert_fusion.1
  277.0 0.8 convert_reduce_fusion
  (90 shorter events, 0.4 us)
Async XLA Ops:
  7.2 109.6 %all-gather.2.cloned.1.call-start = ((), (), s32[]{:S(2)}) async-start(), calls=%async_computation.6 | async-start | bytes 8912896 | tf_op jit(solution)/shard_map/all_gather | solution.py:199
  26.2 10.3 %collective-permute-start = (bf16[256,256]{1,0:T(8,128)(2,1)}, bf16[256,256]{1,0:T(8,128)(2,1)S(1)}, u32[]{:S(2)}, u32[]{:S(2)}) collective-permute-start(bf16[256,256]{1,0:T(8,128)(2,1)} %cot_ref.1), channel_id=1, source_target_pairs={{0,2},{2,4},{4,6},{6,8},{8,10},{10,12},{12,14},{14,0},{1,3},{3,5},... | collective-permute-start | bytes 393224 | tf_op jit(solution)/shard_map/ppermute | solution.py:147
  28.2 8.3 %collective-permute-start.1 = (bf16[256,256]{1,0:T(8,128)(2,1)}, bf16[256,256]{1,0:T(8,128)(2,1)S(1)}, u32[]{:S(2)}, u32[]{:S(2)}) collective-permute-start(bf16[256,256]{1,0:T(8,128)(2,1)} %cot_ref.1), channel_id=1, source_target_pairs={{0,14},{2,0},{4,2},{6,4},{8,6},{10,8},{12,10},{14,12},{1,15},{3,1}... | collective-permute-start | bytes 393224 | tf_op jit(solution)/shard_map/ppermute | solution.py:147
  32.2 9.2 %collective-permute-start.2 = (bf16[256,256]{1,0:T(8,128)(2,1)}, bf16[256,256]{1,0:T(8,128)(2,1)S(1)}, u32[]{:S(2)}, u32[]{:S(2)}) collective-permute-start(bf16[256,256]{1,0:T(8,128)(2,1)} %cot_ref.1), channel_id=1, source_target_pairs={{0,4},{2,6},{4,8},{6,10},{8,12},{10,14},{12,0},{14,2},{1,5},{3,7},... | collective-permute-start | bytes 393224 | tf_op jit(solution)/shard_map/ppermute | solution.py:147
  36.5 5.0 %copy-start.24 = (bf16[256,256]{1,0:T(8,128)(2,1)}, bf16[256,256]{1,0:T(8,128)(2,1)S(1)}, u32[]{:S(2)}) copy-start(bf16[256,256]{1,0:T(8,128)(2,1)S(1)} %collective-permute-done.refs_1_) | copy-start | bytes 393220
  36.5 5.0 %copy-start.26 = (bf16[256,256]{1,0:T(8,128)(2,1)}, bf16[256,256]{1,0:T(8,128)(2,1)S(1)}, u32[]{:S(2)}) copy-start(bf16[256,256]{1,0:T(8,128)(2,1)S(1)} %collective-permute-done.1.refs_2_) | copy-start | bytes 393220
  41.5 0.7 copy-start.27
  45.5 7.3 %copy-start.1 = (bf16[256,256]{1,0:T(8,128)(2,1)S(1)}, bf16[256,256]{1,0:T(8,128)(2,1)}, u32[]{:S(2)}) copy-start(bf16[256,256]{1,0:T(8,128)(2,1)} %cot_ref.1) | copy-start | bytes 393220
  45.5 36.7 %all-to-all-start.1 = ((bf16[16,64,1024]{2,1,0:T(8,128)(2,1)}), bf16[16,64,1024]{2,1,0:T(8,128)(2,1)S(1)}, u32[]{:S(2)}, u32[]{:S(2)}) async-start(bf16[16,64,1024]{2,1,0:T(8,128)(2,1)} %bitcast.33), calls=%async_computation.1 | async-start | bytes 4194304 | tf_op jit(solution)/shard_map/all_to_all | solution.py:212
  52.8 13.8 %collective-permute-start.3 = (bf16[256,256]{1,0:T(8,128)(2,1)S(1)}, bf16[256,256]{1,0:T(8,128)(2,1)S(1)}, u32[]{:S(2)}, u32[]{:S(2)}) collective-permute-start(bf16[256,256]{1,0:T(8,128)(2,1)S(1)} %copy-done.1), channel_id=1, source_target_pairs={{0,12},{2,14},{4,0},{6,2},{8,4},{10,6},{12,8},{14,10},{1,13},{3,15... | collective-permute-start | bytes 393224 | tf_op jit(solution)/shard_map/ppermute | solution.py:147
  52.9 15.4 %collective-permute-start.4 = (bf16[256,256]{1,0:T(8,128)(2,1)S(1)}, bf16[256,256]{1,0:T(8,128)(2,1)S(1)}, u32[]{:S(2)}, u32[]{:S(2)}) collective-permute-start(bf16[256,256]{1,0:T(8,128)(2,1)S(1)} %copy-done.1), channel_id=1, source_target_pairs={{0,6},{2,8},{4,10},{6,12},{8,14},{10,0},{12,2},{14,4},{1,7},{3,9},... | collective-permute-start | bytes 393224 | tf_op jit(solution)/shard_map/ppermute | solution.py:147
  53.0 20.4 %collective-permute-start.5 = (bf16[256,256]{1,0:T(8,128)(2,1)S(1)}, bf16[256,256]{1,0:T(8,128)(2,1)S(1)}, u32[]{:S(2)}, u32[]{:S(2)}) collective-permute-start(bf16[256,256]{1,0:T(8,128)(2,1)S(1)} %copy-done.1), channel_id=1, source_target_pairs={{0,10},{2,12},{4,14},{6,0},{8,2},{10,4},{12,6},{14,8},{1,11},{3,13... | collective-permute-start | bytes 393224 | tf_op jit(solution)/shard_map/ppermute | solution.py:147
  58.0 20.0 %collective-permute-start.6 = (bf16[256,256]{1,0:T(8,128)(2,1)S(1)}, bf16[256,256]{1,0:T(8,128)(2,1)S(1)}, u32[]{:S(2)}, u32[]{:S(2)}) collective-permute-start(bf16[256,256]{1,0:T(8,128)(2,1)S(1)} %copy-done.1), channel_id=1, source_target_pairs={{0,8},{2,10},{4,12},{6,14},{8,0},{10,2},{12,4},{14,6},{1,9},{3,11}... | collective-permute-start | bytes 393224 | tf_op jit(solution)/shard_map/ppermute | solution.py:147
  66.7 11.4 %copy-start.21 = (bf16[256,256]{1,0:T(8,128)(2,1)}, bf16[256,256]{1,0:T(8,128)(2,1)S(1)}, u32[]{:S(2)}) copy-start(bf16[256,256]{1,0:T(8,128)(2,1)S(1)} %collective-permute-done.3.refs_0_) | copy-start | bytes 393220
  68.3 9.7 %copy-start.22 = (bf16[256,256]{1,0:T(8,128)(2,1)}, bf16[256,256]{1,0:T(8,128)(2,1)S(1)}, u32[]{:S(2)}) copy-start(bf16[256,256]{1,0:T(8,128)(2,1)S(1)} %collective-permute-done.4.refs_1_) | copy-start | bytes 393220
  73.4 4.7 %copy-start.23 = (bf16[256,256]{1,0:T(8,128)(2,1)}, bf16[256,256]{1,0:T(8,128)(2,1)S(1)}, u32[]{:S(2)}) copy-start(bf16[256,256]{1,0:T(8,128)(2,1)S(1)} %collective-permute-done.5.refs_2_) | copy-start | bytes 393220
  78.1 0.7 copy-start.25
  82.2 7.3 %copy-start.2 = (bf16[16,64,1024]{2,1,0:T(8,128)(2,1)}, bf16[16,64,1024]{2,1,0:T(8,128)(2,1)S(1)}, u32[]{:S(2)}) copy-start(bf16[16,64,1024]{2,1,0:T(8,128)(2,1)S(1)} %all-to-all-done.1) | copy-start | bytes 6291460
  82.2 30.1 %copy-start.29 = (s32[8]{0:T(128)S(1)}, s32[8]{0:T(128)}, u32[]{:S(2)}) copy-start(s32[8]{0:T(128)} %constant.35) | copy-start | bytes 100
  82.2 30.1 %all-to-all-start.2 = ((bf16[16,64,1024]{2,1,0:T(8,128)(2,1)}), bf16[16,64,1024]{2,1,0:T(8,128)(2,1)}, u32[]{:S(2)}, u32[]{:S(2)}) async-start(bf16[16,64,1024]{2,1,0:T(8,128)(2,1)} %bitcast.34), calls=%async_computation.2 | async-start | bytes 4194304 | tf_op jit(solution)/shard_map/all_to_all | solution.py:212
  89.4 116.1 %reduce-scatter.2.cloned.1.call-start = ((), (), s32[]{:S(2)}) async-start(), calls=%async_computation.7 | async-start | bytes 8912896 | tf_op jit(solution)/shard_map/reduce_scatter | solution.py:245
  89.5 23.4 %collective-permute-start.7 = (bf16[1024,1024]{1,0:T(8,128)(2,1)S(1)}, bf16[1024,1024]{1,0:T(8,128)(2,1)}, u32[]{:S(2)}, u32[]{:S(2)}) collective-permute-start(bf16[1024,1024]{1,0:T(8,128)(2,1)S(1)} %bitcast.30), channel_id=1, source_target_pairs={{0,1},{1,0},{2,3},{3,2},{4,5},{5,4},{6,7},{7,6},{8,9},{9,8},{10,11... | collective-permute-start | bytes 6291464 | tf_op jit(solution)/shard_map/ppermute | solution.py:215
  112.2 4.5 %collective-permute-start.8 = (bf16[1024,1024]{1,0:T(8,128)(2,1)}, bf16[1024,1024]{1,0:T(8,128)(2,1)}, u32[]{:S(2)}, u32[]{:S(2)}) collective-permute-start(bf16[1024,1024]{1,0:T(8,128)(2,1)} %bitcast.7.mh_ref), channel_id=1, source_target_pairs={{0,1},{1,0},{2,3},{3,2},{4,5},{5,4},{6,7},{7,6},{8,9},{9,8},{10,11... | collective-permute-start | bytes 6291464 | tf_op jit(solution)/shard_map/ppermute | solution.py:215
  131.2 81.5 %copy-start.19 = (bf16[128,256]{1,0:T(8,128)(2,1)S(1)}, bf16[128,256]{1,0:T(8,128)(2,1)}, u32[]{:S(2)}) copy-start(bf16[128,256]{1,0:T(8,128)(2,1)} %param.15) | copy-start | bytes 196612
  131.2 81.7 %copy-start.18 = (bf16[128,256]{1,0:T(8,128)(2,1)S(1)}, bf16[128,256]{1,0:T(8,128)(2,1)}, u32[]{:S(2)}) copy-start(bf16[128,256]{1,0:T(8,128)(2,1)} %param.14) | copy-start | bytes 196612
  131.2 89.3 %copy-start = (bf16[1024,256]{1,0:T(8,128)(2,1)S(1)}, bf16[1024,256]{1,0:T(8,128)(2,1)}, u32[]{:S(2)}) copy-start(bf16[1024,256]{1,0:T(8,128)(2,1)} %get-tuple-element.23.pick_ref) | copy-start | bytes 1572868
  150.6 78.8 %copy-start.28 = (f32[3,128]{1,0:T(4,128)S(1)}, f32[3,128]{1,0:T(4,128)}, u32[]{:S(2)}) copy-start(f32[3,128]{1,0:T(4,128)} %param.16) | copy-start | bytes 4612
  150.6 98.0 %copy-start.20 = (bf16[128,256]{1,0:T(8,128)(2,1)S(1)}, bf16[128,256]{1,0:T(8,128)(2,1)}, u32[]{:S(2)}) copy-start(bf16[128,256]{1,0:T(8,128)(2,1)} %outer_ref.1) | copy-start | bytes 196612
  205.5 15.0 %all-to-all-start.3 = ((bf16[16,64,256]{2,1,0:T(8,128)(2,1)}), bf16[16,64,256]{2,1,0:T(8,128)(2,1)S(1)}, u32[]{:S(2)}, u32[]{:S(2)}) async-start(bf16[16,64,256]{2,1,0:T(8,128)(2,1)} %bitcast.39), calls=%async_computation.4 | async-start | bytes 1048576 | tf_op jit(solution)/shard_map/all_to_all | solution.py:275
  213.2 15.7 %collective-permute-start.9 = (bf16[2,128,2]{2,1,0:T(8,128)(2,1)S(1)}, bf16[2,128,2]{2,1,0:T(8,128)(2,1)S(1)}, u32[]{:S(2)}, u32[]{:S(2)}) collective-permute-start(bf16[2,128,2]{2,1,0:T(8,128)(2,1)S(1)} %copy.23), channel_id=1, source_target_pairs={{0,16},{16,32},{32,48},{48,64},{64,80},{80,96},{96,112},{112,128},... | collective-permute-start | bytes 3080 | tf_op jit(solution)/shard_map/ppermute | solution.py:154
  221.5 7.9 %collective-permute-start.10 = (bf16[256,256]{1,0:T(8,128)(2,1)}, bf16[256,256]{1,0:T(8,128)(2,1)S(1)}, u32[]{:S(2)}, u32[]{:S(2)}) collective-permute-start(bf16[256,256]{1,0:T(8,128)(2,1)} %combine.1.refs_0_), channel_id=1, source_target_pairs={{0,2},{2,4},{4,6},{6,8},{8,10},{10,12},{12,14},{14,0},{1,3},{3,5},... | collective-permute-start | bytes 393224 | tf_op jit(solution)/shard_map/ppermute | solution.py:147
  221.5 12.5 %collective-permute-start.11 = (bf16[256,256]{1,0:T(8,128)(2,1)}, bf16[256,256]{1,0:T(8,128)(2,1)S(1)}, u32[]{:S(2)}, u32[]{:S(2)}) collective-permute-start(bf16[256,256]{1,0:T(8,128)(2,1)} %combine.1.refs_0_), channel_id=1, source_target_pairs={{0,14},{2,0},{4,2},{6,4},{8,6},{10,8},{12,10},{14,12},{1,15},{3,1}... | collective-permute-start | bytes 393224 | tf_op jit(solution)/shard_map/ppermute | solution.py:147
  224.8 13.6 %collective-permute-start.12 = (bf16[256,256]{1,0:T(8,128)(2,1)}, bf16[256,256]{1,0:T(8,128)(2,1)S(1)}, u32[]{:S(2)}, u32[]{:S(2)}) collective-permute-start(bf16[256,256]{1,0:T(8,128)(2,1)} %combine.1.refs_0_), channel_id=1, source_target_pairs={{0,4},{2,6},{4,8},{6,10},{8,12},{10,14},{12,0},{14,2},{1,5},{3,7},... | collective-permute-start | bytes 393224 | tf_op jit(solution)/shard_map/ppermute | solution.py:147
  224.8 13.6 %collective-permute-start.13 = (bf16[256,256]{1,0:T(8,128)(2,1)}, bf16[256,256]{1,0:T(8,128)(2,1)S(1)}, u32[]{:S(2)}, u32[]{:S(2)}) collective-permute-start(bf16[256,256]{1,0:T(8,128)(2,1)} %combine.1.refs_0_), channel_id=1, source_target_pairs={{0,12},{2,14},{4,0},{6,2},{8,4},{10,6},{12,8},{14,10},{1,13},{3,15... | collective-permute-start | bytes 393224 | tf_op jit(solution)/shard_map/ppermute | solution.py:147
  228.9 17.0 %collective-permute-start.14 = (bf16[256,256]{1,0:T(8,128)(2,1)}, bf16[256,256]{1,0:T(8,128)(2,1)S(1)}, u32[]{:S(2)}, u32[]{:S(2)}) collective-permute-start(bf16[256,256]{1,0:T(8,128)(2,1)} %combine.1.refs_0_), channel_id=1, source_target_pairs={{0,6},{2,8},{4,10},{6,12},{8,14},{10,0},{12,2},{14,4},{1,7},{3,9},... | collective-permute-start | bytes 393224 | tf_op jit(solution)/shard_map/ppermute | solution.py:147
  229.4 20.3 %copy-start.3 = (bf16[256,256]{1,0:T(8,128)(2,1)}, bf16[256,256]{1,0:T(8,128)(2,1)S(1)}, u32[]{:S(2)}) copy-start(bf16[256,256]{1,0:T(8,128)(2,1)S(1)} %collective-permute-done.10.refs_1_) | copy-start | bytes 393220
  229.4 17.9 %collective-permute-start.15 = (bf16[256,256]{1,0:T(8,128)(2,1)}, bf16[256,256]{1,0:T(8,128)(2,1)S(1)}, u32[]{:S(2)}, u32[]{:S(2)}) collective-permute-start(bf16[256,256]{1,0:T(8,128)(2,1)} %combine.1.refs_0_), channel_id=1, source_target_pairs={{0,10},{2,12},{4,14},{6,0},{8,2},{10,4},{12,6},{14,8},{1,11},{3,13... | collective-permute-start | bytes 393224 | tf_op jit(solution)/shard_map/ppermute | solution.py:147
  234.0 15.6 %copy-start.4 = (bf16[256,256]{1,0:T(8,128)(2,1)}, bf16[256,256]{1,0:T(8,128)(2,1)S(1)}, u32[]{:S(2)}) copy-start(bf16[256,256]{1,0:T(8,128)(2,1)S(1)} %collective-permute-done.11.refs_2_) | copy-start | bytes 393220
  234.0 13.2 %collective-permute-start.16 = (bf16[256,256]{1,0:T(8,128)(2,1)}, bf16[256,256]{1,0:T(8,128)(2,1)S(1)}, u32[]{:S(2)}, u32[]{:S(2)}) collective-permute-start(bf16[256,256]{1,0:T(8,128)(2,1)} %combine.1.refs_0_), channel_id=1, source_target_pairs={{0,8},{2,10},{4,12},{6,14},{8,0},{10,2},{12,4},{14,6},{1,9},{3,11}... | collective-permute-start | bytes 393224 | tf_op jit(solution)/shard_map/ppermute | solution.py:147
  238.4 11.3 %copy-start.5 = (bf16[256,256]{1,0:T(8,128)(2,1)}, bf16[256,256]{1,0:T(8,128)(2,1)S(1)}, u32[]{:S(2)}) copy-start(bf16[256,256]{1,0:T(8,128)(2,1)S(1)} %collective-permute-done.12.refs_3_) | copy-start | bytes 393220
  238.4 9.4 %collective-permute-start.17 = (bf16[256,256]{1,0:T(8,128)(2,1)}, bf16[256,256]{1,0:T(8,128)(2,1)S(1)}, u32[]{:S(2)}, u32[]{:S(2)}) collective-permute-start(bf16[256,256]{1,0:T(8,128)(2,1)} %combine.1.refs_0_), channel_id=1, source_target_pairs={{0,1},{1,0},{2,3},{3,2},{4,5},{5,4},{6,7},{7,6},{8,9},{9,8},{10,11... | collective-permute-start | bytes 393224 | tf_op jit(solution)/shard_map/ppermute | solution.py:286
  238.4 11.2 %copy-start.6 = (bf16[256,256]{1,0:T(8,128)(2,1)}, bf16[256,256]{1,0:T(8,128)(2,1)S(1)}, u32[]{:S(2)}) copy-start(bf16[256,256]{1,0:T(8,128)(2,1)S(1)} %collective-permute-done.13.refs_4_) | copy-start | bytes 393220
  238.4 9.7 %collective-permute-start.18 = (bf16[256,256]{1,0:T(8,128)(2,1)S(1)}, bf16[256,256]{1,0:T(8,128)(2,1)S(1)}, u32[]{:S(2)}, u32[]{:S(2)}) collective-permute-start(bf16[256,256]{1,0:T(8,128)(2,1)S(1)} %collective-permute-done.10.refs_1_), channel_id=1, source_target_pairs={{0,1},{1,0},{2,3},{3,2},{4,5},{5,4},{6,7},{7,6},{8,9},{9,8},{10,11... | collective-permute-start | bytes 393224 | tf_op jit(solution)/shard_map/ppermute | solution.py:286
  245.9 3.8 %copy-start.7 = (bf16[256,256]{1,0:T(8,128)(2,1)}, bf16[256,256]{1,0:T(8,128)(2,1)S(1)}, u32[]{:S(2)}) copy-start(bf16[256,256]{1,0:T(8,128)(2,1)S(1)} %collective-permute-done.14.refs_5_) | copy-start | bytes 393220
  245.9 2.4 collective-permute-start.19
  247.3 2.4 copy-start.8
  247.3 2.2 collective-permute-start.20
  247.3 2.4 copy-start.9
  247.3 2.2 collective-permute-start.21
  247.8 1.9 copy-start.10
  247.8 1.7 collective-permute-start.22
  248.1 1.6 copy-start.11
  248.1 1.4 collective-permute-start.23
  248.3 1.4 copy-start.12
  248.3 1.3 collective-permute-start.24
  249.5 0.6 copy-start.13
  249.5 0.7 copy-start.14
  249.5 0.7 copy-start.15
  249.5 0.7 copy-start.16
  249.7 0.7 copy-start.17
  253.4 23.6 %all-to-all-start.4 = ((bf16[16,128,256]{2,1,0:T(8,128)(2,1)}), bf16[16,128,256]{2,1,0:T(8,128)(2,1)S(1)}, u32[]{:S(2)}, u32[]{:S(2)}) async-start(bf16[16,128,256]{2,1,0:T(8,128)(2,1)} %proj.1), calls=%async_computation.5 | async-start | bytes 2097152 | tf_op jit(solution)/shard_map/all_to_all | solution.py:314
  263.7 11.0 %collective-permute-start.25 = (f32[128,2]{1,0:T(8,128)S(1)}, f32[128,2]{1,0:T(8,128)S(1)}, u32[]{:S(2)}, u32[]{:S(2)}) collective-permute-start(f32[128,2]{1,0:T(8,128)S(1)} %slice.52), channel_id=1, source_target_pairs={{16,0},{32,16},{48,32},{64,48},{80,64},{96,80},{112,96},{128,112},... | collective-permute-start | bytes 3080 | tf_op jit(solution)/shard_map/ppermute | solution.py:154
Sparse Core Ops, SparseCore 0:
  26.3 74.6 all-gather.1
  131.3 74.1 reduce-scatter.1

commit v5 on v4

--- a/solution.py
+++ b/solution.py
@@ -34,7 +34,9 @@
     return pl.CostEstimate(flops=int(flops), bytes_accessed=int(nbytes), transcendentals=0)
 
 
-def route_kernel(experts, cap, ids_ref, wts_ref, state_ref, sent_ref, pick_ref, scale_ref):
+def route_kernel(
+    experts, cap, early, ids_ref, wts_ref, state_ref, cot_ref, sent_ref, pick_ref, late_ref, scale_ref
+):
     tokens = ids_ref.shape[1]
     first, second = ids_ref[0:1, :], ids_ref[1:2, :]
     expert = lax.broadcasted_iota(jnp.int32, (experts, tokens), 0)
@@ -47,12 +49,25 @@
     slot = jnp.where(named, earlier.astype(jnp.int32), -1)
     weight = jnp.where(is_first, wts_ref[0:1, :], jnp.where(is_second, wts_ref[1:2, :], 0.0))
     place = lax.broadcasted_iota(jnp.int32, (cap, tokens), 0)
+    hits, scales = [], []
     for e in range(experts):
         hit = slot[e : e + 1, :] == place
-        pick_ref[e * cap : (e + 1) * cap, :] = hit.astype(F32).astype(BF16)
-        taken = jnp.sum(jnp.where(hit, weight[e : e + 1, :], 0.0), axis=1, keepdims=True)
-        scale_ref[e * cap : (e + 1) * cap, :] = jnp.broadcast_to(taken, (cap, 128))
-    sent_ref[...] = dot_nn(pick_ref[...], state_ref[...]).astype(BF16)
+        hits.append(hit.astype(F32))
+        scales.append(jnp.sum(jnp.where(hit, weight[e : e + 1, :], 0.0), axis=1, keepdims=True))
+    pick = jnp.concatenate(hits, axis=0).astype(BF16)
+    pick_ref[...] = pick
+    late_ref[...] = jnp.concatenate([hit[early:] for hit in hits], axis=0).astype(BF16)
+    late_scale = jnp.concatenate([taken[early:] for taken in scales], axis=0)
+    scale_ref[...] = jnp.broadcast_to(late_scale, scale_ref.shape)
+    state_rows = dot_nn(pick, state_ref[...])
+    soon = jnp.concatenate([hit[:early] for hit in hits], axis=0).astype(BF16)
+    soon_rows = dot_nn(soon, cot_ref[...]) * jnp.concatenate(
+        [taken[:early] for taken in scales], axis=0
+    )
+    both = []
+    for e in range(experts):
+        both += [state_rows[e * cap : (e + 1) * cap], soon_rows[e * early : (e + 1) * early]]
+    sent_ref[...] = jnp.concatenate(both, axis=0).astype(BF16)
 
 
 def spread_kernel(pick_ref, scale_ref, *refs):
@@ -64,8 +79,33 @@
         out_ref[:, j * width : (j + 1) * width] = rows
 
 
+def down_columns(slab_ref, base, wd_ref, count, width):
+    pieces = [
+        wd_ref[:, pl.ds(pl.multiple_of(slab_ref[base + j] * width, width), width)]
+        for j in range(count)
+    ]
+    return jnp.concatenate(pieces, axis=1)
+
+
 def expert_kernel(
-    slab_ref, state_ref, ml_ref, mh_ref, tl_ref, th_ref, wg_ref, wu_ref, wd_ref, part_ref, act_ref, wgu_ref
+    cap,
+    early,
+    slab_ref,
+    state_ref,
+    early_ref,
+    ml_ref,
+    mh_ref,
+    tl_ref,
+    th_ref,
+    wg_ref,
+    wu_ref,
+    wd_ref,
+    part_ref,
+    act_ref,
+    soon_ref,
+    late_ref,
+    wgu_ref,
+    soon_back_ref,
 ):
     slabs, width = state_ref.shape[0], state_ref.shape[2]
     hidden_n = wd_ref.shape[0]
@@ -74,41 +114,74 @@
     def _():
         wgu_ref[:hidden_n] = wg_ref[...]
         wgu_ref[hidden_n:] = wu_ref[...]
+        soon = jnp.concatenate([early_ref[s] for s in range(slabs)], axis=1)
+        soon_back_ref[...] = dot_nt(soon, wd_ref[...])
 
     rows = jnp.concatenate([state_ref[s] for s in range(slabs)], axis=1)
     pre = dot_nt(rows, wgu_ref[...])
     gate_pre, up_pre = pre[:, :hidden_n], pre[:, hidden_n:]
-    back_hidden = jnp.zeros(gate_pre.shape, F32)
     per = ml_ref.shape[1] // width
+    late = jnp.zeros((ml_ref.shape[0], hidden_n), F32)
     for q, ref in enumerate((ml_ref, mh_ref, tl_ref, th_ref)):
-        pieces = [
-            wd_ref[:, pl.ds(pl.multiple_of(slab_ref[q * per + j] * width, width), width)]
-            for j in range(per)
-        ]
-        back_hidden = back_hidden + dot_nt(ref[...], jnp.concatenate(pieces, axis=1))
+        late = late + dot_nt(ref[...], down_columns(slab_ref, q * per, wd_ref, per, width))
+    late_n = cap - early
+    groups = range(rows.shape[0] // cap)
+    few = len(groups) * early
+    soon_back = soon_back_ref[pl.ds(pl.multiple_of(pl.program_id(0) * few, few), few), :]
+    back_hidden = jnp.concatenate(
+        [
+            x
+            for i in groups
+            for x in (
+                soon_back[i * early : (i + 1) * early],
+                late[i * late_n : (i + 1) * late_n],
+            )
+        ],
+        axis=0,
+    )
     sig_gate = jax.nn.sigmoid(gate_pre)
     silu_gate = gate_pre * sig_gate
-    hidden = (silu_gate * up_pre).astype(BF16)
+    hidden = silu_gate * up_pre
     back_gate = (back_hidden * up_pre * sig_gate * (1.0 + gate_pre * (1.0 - sig_gate))).astype(BF16)
     back_up = (back_hidden * silu_gate).astype(BF16)
     back = jnp.concatenate([back_gate, back_up], axis=1)
-    act_ref[:, : 2 * hidden_n] = back
-    act_ref[:, 2 * hidden_n :] = hidden
+    act_ref[...] = back
+    soon_ref[...] = jnp.concatenate(
+        [hidden[i * cap : i * cap + early] for i in groups], axis=0
+    ).astype(BF16)
+    late_ref[...] = jnp.concatenate(
+        [hidden[i * cap + early : (i + 1) * cap] for i in groups], axis=0
+    ).astype(BF16)
     for s in range(slabs):
         part_ref[s] = dot_nn(back, wgu_ref[:, s * width : (s + 1) * width]).astype(BF16)
 
 
-def weight_grad_kernel(slab_ref, act_ref, state_ref, ml_ref, mh_ref, tl_ref, th_ref, gg_ref, gu_ref, gd_ref):
+def weight_grad_kernel(
+    slab_ref,
+    act_ref,
+    soon_ref,
+    late_ref,
+    state_ref,
+    early_ref,
+    ml_ref,
+    mh_ref,
+    tl_ref,
+    th_ref,
+    gg_ref,
+    gu_ref,
+    gd_ref,
+):
     hidden_n = gg_ref.shape[0]
     step, per = pl.program_id(0), pl.num_programs(0) // 4
-    both = dot_tn(act_ref[:, : 2 * hidden_n], state_ref[0])
+    both = dot_tn(act_ref[...], state_ref[0])
     gg_ref[...] = both[:hidden_n]
     gu_ref[...] = both[hidden_n:]
+    soon = dot_tn(soon_ref[...], early_ref[0])
     for q, ref in enumerate((ml_ref, mh_ref, tl_ref, th_ref)):
 
         @pl.when(step // per == q)
         def _(ref=ref):
-            gd_ref[...] = dot_tn(act_ref[:, 2 * hidden_n :], ref[...])
+            gd_ref[...] = soon + dot_tn(late_ref[...], ref[...])
 
 
 def combine_kernel(pick_ref, rows_ref, cot_ref, out_ref):
@@ -183,20 +256,31 @@
 
     cot_pieces = gathered(cotangent, "z")
 
-    sent_state, pick, scale = pl.pallas_call(
-        functools.partial(route_kernel, experts, cap),
+    early = cap // 8
+    late_n = cap - early
+    own, late_rows, soon_rows = experts * (cap + early), experts * late_n, experts * early
+    sent_rows, pick, late_pick, late_scale = pl.pallas_call(
+        functools.partial(route_kernel, experts, cap, early),
         out_shape=(
-            shape((slots, width), BF16),
+            shape((own, width), BF16),
             shape((slots, tok_count), BF16),
-            shape((slots, 128), F32),
+            shape((late_rows, tok_count), BF16),
+            shape((late_rows, 128), F32),
         ),
         cost_estimate=cost(2 * slots * tok_count * width, 4 * slots * width),
         name="route",
-    )(route_ids.T, route_weights.T, mixed_state)
-    recv_state = lax.all_to_all(
-        sent_state.reshape(experts, cap, width), "sp", split_axis=0, concat_axis=0, tiled=True
-    )
-    state_all = lax.all_gather(recv_state.reshape(slots, width), TP, axis=0, tiled=False)
+    )(route_ids.T, route_weights.T, mixed_state, cotangent)
+    recv_rows = lax.all_to_all(
+        sent_rows.reshape(experts, cap + early, width), "sp", split_axis=0, concat_axis=0, tiled=True
+    )
+    ordered = jnp.concatenate(
+        [
+            recv_rows[:, :cap].reshape(slots, width),
+            recv_rows[:, cap:].reshape(soon_rows, width),
+        ],
+        axis=0,
+    )
+    state_all = lax.all_gather(ordered, TP, axis=0, tiled=False)
 
     half = z_size // 2 * width
     swap = [(0, 1), (1, 0)]
@@ -204,43 +288,56 @@
     def spread(pieces):
         return pl.pallas_call(
             spread_kernel,
-            out_shape=shape((slots, half), BF16),
-            cost_estimate=cost(2 * slots * tok_count * half, 4 * slots * half),
-        )(pick, scale, *pieces)
+            out_shape=shape((late_rows, half), BF16),
+            cost_estimate=cost(2 * late_rows * tok_count * half, 4 * late_rows * half),
+        )(late_pick, late_scale, *pieces)
 
     def exchanged(part):
         got = lax.all_to_all(
-            part.reshape(experts, cap, half), "sp", split_axis=0, concat_axis=0, tiled=True
-        ).reshape(slots, half)
+            part.reshape(experts, late_n, half), "sp", split_axis=0, concat_axis=0, tiled=True
+        ).reshape(late_rows, half)
         return got, lax.ppermute(got, "c", swap)
 
     my_low, their_low = exchanged(spread(cot_pieces[: z_size // 2]))
     my_high, their_high = exchanged(spread(cot_pieces[z_size // 2 :]))
     cots = (my_low, my_high, their_low, their_high)
 
-    block = 256
+    steps = 4
+    block = slots // steps
     whole = lambda *dims: pl.BlockSpec(dims, lambda *_: (0,) * len(dims))
-    cot_rows = pl.BlockSpec((block, half), lambda r, core: (r, 0))
-    partial_value, acts = pl.pallas_call(
-        expert_kernel,
+    by_rows = lambda *dims: pl.BlockSpec(dims, lambda r, slab: (r, 0))
+    partial_value, acts, soon_acts, late_acts = pl.pallas_call(
+        functools.partial(expert_kernel, cap, early),
         grid_spec=pltpu.PrefetchScalarGridSpec(
             num_scalar_prefetch=1,
-            grid=(slots // block,),
+            grid=(steps,),
             in_specs=[
-                pl.BlockSpec((slabs, block, width), lambda r, core: (0, r, 0)),
-                *[cot_rows] * 4,
+                pl.BlockSpec((slabs, block, width), lambda r, slab: (0, r, 0)),
+                pl.BlockSpec((slabs, soon_rows, width), lambda r, slab: (0, slots // soon_rows, 0)),
+                *[by_rows(late_rows // steps, half)] * 4,
                 *[whole(hidden_n, features)] * 3,
             ],
             out_specs=[
-                pl.BlockSpec((slabs, block, width), lambda r, core: (0, r, 0)),
-                pl.BlockSpec((block, 3 * hidden_n), lambda r, core: (r, 0)),
+                pl.BlockSpec((slabs, block, width), lambda r, slab: (0, r, 0)),
+                by_rows(block, 2 * hidden_n),
+                by_rows(soon_rows // steps, hidden_n),
+                by_rows(late_rows // steps, hidden_n),
             ],
-            scratch_shapes=[pltpu.VMEM((2 * hidden_n, features), BF16)],
-        ),
-        out_shape=(shape((slabs, slots, width), BF16), shape((slots, 3 * hidden_n), BF16)),
+            scratch_shapes=[
+                pltpu.VMEM((2 * hidden_n, features), BF16),
+                pltpu.VMEM((soon_rows, hidden_n), F32),
+            ],
+        ),
+        out_shape=(
+            shape((slabs, slots, width), BF16),
+            shape((slots, 2 * hidden_n), BF16),
+            shape((soon_rows, hidden_n), BF16),
+            shape((late_rows, hidden_n), BF16),
+        ),
         cost_estimate=cost(10 * slots * hidden_n * features, 6 * slots * features),
         name="expert",
-    )(slab_of, state_all, *cots, w_gate[0], w_up[0], w_down[0])
+        compiler_params=grant(50),
+    )(slab_of, state_all, state_all, *cots, w_gate[0], w_up[0], w_down[0])
 
     row_back = lax.psum_scatter(partial_value, TP, scatter_dimension=0, tiled=False)
 
@@ -248,7 +345,7 @@
 
     def cot_piece(q):
         return pl.BlockSpec(
-            (slots, width), lambda s, core: (0, jnp.clip(s - q * quarter, 0, quarter - 1))
+            (late_rows, width), lambda s, slab: (0, jnp.clip(s - q * quarter, 0, quarter - 1))
         )
 
     grad_out = pl.BlockSpec((hidden_n, width), lambda s, slab: (0, slab[s]))
@@ -258,8 +355,11 @@
             num_scalar_prefetch=1,
             grid=(slabs,),
             in_specs=[
-                whole(slots, 3 * hidden_n),
+                whole(slots, 2 * hidden_n),
+                whole(soon_rows, hidden_n),
+                whole(late_rows, hidden_n),
                 pl.BlockSpec((1, slots, width), lambda s, slab: (slab[s], 0, 0)),
+                pl.BlockSpec((1, soon_rows, width), lambda s, slab: (slab[s], slots // soon_rows, 0)),
                 *[cot_piece(q) for q in range(4)],
             ],
             out_specs=[grad_out] * 3,
@@ -267,7 +367,7 @@
         out_shape=(shape((hidden_n, features), F32),) * 3,
         cost_estimate=cost(6 * slots * hidden_n * features, 6 * slots * features),
         name="weight_grads",
-    )(slab_of, acts, state_all, *cots)
+    )(slab_of, acts, soon_acts, late_acts, state_all, state_all, *cots)
     row_back, grad_gate, grad_up, grad_down = lax.optimization_barrier(
         (row_back, grad_gate, grad_up, grad_down)
     )

time: 290 us -> 291 us (level)
  local copies, waits for them, and re-layouts: 4.25 us -> 7.68 us
  waiting for transfers between devices: 123 us -> 120 us
    unnamed x63 -> x79, local copies, waits for them, and re-layouts: 3.06 us -> 6.45 us
    all_to_all x2, waiting for transfers between devices: 22.7 us -> 19.7 us  [exchanged(): lax.all_to_all(part.reshape(experts, late_n, half), 'sp', split_axis=0, c...]
where the time goes in v5:
time: 291 us; the launch traced here: 286 us
  waiting for transfers between devices  120 us (41%)
  starting transfers between devices  70.6 us (24%)
  Pallas kernels  50.1 us (17%)
  blocking collectives  17.5 us (6%)
  between operations  14.4 us (5%)
  local copies, waits for them, and re-layouts  7.68 us (3%)
  other arithmetic  5.12 us (2%)
    reduce_scatter x1, waiting for transfers between devices, shards(): lax.psum_scatter(partial_value, TP, scatter_dimension=0, tiled=False)  54.8 us
    ppermute x14, starting transfers between devices, gathered(): lax.ppermute(value, axis, [(i, (i + k) % size) for i in range(size)])  33.8 us
    ppermute x14, waiting for transfers between devices, gathered(): lax.ppermute(value, axis, [(i, (i + k) % size) for i in range(size)])  32.6 us
    all_to_all x2, waiting for transfers between devices, exchanged(): lax.all_to_all(part.reshape(experts, late_n, half), 'sp', split_axis=0, c...  19.7 us
    pallas_call x1, Pallas kernels, shards(): pl.pallas_call(weight_grad_kernel, grid_spec=pltpu.PrefetchScalarGridSpec...  19.4 us
    all_to_all x1, blocking collectives, shards(): lax.all_to_all(sent_rows.reshape(experts, cap + early, width), 'sp', spli...  17.5 us
    pallas_call x1, Pallas kernels, shards(): pl.pallas_call(functools.partial(expert_kernel, cap, early), grid_spec=pl...  13.9 us
    all_to_all x2, starting transfers between devices, exchanged(): lax.all_to_all(part.reshape(experts, late_n, half), 'sp', split_axis=0, c...  13.4 us
  transfers between devices with their start and end apart: 32, of which 14 were waited for; matrix products, arithmetic and copies ran while one was open for 2% of the time, Pallas kernels for 11%

profile of v5, /device:TPU:24, one launch (start us, length us, event | category | flops | bytes accessed | tf_op | source)
XLA Modules:
  0.0 285.8 jit_solution(5215415478764157131)
XLA Ops:
  7.2 2.7 route.1
  9.9 17.5 %all_to_all.25 = bf16[16,72,256]{2,1,0:T(8,128)(2,1)S(1)} all-to-all(bf16[16,72,256]{2,1,0:T(8,128)(2,1)} %bitcast.46), channel_id=1, replica_groups=mesh['sp'=16,'z'=8,'c'=2] {'sp'}, dimensions={0} | all-to-all | bytes 1179648 | tf_op jit(solution)/shard_map/all_to_all | solution.py:273
  27.5 0.9 pad_maximum_fusion
  28.4 2.0 collective-permute-start
  30.4 4.0 %collective-permute-start.1 = (bf16[256,256]{1,0:T(8,128)(2,1)S(1)}, bf16[256,256]{1,0:T(8,128)(2,1)S(1)}, u32[]{:S(2)}, u32[]{:S(2)}) collective-permute-start(bf16[256,256]{1,0:T(8,128)(2,1)S(1)} %copy-done.4), channel_id=1, source_target_pairs={{0,14},{2,0},{4,2},{6,4},{8,6},{10,8},{12,10},{14,12},{1,15},{3,1}... | collective-permute-start | bytes 393224 | tf_op jit(solution)/shard_map/ppermute | solution.py:220
  34.4 3.8 %collective-permute-done.refs_1_ = bf16[256,256]{1,0:T(8,128)(2,1)S(1)} collective-permute-done((bf16[256,256]{1,0:T(8,128)(2,1)S(1)}, bf16[256,256]{1,0:T(8,128)(2,1)S(1)}, u32[]{:S(2)}, u32[]{:S(2)}) %collective-permute-start) | collective-permute-done | bytes 131104 | tf_op jit(solution)/shard_map/ppermute | solution.py:220
  38.3 5.1 %collective-permute-done.2.refs_3_ = bf16[256,256]{1,0:T(8,128)(2,1)S(1)} collective-permute-done((bf16[256,256]{1,0:T(8,128)(2,1)S(1)}, bf16[256,256]{1,0:T(8,128)(2,1)S(1)}, u32[]{:S(2)}, u32[]{:S(2)}) %collective-permute-start.2) | collective-permute-done | bytes 131104 | tf_op jit(solution)/shard_map/ppermute | solution.py:220
  43.4 0.6 copy-done.35
  44.1 3.2 %shard_map.188 = bf16[896,1024]{1,0:T(8,128)(2,1)} custom-call(bf16[896,256]{1,0:T(8,128)(2,1)} %get-tuple-element.26.pick_ref, f32[896,128]{1,0:T(8,128)} %get-tuple-element.27.scale_ref, bf16[256,256]{1,0:T(8,128)(2,1)} %cot_ref.3, bf16[256,256]{1,0:T(8,128)(2,1)} %copy-done.32, bf16[256,256]{1,0:T(8,128)(2,1)} %copy-done.34, bf16[256,256]{1,0:T(8,128)(2,1)} %copy-done.35), custom_call_target="tpu_custom_call" | custom-call | flops 469762048 | bytes 3670016 | tf_op jit(solution)/shard_map/pallas_call | solution.py:289
  47.3 5.9 %all-to-all-start.1 = ((bf16[16,56,1024]{2,1,0:T(8,128)(2,1)}), bf16[16,56,1024]{2,1,0:T(8,128)(2,1)S(1)}, u32[]{:S(2)}, u32[]{:S(2)}) async-start(bf16[16,56,1024]{2,1,0:T(8,128)(2,1)} %bitcast.43), calls=%async_computation.1 | async-start | bytes 3670016 | tf_op jit(solution)/shard_map/all_to_all | solution.py:296
  53.2 0.6 collective-permute-start.3
  53.8 0.2 collective-permute-start.4
  54.0 4.8 %collective-permute-start.5 = (bf16[256,256]{1,0:T(8,128)(2,1)S(1)}, bf16[256,256]{1,0:T(8,128)(2,1)S(1)}, u32[]{:S(2)}, u32[]{:S(2)}) collective-permute-start(bf16[256,256]{1,0:T(8,128)(2,1)S(1)} %copy-done.5), channel_id=1, source_target_pairs={{0,10},{2,12},{4,14},{6,0},{8,2},{10,4},{12,6},{14,8},{1,11},{3,13... | collective-permute-start | bytes 393224 | tf_op jit(solution)/shard_map/ppermute | solution.py:220
  58.8 5.3 %collective-permute-start.6 = (bf16[256,256]{1,0:T(8,128)(2,1)S(1)}, bf16[256,256]{1,0:T(8,128)(2,1)S(1)}, u32[]{:S(2)}, u32[]{:S(2)}) collective-permute-start(bf16[256,256]{1,0:T(8,128)(2,1)S(1)} %copy-done.5), channel_id=1, source_target_pairs={{0,8},{2,10},{4,12},{6,14},{8,0},{10,2},{12,4},{14,6},{1,9},{3,11}... | collective-permute-start | bytes 393224 | tf_op jit(solution)/shard_map/ppermute | solution.py:220
  64.1 3.2 %collective-permute-done.3.refs_0_ = bf16[256,256]{1,0:T(8,128)(2,1)S(1)} collective-permute-done((bf16[256,256]{1,0:T(8,128)(2,1)S(1)}, bf16[256,256]{1,0:T(8,128)(2,1)S(1)}, u32[]{:S(2)}, u32[]{:S(2)}) %collective-permute-start.3) | collective-permute-done | bytes 131104 | tf_op jit(solution)/shard_map/ppermute | solution.py:220
  67.3 2.0 collective-permute-done.4.refs_1_
  69.3 5.1 %collective-permute-done.5.refs_2_ = bf16[256,256]{1,0:T(8,128)(2,1)S(1)} collective-permute-done((bf16[256,256]{1,0:T(8,128)(2,1)S(1)}, bf16[256,256]{1,0:T(8,128)(2,1)S(1)}, u32[]{:S(2)}, u32[]{:S(2)}) %collective-permute-start.5) | collective-permute-done | bytes 131104 | tf_op jit(solution)/shard_map/ppermute | solution.py:220
  74.4 5.1 %collective-permute-done.6.refs_3_ = bf16[256,256]{1,0:T(8,128)(2,1)S(1)} collective-permute-done((bf16[256,256]{1,0:T(8,128)(2,1)S(1)}, bf16[256,256]{1,0:T(8,128)(2,1)S(1)}, u32[]{:S(2)}, u32[]{:S(2)}) %collective-permute-start.6) | collective-permute-done | bytes 131104 | tf_op jit(solution)/shard_map/ppermute | solution.py:220
  79.5 0.6 copy-done.33
  80.1 3.3 %shard_map.189 = bf16[896,1024]{1,0:T(8,128)(2,1)} custom-call(bf16[896,256]{1,0:T(8,128)(2,1)} %get-tuple-element.26.pick_ref, f32[896,128]{1,0:T(8,128)} %get-tuple-element.27.scale_ref, bf16[256,256]{1,0:T(8,128)(2,1)} %copy-done.29, bf16[256,256]{1,0:T(8,128)(2,1)} %copy-done.30, bf16[256,256]{1,0:T(8,128)(2,1)} %copy-done.31, bf16[256,256]{1,0:T(8,128)(2,1)} %copy-done.33), custom_call_target="tpu_custom_call" | custom-call | flops 469762048 | bytes 3670016 | tf_op jit(solution)/shard_map/pallas_call | solution.py:289
  83.4 1.3 copy-done.10
  84.7 7.5 %all-to-all-start.2 = ((bf16[16,56,1024]{2,1,0:T(8,128)(2,1)}), bf16[16,56,1024]{2,1,0:T(8,128)(2,1)}, u32[]{:S(2)}, u32[]{:S(2)}) async-start(bf16[16,56,1024]{2,1,0:T(8,128)(2,1)} %bitcast.44), calls=%async_computation.2 | async-start | bytes 3670016 | tf_op jit(solution)/shard_map/all_to_all | solution.py:296
  92.2 0.1 collective-permute-start.7
  92.3 19.7 %all-to-all-done.2 = bf16[16,56,1024]{2,1,0:T(8,128)(2,1)} async-done(((bf16[16,56,1024]{2,1,0:T(8,128)(2,1)}), bf16[16,56,1024]{2,1,0:T(8,128)(2,1)}, u32[]{:S(2)}, u32[]{:S(2)}) %all-to-all-start.2) | async-done | bytes 1835040 | tf_op jit(solution)/shard_map/all_to_all | solution.py:296
  112.1 4.0 %collective-permute-done.8.th_ref = bf16[896,1024]{1,0:T(8,128)(2,1)} collective-permute-done((bf16[896,1024]{1,0:T(8,128)(2,1)}, bf16[896,1024]{1,0:T(8,128)(2,1)}, u32[]{:S(2)}, u32[]{:S(2)}) %collective-permute-start.8) | collective-permute-done | bytes 1835040 | tf_op jit(solution)/shard_map/ppermute | solution.py:299
  116.1 13.9 %expert.1 = (bf16[16,1024,256]{2,1,0:T(8,128)(2,1)}, bf16[1024,256]{1,0:T(8,128)(2,1)S(1)}, bf16[128,128]{1,0:T(8,128)(2,1)S(1)}, bf16[896,128]{1,0:T(8,128)(2,1)S(1)}) custom-call(s32[16]{0:T(128)S(1)} %pad_add_fusion.slab_ref, bf16[16,1152,256]{2,1,0:T(8,128)(2,1)} %bitcast.36, bf16[16,1152,256]{2,1,0:T(8,128)(2,1)} %bitcast.37, ...), custom_call_target="tpu_custom_call" | custom-call | flops 5368709120 | bytes 25165824 | tf_op jit(solution)/shard_map/expert/pallas_call | solution.py:309
  130.1 0.8 copy-done.3
  130.9 0.7 copy-done.7
  131.6 0.6 copy-done.8
  132.2 19.4 %weight_grads.1 = (f32[128,4096]{1,0:T(8,128)}, f32[128,4096]{1,0:T(8,128)}, f32[128,4096]{1,0:T(8,128)}) custom-call(s32[16]{0:T(128)} %copy-done.9, bf16[1024,256]{1,0:T(8,128)(2,1)} %copy-done.3, bf16[128,128]{1,0:T(8,128)(2,1)} %copy-done.8, bf16[896,128]{1,0:T(8,128)(2,1)} %copy-done.7, bf16[16,1152,256]{2,1,0:T(8,128)(2,1)} %bitcast.38, ...), custom_call_target="tpu_custom_call" | custom-call | flops 3221225472 | bytes 25165824 | tf_op jit(solution)/shard_map/weight_grads/pallas_call | solution.py:352
  151.7 54.8 %reduce-scatter.2.cloned.1.call-done = bf16[1,1024,256]{2,1,0:T(8,128)(2,1)} async-done(((bf16[16,1024,256]{2,1,0:T(8,128)(2,1)}), bf16[1,1024,256]{2,1,0:T(8,128)(2,1)}) %reduce-scatter.2.cloned.1.call-update) | async-done | bytes 524304 | tf_op jit(solution)/shard_map/reduce_scatter | solution.py:342
  206.4 7.3 %all-to-all-start.3 = ((bf16[16,64,256]{2,1,0:T(8,128)(2,1)}), bf16[16,64,256]{2,1,0:T(8,128)(2,1)S(1)}, u32[]{:S(2)}, u32[]{:S(2)}) async-start(bf16[16,64,256]{2,1,0:T(8,128)(2,1)} %bitcast.47), calls=%async_computation.4 | async-start | bytes 1048576 | tf_op jit(solution)/shard_map/all_to_all | solution.py:375
  213.8 0.1 slice.52
  213.9 0.1 slice.51
  214.1 0.1 copy.23
  214.3 3.4 %collective-permute-start.9 = (bf16[2,128,2]{2,1,0:T(8,128)(2,1)S(1)}, bf16[2,128,2]{2,1,0:T(8,128)(2,1)S(1)}, u32[]{:S(2)}, u32[]{:S(2)}) collective-permute-start(bf16[2,128,2]{2,1,0:T(8,128)(2,1)S(1)} %copy.23), channel_id=1, source_target_pairs={{0,16},{16,32},{32,48},{48,64},{64,80},{80,96},{96,112},{112,128},... | collective-permute-start | bytes 3080 | tf_op jit(solution)/shard_map/ppermute | solution.py:227
  217.7 4.0 %all-to-all-done.3 = bf16[16,64,256]{2,1,0:T(8,128)(2,1)S(1)} async-done(((bf16[16,64,256]{2,1,0:T(8,128)(2,1)}), bf16[16,64,256]{2,1,0:T(8,128)(2,1)S(1)}, u32[]{:S(2)}, u32[]{:S(2)}) %all-to-all-start.3) | async-done | bytes 524320 | tf_op jit(solution)/shard_map/all_to_all | solution.py:375
  221.6 1.0 combine.1.refs_0_
  222.6 3.2 %collective-permute-start.11 = (bf16[256,256]{1,0:T(8,128)(2,1)}, bf16[256,256]{1,0:T(8,128)(2,1)S(1)}, u32[]{:S(2)}, u32[]{:S(2)}) collective-permute-start(bf16[256,256]{1,0:T(8,128)(2,1)} %combine.1.refs_0_), channel_id=1, source_target_pairs={{0,14},{2,0},{4,2},{6,4},{8,6},{10,8},{12,10},{14,12},{1,15},{3,1}... | collective-permute-start | bytes 393224 | tf_op jit(solution)/shard_map/ppermute | solution.py:220
  225.9 4.1 %collective-permute-start.13 = (bf16[256,256]{1,0:T(8,128)(2,1)}, bf16[256,256]{1,0:T(8,128)(2,1)S(1)}, u32[]{:S(2)}, u32[]{:S(2)}) collective-permute-start(bf16[256,256]{1,0:T(8,128)(2,1)} %combine.1.refs_0_), channel_id=1, source_target_pairs={{0,12},{2,14},{4,0},{6,2},{8,4},{10,6},{12,8},{14,10},{1,13},{3,15... | collective-permute-start | bytes 393224 | tf_op jit(solution)/shard_map/ppermute | solution.py:220
  230.0 0.5 collective-permute-start.14
  230.5 4.7 %collective-permute-start.15 = (bf16[256,256]{1,0:T(8,128)(2,1)}, bf16[256,256]{1,0:T(8,128)(2,1)S(1)}, u32[]{:S(2)}, u32[]{:S(2)}) collective-permute-start(bf16[256,256]{1,0:T(8,128)(2,1)} %combine.1.refs_0_), channel_id=1, source_target_pairs={{0,10},{2,12},{4,14},{6,0},{8,2},{10,4},{12,6},{14,8},{1,11},{3,13... | collective-permute-start | bytes 393224 | tf_op jit(solution)/shard_map/ppermute | solution.py:220
  235.1 4.3 %collective-permute-start.16 = (bf16[256,256]{1,0:T(8,128)(2,1)}, bf16[256,256]{1,0:T(8,128)(2,1)S(1)}, u32[]{:S(2)}, u32[]{:S(2)}) collective-permute-start(bf16[256,256]{1,0:T(8,128)(2,1)} %combine.1.refs_0_), channel_id=1, source_target_pairs={{0,8},{2,10},{4,12},{6,14},{8,0},{10,2},{12,4},{14,6},{1,9},{3,11}... | collective-permute-start | bytes 393224 | tf_op jit(solution)/shard_map/ppermute | solution.py:220
  239.5 0.5 collective-permute-start.18
  240.0 6.9 %collective-permute-done.14.refs_5_ = bf16[256,256]{1,0:T(8,128)(2,1)S(1)} collective-permute-done((bf16[256,256]{1,0:T(8,128)(2,1)}, bf16[256,256]{1,0:T(8,128)(2,1)S(1)}, u32[]{:S(2)}, u32[]{:S(2)}) %collective-permute-start.14) | collective-permute-done | bytes 131104 | tf_op jit(solution)/shard_map/ppermute | solution.py:220
  246.9 0.1 convert_multiply_fusion
  247.1 1.3 collective-permute-done.15.refs_6_
  248.4 0.5 collective-permute-start.21
  248.9 0.3 collective-permute-start.22
  249.2 0.2 collective-permute-start.23
  249.4 0.3 collective-permute-start.24
  249.7 0.9 multiply_convert_fusion.2
  250.7 0.1 collective-permute-done.24.refs_15_
  250.8 0.4 copy-done.21
  251.4 3.1 %proj.1 = bf16[16,128,256]{2,1,0:T(8,128)(2,1)} custom-call(s32[16]{0:T(128)} %copy-done.9, bf16[128,256]{1,0:T(8,128)(2,1)} %get-tuple-element.44.act_ref, bf16[256,256]{1,0:T(8,128)(2,1)} %combine.1.refs_0_, bf16[256,256]{1,0:T(8,128)(2,1)} %copy-done.11, bf16[256,256]{1,0:T(8,128)(2,1)} %copy-done.12, bf16[256,256]{1,0:T(8,128)(2,1)} %copy-done.13, ...), custom_call_target="tpu_custom_call" | custom-call | flops 268435456 | bytes 4194304 | tf_op jit(solution)/shard_map/proj/pallas_call | solution.py:407
  254.5 5.9 %all-to-all-start.4 = ((bf16[16,128,256]{2,1,0:T(8,128)(2,1)}), bf16[16,128,256]{2,1,0:T(8,128)(2,1)S(1)}, u32[]{:S(2)}, u32[]{:S(2)}) async-start(bf16[16,128,256]{2,1,0:T(8,128)(2,1)} %proj.1), calls=%async_computation.5 | async-start | bytes 2097152 | tf_op jit(solution)/shard_map/all_to_all | solution.py:414
  260.4 3.5 %mixer.1 = (bf16[128,256]{1,0:T(8,128)(2,1)}, f32[128,256]{1,0:T(8,128)}) custom-call(s32[16]{0:T(128)} %copy-done.9, bf16[128,4096]{1,0:T(8,128)(2,1)} %proj_ref.1, f32[128,256]{1,0:T(8,128)} %get-tuple-element.45.conv_ref, bf16[128,256]{1,0:T(8,128)(2,1)} %outer_ref.1, bf16[256,256]{1,0:T(8,128)(2,1)} %combine.1.refs_0_, bf16[256,256]{1,0:T(8,128)(2,1)} %copy-done.11, ...), custom_call_target="tpu_custom_call" | custom-call | flops 268435456 | bytes 4194304 | tf_op jit(solution)/shard_map/mixer/pallas_call | solution.py:416
  263.9 0.8 slice.60
  264.7 4.9 %collective-permute-start.25 = (f32[128,2]{1,0:T(8,128)S(1)}, f32[128,2]{1,0:T(8,128)S(1)}, u32[]{:S(2)}, u32[]{:S(2)}) collective-permute-start(f32[128,2]{1,0:T(8,128)S(1)} %slice.60), channel_id=1, source_target_pairs={{16,0},{32,16},{48,32},{64,48},{80,64},{96,80},{112,96},{128,112},... | collective-permute-start | bytes 3080 | tf_op jit(solution)/shard_map/ppermute | solution.py:227
  269.6 0.9 constant_dynamic-update-slice_fusion.1
  270.5 5.2 %collective-permute-done.25 = f32[128,2]{1,0:T(8,128)S(1)} collective-permute-done((f32[128,2]{1,0:T(8,128)S(1)}, f32[128,2]{1,0:T(8,128)S(1)}, u32[]{:S(2)}, u32[]{:S(2)}) %collective-permute-start.25) | collective-permute-done | bytes 1056 | tf_op jit(solution)/shard_map/ppermute | solution.py:227
  275.8 1.7 multiply_convert_fusion
  277.5 0.6 multiply_convert_fusion.1
  278.1 0.8 convert_reduce_fusion
  (109 shorter events, 0.8 us)
Async XLA Ops:
  7.2 109.0 %all-gather.3.cloned.1.call-start = ((), (), s32[]{:S(2)}) async-start(), calls=%async_computation.7 | async-start | bytes 10027008 | tf_op jit(solution)/shard_map/all_gather | solution.py:283
  9.9 18.5 %copy-start.4 = (bf16[256,256]{1,0:T(8,128)(2,1)S(1)}, bf16[256,256]{1,0:T(8,128)(2,1)}, u32[]{:S(2)}) copy-start(bf16[256,256]{1,0:T(8,128)(2,1)} %cot_ref.3) | copy-start | bytes 393220
  28.4 9.9 %collective-permute-start = (bf16[256,256]{1,0:T(8,128)(2,1)S(1)}, bf16[256,256]{1,0:T(8,128)(2,1)S(1)}, u32[]{:S(2)}, u32[]{:S(2)}) collective-permute-start(bf16[256,256]{1,0:T(8,128)(2,1)S(1)} %copy-done.4), channel_id=1, source_target_pairs={{0,2},{2,4},{4,6},{6,8},{8,10},{10,12},{12,14},{14,0},{1,3},{3,5},... | collective-permute-start | bytes 393224 | tf_op jit(solution)/shard_map/ppermute | solution.py:220
  30.4 7.9 %collective-permute-start.1 = (bf16[256,256]{1,0:T(8,128)(2,1)S(1)}, bf16[256,256]{1,0:T(8,128)(2,1)S(1)}, u32[]{:S(2)}, u32[]{:S(2)}) collective-permute-start(bf16[256,256]{1,0:T(8,128)(2,1)S(1)} %copy-done.4), channel_id=1, source_target_pairs={{0,14},{2,0},{4,2},{6,4},{8,6},{10,8},{12,10},{14,12},{1,15},{3,1}... | collective-permute-start | bytes 393224 | tf_op jit(solution)/shard_map/ppermute | solution.py:220
  34.4 9.0 %collective-permute-start.2 = (bf16[256,256]{1,0:T(8,128)(2,1)S(1)}, bf16[256,256]{1,0:T(8,128)(2,1)S(1)}, u32[]{:S(2)}, u32[]{:S(2)}) collective-permute-start(bf16[256,256]{1,0:T(8,128)(2,1)S(1)} %copy-done.4), channel_id=1, source_target_pairs={{0,4},{2,6},{4,8},{6,10},{8,12},{10,14},{12,0},{14,2},{1,5},{3,7},... | collective-permute-start | bytes 393224 | tf_op jit(solution)/shard_map/ppermute | solution.py:220
  38.3 5.2 %copy-start.32 = (bf16[256,256]{1,0:T(8,128)(2,1)}, bf16[256,256]{1,0:T(8,128)(2,1)S(1)}, u32[]{:S(2)}) copy-start(bf16[256,256]{1,0:T(8,128)(2,1)S(1)} %collective-permute-done.refs_1_) | copy-start | bytes 393220
  38.3 5.2 %copy-start.34 = (bf16[256,256]{1,0:T(8,128)(2,1)}, bf16[256,256]{1,0:T(8,128)(2,1)S(1)}, u32[]{:S(2)}) copy-start(bf16[256,256]{1,0:T(8,128)(2,1)S(1)} %collective-permute-done.1.refs_2_) | copy-start | bytes 393220
  47.3 5.9 %copy-start.5 = (bf16[256,256]{1,0:T(8,128)(2,1)S(1)}, bf16[256,256]{1,0:T(8,128)(2,1)}, u32[]{:S(2)}) copy-start(bf16[256,256]{1,0:T(8,128)(2,1)} %cot_ref.3) | copy-start | bytes 393220
  47.3 36.1 %all-to-all-start.1 = ((bf16[16,56,1024]{2,1,0:T(8,128)(2,1)}), bf16[16,56,1024]{2,1,0:T(8,128)(2,1)S(1)}, u32[]{:S(2)}, u32[]{:S(2)}) async-start(bf16[16,56,1024]{2,1,0:T(8,128)(2,1)} %bitcast.43), calls=%async_computation.1 | async-start | bytes 3670016 | tf_op jit(solution)/shard_map/all_to_all | solution.py:296
  53.2 14.1 %collective-permute-start.3 = (bf16[256,256]{1,0:T(8,128)(2,1)S(1)}, bf16[256,256]{1,0:T(8,128)(2,1)S(1)}, u32[]{:S(2)}, u32[]{:S(2)}) collective-permute-start(bf16[256,256]{1,0:T(8,128)(2,1)S(1)} %copy-done.5), channel_id=1, source_target_pairs={{0,12},{2,14},{4,0},{6,2},{8,4},{10,6},{12,8},{14,10},{1,13},{3,15... | collective-permute-start | bytes 393224 | tf_op jit(solution)/shard_map/ppermute | solution.py:220
  53.8 15.5 %collective-permute-start.4 = (bf16[256,256]{1,0:T(8,128)(2,1)S(1)}, bf16[256,256]{1,0:T(8,128)(2,1)S(1)}, u32[]{:S(2)}, u32[]{:S(2)}) collective-permute-start(bf16[256,256]{1,0:T(8,128)(2,1)S(1)} %copy-done.5), channel_id=1, source_target_pairs={{0,6},{2,8},{4,10},{6,12},{8,14},{10,0},{12,2},{14,4},{1,7},{3,9},... | collective-permute-start | bytes 393224 | tf_op jit(solution)/shard_map/ppermute | solution.py:220
  54.0 20.4 %collective-permute-start.5 = (bf16[256,256]{1,0:T(8,128)(2,1)S(1)}, bf16[256,256]{1,0:T(8,128)(2,1)S(1)}, u32[]{:S(2)}, u32[]{:S(2)}) collective-permute-start(bf16[256,256]{1,0:T(8,128)(2,1)S(1)} %copy-done.5), channel_id=1, source_target_pairs={{0,10},{2,12},{4,14},{6,0},{8,2},{10,4},{12,6},{14,8},{1,11},{3,13... | collective-permute-start | bytes 393224 | tf_op jit(solution)/shard_map/ppermute | solution.py:220
  58.8 20.6 %collective-permute-start.6 = (bf16[256,256]{1,0:T(8,128)(2,1)S(1)}, bf16[256,256]{1,0:T(8,128)(2,1)S(1)}, u32[]{:S(2)}, u32[]{:S(2)}) collective-permute-start(bf16[256,256]{1,0:T(8,128)(2,1)S(1)} %copy-done.5), channel_id=1, source_target_pairs={{0,8},{2,10},{4,12},{6,14},{8,0},{10,2},{12,4},{14,6},{1,9},{3,11}... | collective-permute-start | bytes 393224 | tf_op jit(solution)/shard_map/ppermute | solution.py:220
  67.3 12.2 %copy-start.29 = (bf16[256,256]{1,0:T(8,128)(2,1)}, bf16[256,256]{1,0:T(8,128)(2,1)S(1)}, u32[]{:S(2)}) copy-start(bf16[256,256]{1,0:T(8,128)(2,1)S(1)} %collective-permute-done.3.refs_0_) | copy-start | bytes 393220
  69.3 10.2 %copy-start.30 = (bf16[256,256]{1,0:T(8,128)(2,1)}, bf16[256,256]{1,0:T(8,128)(2,1)S(1)}, u32[]{:S(2)}) copy-start(bf16[256,256]{1,0:T(8,128)(2,1)S(1)} %collective-permute-done.4.refs_1_) | copy-start | bytes 393220
  74.4 5.1 %copy-start.31 = (bf16[256,256]{1,0:T(8,128)(2,1)}, bf16[256,256]{1,0:T(8,128)(2,1)S(1)}, u32[]{:S(2)}) copy-start(bf16[256,256]{1,0:T(8,128)(2,1)S(1)} %collective-permute-done.5.refs_2_) | copy-start | bytes 393220
  83.4 1.3 copy-start.10
  84.7 27.3 %copy-start.37 = (s32[8]{0:T(128)S(1)}, s32[8]{0:T(128)}, u32[]{:S(2)}) copy-start(s32[8]{0:T(128)} %constant.35) | copy-start | bytes 100
  84.7 31.5 %copy-start = (bf16[1,128,4096]{2,1,0:T(8,128)(2,1)S(1)}, bf16[1,128,4096]{2,1,0:T(8,128)(2,1)}, u32[]{:S(2)}) copy-start(bf16[1,128,4096]{2,1,0:T(8,128)(2,1)} %param.21) | copy-start | bytes 3145732
  84.7 31.5 %copy-start.1 = (bf16[1,128,4096]{2,1,0:T(8,128)(2,1)S(1)}, bf16[1,128,4096]{2,1,0:T(8,128)(2,1)}, u32[]{:S(2)}) copy-start(bf16[1,128,4096]{2,1,0:T(8,128)(2,1)} %param.22) | copy-start | bytes 3145732
  84.7 31.5 %copy-start.2 = (bf16[1,128,4096]{2,1,0:T(8,128)(2,1)S(1)}, bf16[1,128,4096]{2,1,0:T(8,128)(2,1)}, u32[]{:S(2)}) copy-start(bf16[1,128,4096]{2,1,0:T(8,128)(2,1)} %param.23) | copy-start | bytes 3145732
  84.7 27.3 %all-to-all-start.2 = ((bf16[16,56,1024]{2,1,0:T(8,128)(2,1)}), bf16[16,56,1024]{2,1,0:T(8,128)(2,1)}, u32[]{:S(2)}, u32[]{:S(2)}) async-start(bf16[16,56,1024]{2,1,0:T(8,128)(2,1)} %bitcast.44), calls=%async_computation.2 | async-start | bytes 3670016 | tf_op jit(solution)/shard_map/all_to_all | solution.py:296
  92.2 114.3 %reduce-scatter.2.cloned.1.call-start = ((), (), s32[]{:S(2)}) async-start(), calls=%async_computation.6 | async-start | bytes 8912896 | tf_op jit(solution)/shard_map/reduce_scatter | solution.py:342
  92.2 19.9 %collective-permute-start.7 = (bf16[896,1024]{1,0:T(8,128)(2,1)}, bf16[896,1024]{1,0:T(8,128)(2,1)}, u32[]{:S(2)}, u32[]{:S(2)}) collective-permute-start(bf16[896,1024]{1,0:T(8,128)(2,1)} %bitcast.40), channel_id=1, source_target_pairs={{0,1},{1,0},{2,3},{3,2},{4,5},{5,4},{6,7},{7,6},{8,9},{9,8},{10,11... | collective-permute-start | bytes 5505032 | tf_op jit(solution)/shard_map/ppermute | solution.py:299
  112.0 4.1 %collective-permute-start.8 = (bf16[896,1024]{1,0:T(8,128)(2,1)}, bf16[896,1024]{1,0:T(8,128)(2,1)}, u32[]{:S(2)}, u32[]{:S(2)}) collective-permute-start(bf16[896,1024]{1,0:T(8,128)(2,1)} %bitcast.9.mh_ref), channel_id=1, source_target_pairs={{0,1},{1,0},{2,3},{3,2},{4,5},{5,4},{6,7},{7,6},{8,9},{9,8},{10,11... | collective-permute-start | bytes 5505032 | tf_op jit(solution)/shard_map/ppermute | solution.py:299
  112.1 18.0 %copy-start.9 = (s32[16]{0:T(128)}, s32[16]{0:T(128)S(1)}, u32[]{:S(2)}) copy-start(s32[16]{0:T(128)S(1)} %pad_add_fusion.slab_ref) | copy-start | bytes 196
  130.1 0.8 copy-start.3
  130.9 0.7 copy-start.7
  132.2 81.6 %copy-start.27 = (bf16[128,256]{1,0:T(8,128)(2,1)S(1)}, bf16[128,256]{1,0:T(8,128)(2,1)}, u32[]{:S(2)}) copy-start(bf16[128,256]{1,0:T(8,128)(2,1)} %param.15) | copy-start | bytes 196612
  132.2 81.7 %copy-start.26 = (bf16[128,256]{1,0:T(8,128)(2,1)S(1)}, bf16[128,256]{1,0:T(8,128)(2,1)}, u32[]{:S(2)}) copy-start(bf16[128,256]{1,0:T(8,128)(2,1)} %param.14) | copy-start | bytes 196612
  132.2 89.4 %copy-start.6 = (bf16[1024,256]{1,0:T(8,128)(2,1)S(1)}, bf16[1024,256]{1,0:T(8,128)(2,1)}, u32[]{:S(2)}) copy-start(bf16[1024,256]{1,0:T(8,128)(2,1)} %get-tuple-element.38.pick_ref) | copy-start | bytes 1572868
  151.6 78.8 %copy-start.36 = (f32[3,128]{1,0:T(4,128)S(1)}, f32[3,128]{1,0:T(4,128)}, u32[]{:S(2)}) copy-start(f32[3,128]{1,0:T(4,128)} %param.16) | copy-start | bytes 4612
  151.6 98.1 %copy-start.28 = (bf16[128,256]{1,0:T(8,128)(2,1)S(1)}, bf16[128,256]{1,0:T(8,128)(2,1)}, u32[]{:S(2)}) copy-start(bf16[128,256]{1,0:T(8,128)(2,1)} %outer_ref.1) | copy-start | bytes 196612
  206.4 15.2 %all-to-all-start.3 = ((bf16[16,64,256]{2,1,0:T(8,128)(2,1)}), bf16[16,64,256]{2,1,0:T(8,128)(2,1)S(1)}, u32[]{:S(2)}, u32[]{:S(2)}) async-start(bf16[16,64,256]{2,1,0:T(8,128)(2,1)} %bitcast.47), calls=%async_computation.4 | async-start | bytes 1048576 | tf_op jit(solution)/shard_map/all_to_all | solution.py:375
  214.3 15.7 %collective-permute-start.9 = (bf16[2,128,2]{2,1,0:T(8,128)(2,1)S(1)}, bf16[2,128,2]{2,1,0:T(8,128)(2,1)S(1)}, u32[]{:S(2)}, u32[]{:S(2)}) collective-permute-start(bf16[2,128,2]{2,1,0:T(8,128)(2,1)S(1)} %copy.23), channel_id=1, source_target_pairs={{0,16},{16,32},{32,48},{48,64},{64,80},{80,96},{96,112},{112,128},... | collective-permute-start | bytes 3080 | tf_op jit(solution)/shard_map/ppermute | solution.py:227
  222.6 7.8 %collective-permute-start.10 = (bf16[256,256]{1,0:T(8,128)(2,1)}, bf16[256,256]{1,0:T(8,128)(2,1)S(1)}, u32[]{:S(2)}, u32[]{:S(2)}) collective-permute-start(bf16[256,256]{1,0:T(8,128)(2,1)} %combine.1.refs_0_), channel_id=1, source_target_pairs={{0,2},{2,4},{4,6},{6,8},{8,10},{10,12},{12,14},{14,0},{1,3},{3,5},... | collective-permute-start | bytes 393224 | tf_op jit(solution)/shard_map/ppermute | solution.py:220
  222.6 12.5 %collective-permute-start.11 = (bf16[256,256]{1,0:T(8,128)(2,1)}, bf16[256,256]{1,0:T(8,128)(2,1)S(1)}, u32[]{:S(2)}, u32[]{:S(2)}) collective-permute-start(bf16[256,256]{1,0:T(8,128)(2,1)} %combine.1.refs_0_), channel_id=1, source_target_pairs={{0,14},{2,0},{4,2},{6,4},{8,6},{10,8},{12,10},{14,12},{1,15},{3,1}... | collective-permute-start | bytes 393224 | tf_op jit(solution)/shard_map/ppermute | solution.py:220
  225.9 13.6 %collective-permute-start.12 = (bf16[256,256]{1,0:T(8,128)(2,1)}, bf16[256,256]{1,0:T(8,128)(2,1)S(1)}, u32[]{:S(2)}, u32[]{:S(2)}) collective-permute-start(bf16[256,256]{1,0:T(8,128)(2,1)} %combine.1.refs_0_), channel_id=1, source_target_pairs={{0,4},{2,6},{4,8},{6,10},{8,12},{10,14},{12,0},{14,2},{1,5},{3,7},... | collective-permute-start | bytes 393224 | tf_op jit(solution)/shard_map/ppermute | solution.py:220
  225.9 13.6 %collective-permute-start.13 = (bf16[256,256]{1,0:T(8,128)(2,1)}, bf16[256,256]{1,0:T(8,128)(2,1)S(1)}, u32[]{:S(2)}, u32[]{:S(2)}) collective-permute-start(bf16[256,256]{1,0:T(8,128)(2,1)} %combine.1.refs_0_), channel_id=1, source_target_pairs={{0,12},{2,14},{4,0},{6,2},{8,4},{10,6},{12,8},{14,10},{1,13},{3,15... | collective-permute-start | bytes 393224 | tf_op jit(solution)/shard_map/ppermute | solution.py:220
  230.0 16.9 %collective-permute-start.14 = (bf16[256,256]{1,0:T(8,128)(2,1)}, bf16[256,256]{1,0:T(8,128)(2,1)S(1)}, u32[]{:S(2)}, u32[]{:S(2)}) collective-permute-start(bf16[256,256]{1,0:T(8,128)(2,1)} %combine.1.refs_0_), channel_id=1, source_target_pairs={{0,6},{2,8},{4,10},{6,12},{8,14},{10,0},{12,2},{14,4},{1,7},{3,9},... | collective-permute-start | bytes 393224 | tf_op jit(solution)/shard_map/ppermute | solution.py:220
  230.5 20.3 %copy-start.11 = (bf16[256,256]{1,0:T(8,128)(2,1)}, bf16[256,256]{1,0:T(8,128)(2,1)S(1)}, u32[]{:S(2)}) copy-start(bf16[256,256]{1,0:T(8,128)(2,1)S(1)} %collective-permute-done.10.refs_1_) | copy-start | bytes 393220
  230.5 17.9 %collective-permute-start.15 = (bf16[256,256]{1,0:T(8,128)(2,1)}, bf16[256,256]{1,0:T(8,128)(2,1)S(1)}, u32[]{:S(2)}, u32[]{:S(2)}) collective-permute-start(bf16[256,256]{1,0:T(8,128)(2,1)} %combine.1.refs_0_), channel_id=1, source_target_pairs={{0,10},{2,12},{4,14},{6,0},{8,2},{10,4},{12,6},{14,8},{1,11},{3,13... | collective-permute-start | bytes 393224 | tf_op jit(solution)/shard_map/ppermute | solution.py:220
  235.1 15.6 %copy-start.12 = (bf16[256,256]{1,0:T(8,128)(2,1)}, bf16[256,256]{1,0:T(8,128)(2,1)S(1)}, u32[]{:S(2)}) copy-start(bf16[256,256]{1,0:T(8,128)(2,1)S(1)} %collective-permute-done.11.refs_2_) | copy-start | bytes 393220
  235.1 13.2 %collective-permute-start.16 = (bf16[256,256]{1,0:T(8,128)(2,1)}, bf16[256,256]{1,0:T(8,128)(2,1)S(1)}, u32[]{:S(2)}, u32[]{:S(2)}) collective-permute-start(bf16[256,256]{1,0:T(8,128)(2,1)} %combine.1.refs_0_), channel_id=1, source_target_pairs={{0,8},{2,10},{4,12},{6,14},{8,0},{10,2},{12,4},{14,6},{1,9},{3,11}... | collective-permute-start | bytes 393224 | tf_op jit(solution)/shard_map/ppermute | solution.py:220
  239.5 11.3 %copy-start.13 = (bf16[256,256]{1,0:T(8,128)(2,1)}, bf16[256,256]{1,0:T(8,128)(2,1)S(1)}, u32[]{:S(2)}) copy-start(bf16[256,256]{1,0:T(8,128)(2,1)S(1)} %collective-permute-done.12.refs_3_) | copy-start | bytes 393220
  239.5 9.4 %collective-permute-start.17 = (bf16[256,256]{1,0:T(8,128)(2,1)}, bf16[256,256]{1,0:T(8,128)(2,1)S(1)}, u32[]{:S(2)}, u32[]{:S(2)}) collective-permute-start(bf16[256,256]{1,0:T(8,128)(2,1)} %combine.1.refs_0_), channel_id=1, source_target_pairs={{0,1},{1,0},{2,3},{3,2},{4,5},{5,4},{6,7},{7,6},{8,9},{9,8},{10,11... | collective-permute-start | bytes 393224 | tf_op jit(solution)/shard_map/ppermute | solution.py:386
  239.5 11.3 %copy-start.14 = (bf16[256,256]{1,0:T(8,128)(2,1)}, bf16[256,256]{1,0:T(8,128)(2,1)S(1)}, u32[]{:S(2)}) copy-start(bf16[256,256]{1,0:T(8,128)(2,1)S(1)} %collective-permute-done.13.refs_4_) | copy-start | bytes 393220
  239.5 9.7 %collective-permute-start.18 = (bf16[256,256]{1,0:T(8,128)(2,1)S(1)}, bf16[256,256]{1,0:T(8,128)(2,1)S(1)}, u32[]{:S(2)}, u32[]{:S(2)}) collective-permute-start(bf16[256,256]{1,0:T(8,128)(2,1)S(1)} %collective-permute-done.10.refs_1_), channel_id=1, source_target_pairs={{0,1},{1,0},{2,3},{3,2},{4,5},{5,4},{6,7},{7,6},{8,9},{9,8},{10,11... | collective-permute-start | bytes 393224 | tf_op jit(solution)/shard_map/ppermute | solution.py:386
  246.9 3.9 %copy-start.15 = (bf16[256,256]{1,0:T(8,128)(2,1)}, bf16[256,256]{1,0:T(8,128)(2,1)S(1)}, u32[]{:S(2)}) copy-start(bf16[256,256]{1,0:T(8,128)(2,1)S(1)} %collective-permute-done.14.refs_5_) | copy-start | bytes 393220
  246.9 2.5 collective-permute-start.19
  248.4 2.4 copy-start.16
  248.4 2.2 collective-permute-start.20
  248.4 2.4 copy-start.17
  248.4 2.2 collective-permute-start.21
  248.9 1.9 copy-start.18
  248.9 1.7 collective-permute-start.22
  249.2 1.6 copy-start.19
  249.2 1.4 collective-permute-start.23
  249.4 1.4 copy-start.20
  249.4 1.3 collective-permute-start.24
  250.6 0.7 copy-start.23
  250.7 0.8 copy-start.24
  254.5 23.6 %all-to-all-start.4 = ((bf16[16,128,256]{2,1,0:T(8,128)(2,1)}), bf16[16,128,256]{2,1,0:T(8,128)(2,1)S(1)}, u32[]{:S(2)}, u32[]{:S(2)}) async-start(bf16[16,128,256]{2,1,0:T(8,128)(2,1)} %proj.1), calls=%async_computation.5 | async-start | bytes 2097152 | tf_op jit(solution)/shard_map/all_to_all | solution.py:414
  264.7 11.0 %collective-permute-start.25 = (f32[128,2]{1,0:T(8,128)S(1)}, f32[128,2]{1,0:T(8,128)S(1)}, u32[]{:S(2)}, u32[]{:S(2)}) collective-permute-start(f32[128,2]{1,0:T(8,128)S(1)} %slice.60), channel_id=1, source_target_pairs={{16,0},{32,16},{48,32},{64,48},{80,64},{96,80},{112,96},{128,112},... | collective-permute-start | bytes 3080 | tf_op jit(solution)/shard_map/ppermute | solution.py:227
  (6 other events, 3.9 us)
Sparse Core Ops, SparseCore 0:
  28.5 79.4 all-gather.2
  132.3 74.0 reduce-scatter.1

commit v6 on v5

--- a/solution.py
+++ b/solution.py
@@ -336,7 +336,6 @@
         ),
         cost_estimate=cost(10 * slots * hidden_n * features, 6 * slots * features),
         name="expert",
-        compiler_params=grant(50),
     )(slab_of, state_all, state_all, *cots, w_gate[0], w_up[0], w_down[0])
 
     row_back = lax.psum_scatter(partial_value, TP, scatter_dimension=0, tiled=False)
@@ -368,8 +367,26 @@
         cost_estimate=cost(6 * slots * hidden_n * features, 6 * slots * features),
         name="weight_grads",
     )(slab_of, acts, soon_acts, late_acts, state_all, state_all, *cots)
-    row_back, grad_gate, grad_up, grad_down = lax.optimization_barrier(
-        (row_back, grad_gate, grad_up, grad_down)
+    taps_count = conv_taps.shape[0]
+    rim_width = taps_count - 1
+    channels = conv_inner.shape[0]
+    head_block = from_behind(
+        jnp.stack([conv_inner[:, tok_count - rim_width :], conv_input[:, tok_count - rim_width :]]),
+        "sp",
+        1,
+    )
+    inner_ext = jnp.concatenate([head_block[0], conv_inner], axis=1).astype(F32)
+    input_ext = jnp.concatenate([head_block[1], conv_input], axis=1).astype(F32)
+    inner_prod = inner_ext * input_ext
+    conv_out = jnp.zeros((channels, tok_count), F32)
+    for offset in range(taps_count):
+        conv_out = (
+            conv_out + conv_taps[offset][:, None] * inner_prod[:, offset : offset + tok_count]
+        )
+    mixer_act = (conv_outer.astype(F32) * conv_out).astype(BF16)
+
+    row_back, grad_gate, grad_up, grad_down, conv_out, mixer_act = lax.optimization_barrier(
+        (row_back, grad_gate, grad_up, grad_down, conv_out, mixer_act)
     )
 
     arrived = lax.all_to_all(
@@ -384,24 +401,6 @@
     )(pick, arrived, cotangent)
     near = gathered(grad_mixed, "z")
     full_back = near + [lax.ppermute(piece, "c", swap) for piece in near]
-
-    taps_count = conv_taps.shape[0]
-    rim_width = taps_count - 1
-    channels = conv_inner.shape[0]
-    head_block = from_behind(
-        jnp.stack([conv_inner[:, tok_count - rim_width :], conv_input[:, tok_count - rim_width :]]),
-        "sp",
-        1,
-    )
-    inner_ext = jnp.concatenate([head_block[0], conv_inner], axis=1).astype(F32)
-    input_ext = jnp.concatenate([head_block[1], conv_input], axis=1).astype(F32)
-    inner_prod = inner_ext * input_ext
-    conv_out = jnp.zeros((channels, tok_count), F32)
-    for offset in range(taps_count):
-        conv_out = (
-            conv_out + conv_taps[offset][:, None] * inner_prod[:, offset : offset + tok_count]
-        )
-    mixer_act = (conv_outer.astype(F32) * conv_out).astype(BF16)
 
     vmem, smem = pl.BlockSpec(memory_space=pltpu.VMEM), pl.BlockSpec(memory_space=pltpu.SMEM)
     proj_term = pl.pallas_call(

time: 291 us -> 288 us (0.990)
  blocking collectives: 17.5 us -> 32.6 us
  starting transfers between devices: 70.6 us -> 61.6 us
  waiting for transfers between devices: 120 us -> 113 us
    all_to_all x0 -> x1, blocking collectives: none -> 15.1 us  [shards(): lax.all_to_all(row_back.reshape(experts, cap, width), 'sp', split_axis=0,...]
    reduce_scatter x1, waiting for transfers between devices: 54.8 us -> 44.2 us  [shards(): lax.psum_scatter(partial_value, TP, scatter_dimension=0, tiled=False)]
    all_to_all x1 -> x0, starting transfers between devices: 7.32 us -> none  [shards(): lax.all_to_all(row_back.reshape(experts, cap, width), 'sp', split_axis=0,...]
    ppermute x2, waiting for transfers between devices: 5.24 us -> 10.3 us  [from_behind(): lax.ppermute(value, axis, [(source, source + steps) for source in range(f...]
    all_to_all x1 -> x0, waiting for transfers between devices: 3.95 us -> none  [shards(): lax.all_to_all(row_back.reshape(experts, cap, width), 'sp', split_axis=0,...]
    unnamed x79 -> x65, local copies, waits for them, and re-layouts: 6.45 us -> 4.1 us
  transfers between devices with their start and end apart: 32 -> 31, of which waited for: 14 -> 18; matrix products, arithmetic and copies ran while one was open for 2% -> 2% of each run, Pallas kernels for 11% -> 10%
where the time goes in v6:
time: 288 us; the launch traced here: 284 us
  waiting for transfers between devices  113 us (39%)
  starting transfers between devices  61.6 us (21%)
  Pallas kernels  51.5 us (18%)
  blocking collectives  32.6 us (11%)
  between operations  14.4 us (5%)
  other arithmetic  5.66 us (2%)
  local copies, waits for them, and re-layouts  5.33 us (2%)
    reduce_scatter x1, waiting for transfers between devices, shards(): lax.psum_scatter(partial_value, TP, scatter_dimension=0, tiled=False)  44.2 us
    ppermute x14, waiting for transfers between devices, gathered(): lax.ppermute(value, axis, [(i, (i + k) % size) for i in range(size)])  33.8 us
    ppermute x14, starting transfers between devices, gathered(): lax.ppermute(value, axis, [(i, (i + k) % size) for i in range(size)])  32.7 us
    all_to_all x2, waiting for transfers between devices, exchanged(): lax.all_to_all(part.reshape(experts, late_n, half), 'sp', split_axis=0, c...  19.7 us
    pallas_call x1, Pallas kernels, shards(): pl.pallas_call(weight_grad_kernel, grid_spec=pltpu.PrefetchScalarGridSpec...  19.6 us
    all_to_all x1, blocking collectives, shards(): lax.all_to_all(sent_rows.reshape(experts, cap + early, width), 'sp', spli...  17.5 us
    pallas_call x1, Pallas kernels, shards(): pl.pallas_call(functools.partial(expert_kernel, cap, early), grid_spec=pl...  15.1 us
    all_to_all x1, blocking collectives, shards(): lax.all_to_all(row_back.reshape(experts, cap, width), 'sp', split_axis=0,...  15.1 us
  transfers between devices with their start and end apart: 31, of which 18 were waited for; matrix products, arithmetic and copies ran while one was open for 2% of the time, Pallas kernels for 10%

profile of v6, /device:TPU:24, one launch (start us, length us, event | category | flops | bytes accessed | tf_op | source)
XLA Modules:
  0.0 283.7 jit_solution(9660916478346168115)
XLA Ops:
  7.2 2.7 route.1
  9.9 17.5 %all_to_all.25 = bf16[16,72,256]{2,1,0:T(8,128)(2,1)S(1)} all-to-all(bf16[16,72,256]{2,1,0:T(8,128)(2,1)} %bitcast.46), channel_id=1, replica_groups=mesh['sp'=16,'z'=8,'c'=2] {'sp'}, dimensions={0} | all-to-all | bytes 1179648 | tf_op jit(solution)/shard_map/all_to_all | solution.py:273
  27.5 0.9 pad_maximum_fusion
  28.4 2.0 collective-permute-start
  30.4 4.0 %collective-permute-start.1 = (bf16[256,256]{1,0:T(8,128)(2,1)S(1)}, bf16[256,256]{1,0:T(8,128)(2,1)S(1)}, u32[]{:S(2)}, u32[]{:S(2)}) collective-permute-start(bf16[256,256]{1,0:T(8,128)(2,1)S(1)} %copy-done), channel_id=1, source_target_pairs={{0,14},{2,0},{4,2},{6,4},{8,6},{10,8},{12,10},{14,12},{1,15},{3,1}... | collective-permute-start | bytes 393224 | tf_op jit(solution)/shard_map/ppermute | solution.py:220
  34.4 3.8 %collective-permute-done.refs_1_ = bf16[256,256]{1,0:T(8,128)(2,1)S(1)} collective-permute-done((bf16[256,256]{1,0:T(8,128)(2,1)S(1)}, bf16[256,256]{1,0:T(8,128)(2,1)S(1)}, u32[]{:S(2)}, u32[]{:S(2)}) %collective-permute-start) | collective-permute-done | bytes 131104 | tf_op jit(solution)/shard_map/ppermute | solution.py:220
  38.3 5.1 %collective-permute-done.2.refs_3_ = bf16[256,256]{1,0:T(8,128)(2,1)S(1)} collective-permute-done((bf16[256,256]{1,0:T(8,128)(2,1)S(1)}, bf16[256,256]{1,0:T(8,128)(2,1)S(1)}, u32[]{:S(2)}, u32[]{:S(2)}) %collective-permute-start.2) | collective-permute-done | bytes 131104 | tf_op jit(solution)/shard_map/ppermute | solution.py:220
  43.4 0.6 copy-done.28
  44.1 3.2 %shard_map.188 = bf16[896,1024]{1,0:T(8,128)(2,1)} custom-call(bf16[896,256]{1,0:T(8,128)(2,1)} %get-tuple-element.28.pick_ref, f32[896,128]{1,0:T(8,128)} %get-tuple-element.29.scale_ref, bf16[256,256]{1,0:T(8,128)(2,1)} %cot_ref.3, bf16[256,256]{1,0:T(8,128)(2,1)} %copy-done.25, bf16[256,256]{1,0:T(8,128)(2,1)} %copy-done.27, bf16[256,256]{1,0:T(8,128)(2,1)} %copy-done.28), custom_call_target="tpu_custom_call" | custom-call | flops 469762048 | bytes 3670016 | tf_op jit(solution)/shard_map/pallas_call | solution.py:289
  47.3 5.9 %all-to-all-start.1 = ((bf16[16,56,1024]{2,1,0:T(8,128)(2,1)}), bf16[16,56,1024]{2,1,0:T(8,128)(2,1)S(1)}, u32[]{:S(2)}, u32[]{:S(2)}) async-start(bf16[16,56,1024]{2,1,0:T(8,128)(2,1)} %bitcast.40), calls=%async_computation.1 | async-start | bytes 3670016 | tf_op jit(solution)/shard_map/all_to_all | solution.py:296
  53.2 0.6 collective-permute-start.3
  53.8 0.2 collective-permute-start.4
  54.0 4.8 %collective-permute-start.5 = (bf16[256,256]{1,0:T(8,128)(2,1)S(1)}, bf16[256,256]{1,0:T(8,128)(2,1)S(1)}, u32[]{:S(2)}, u32[]{:S(2)}) collective-permute-start(bf16[256,256]{1,0:T(8,128)(2,1)S(1)} %copy-done.1), channel_id=1, source_target_pairs={{0,10},{2,12},{4,14},{6,0},{8,2},{10,4},{12,6},{14,8},{1,11},{3,13... | collective-permute-start | bytes 393224 | tf_op jit(solution)/shard_map/ppermute | solution.py:220
  58.8 5.3 %collective-permute-start.6 = (bf16[256,256]{1,0:T(8,128)(2,1)S(1)}, bf16[256,256]{1,0:T(8,128)(2,1)S(1)}, u32[]{:S(2)}, u32[]{:S(2)}) collective-permute-start(bf16[256,256]{1,0:T(8,128)(2,1)S(1)} %copy-done.1), channel_id=1, source_target_pairs={{0,8},{2,10},{4,12},{6,14},{8,0},{10,2},{12,4},{14,6},{1,9},{3,11}... | collective-permute-start | bytes 393224 | tf_op jit(solution)/shard_map/ppermute | solution.py:220
  64.1 3.2 %collective-permute-done.3.refs_0_ = bf16[256,256]{1,0:T(8,128)(2,1)S(1)} collective-permute-done((bf16[256,256]{1,0:T(8,128)(2,1)S(1)}, bf16[256,256]{1,0:T(8,128)(2,1)S(1)}, u32[]{:S(2)}, u32[]{:S(2)}) %collective-permute-start.3) | collective-permute-done | bytes 131104 | tf_op jit(solution)/shard_map/ppermute | solution.py:220
  67.3 2.0 collective-permute-done.4.refs_1_
  69.3 5.1 %collective-permute-done.5.refs_2_ = bf16[256,256]{1,0:T(8,128)(2,1)S(1)} collective-permute-done((bf16[256,256]{1,0:T(8,128)(2,1)S(1)}, bf16[256,256]{1,0:T(8,128)(2,1)S(1)}, u32[]{:S(2)}, u32[]{:S(2)}) %collective-permute-start.5) | collective-permute-done | bytes 131104 | tf_op jit(solution)/shard_map/ppermute | solution.py:220
  74.4 5.1 %collective-permute-done.6.refs_3_ = bf16[256,256]{1,0:T(8,128)(2,1)S(1)} collective-permute-done((bf16[256,256]{1,0:T(8,128)(2,1)S(1)}, bf16[256,256]{1,0:T(8,128)(2,1)S(1)}, u32[]{:S(2)}, u32[]{:S(2)}) %collective-permute-start.6) | collective-permute-done | bytes 131104 | tf_op jit(solution)/shard_map/ppermute | solution.py:220
  79.5 0.6 copy-done.26
  80.1 3.3 %shard_map.189 = bf16[896,1024]{1,0:T(8,128)(2,1)} custom-call(bf16[896,256]{1,0:T(8,128)(2,1)} %get-tuple-element.28.pick_ref, f32[896,128]{1,0:T(8,128)} %get-tuple-element.29.scale_ref, bf16[256,256]{1,0:T(8,128)(2,1)} %copy-done.22, bf16[256,256]{1,0:T(8,128)(2,1)} %copy-done.23, bf16[256,256]{1,0:T(8,128)(2,1)} %copy-done.24, bf16[256,256]{1,0:T(8,128)(2,1)} %copy-done.26), custom_call_target="tpu_custom_call" | custom-call | flops 469762048 | bytes 3670016 | tf_op jit(solution)/shard_map/pallas_call | solution.py:289
  83.4 7.2 %all-to-all-start.2 = ((bf16[16,56,1024]{2,1,0:T(8,128)(2,1)}), bf16[16,56,1024]{2,1,0:T(8,128)(2,1)}, u32[]{:S(2)}, u32[]{:S(2)}) async-start(bf16[16,56,1024]{2,1,0:T(8,128)(2,1)} %bitcast.41), calls=%async_computation.2 | async-start | bytes 3670016 | tf_op jit(solution)/shard_map/all_to_all | solution.py:296
  90.8 19.7 %all-to-all-done.2 = bf16[16,56,1024]{2,1,0:T(8,128)(2,1)} async-done(((bf16[16,56,1024]{2,1,0:T(8,128)(2,1)}), bf16[16,56,1024]{2,1,0:T(8,128)(2,1)}, u32[]{:S(2)}, u32[]{:S(2)}) %all-to-all-start.2) | async-done | bytes 1835040 | tf_op jit(solution)/shard_map/all_to_all | solution.py:296
  110.5 0.6 pad_add_fusion.slab_ref
  111.1 3.5 %collective-permute-done.8.th_ref = bf16[896,1024]{1,0:T(8,128)(2,1)} collective-permute-done((bf16[896,1024]{1,0:T(8,128)(2,1)}, bf16[896,1024]{1,0:T(8,128)(2,1)}, u32[]{:S(2)}, u32[]{:S(2)}) %collective-permute-start.8) | collective-permute-done | bytes 1835040 | tf_op jit(solution)/shard_map/ppermute | solution.py:299
  114.6 15.1 %expert.1 = (bf16[16,1024,256]{2,1,0:T(8,128)(2,1)}, bf16[1024,256]{1,0:T(8,128)(2,1)}, bf16[128,128]{1,0:T(8,128)(2,1)}, bf16[896,128]{1,0:T(8,128)(2,1)}) custom-call(s32[16]{0:T(128)} %pad_add_fusion.slab_ref, bf16[16,1152,256]{2,1,0:T(8,128)(2,1)} %bitcast.33, bf16[16,1152,256]{2,1,0:T(8,128)(2,1)} %bitcast.34, bf16[896,1024]{1,0:T(8,128)(2,1)} %bitcast.38, ...), custom_call_target="tpu_custom_call" | custom-call | flops 5368709120 | bytes 25165824 | tf_op jit(solution)/shard_map/expert/pallas_call | solution.py:309
  129.8 0.8 copy-done.20
  130.7 0.1 slice.51
  130.9 0.1 copy.23
  131.1 3.2 %collective-permute-start.9 = (bf16[2,128,2]{2,1,0:T(8,128)(2,1)S(1)}, bf16[2,128,2]{2,1,0:T(8,128)(2,1)S(1)}, u32[]{:S(2)}, u32[]{:S(2)}) collective-permute-start(bf16[2,128,2]{2,1,0:T(8,128)(2,1)S(1)} %copy.23), channel_id=1, source_target_pairs={{0,16},{16,32},{32,48},{48,64},{64,80},{80,96},{96,112},{112,128},... | collective-permute-start | bytes 3080 | tf_op jit(solution)/shard_map/ppermute | solution.py:227
  134.3 5.0 %collective-permute-done.9 = bf16[2,128,2]{2,1,0:T(8,128)(2,1)S(1)} collective-permute-done((bf16[2,128,2]{2,1,0:T(8,128)(2,1)S(1)}, bf16[2,128,2]{2,1,0:T(8,128)(2,1)S(1)}, u32[]{:S(2)}, u32[]{:S(2)}) %collective-permute-start.9) | collective-permute-done | bytes 1056 | tf_op jit(solution)/shard_map/ppermute | solution.py:227
  139.3 0.1 convert_multiply_fusion
  139.5 0.9 multiply_convert_fusion.2
  140.3 19.6 %weight_grads.1 = (f32[128,4096]{1,0:T(8,128)}, f32[128,4096]{1,0:T(8,128)}, f32[128,4096]{1,0:T(8,128)}) custom-call(s32[16]{0:T(128)} %pad_add_fusion.slab_ref, bf16[1024,256]{1,0:T(8,128)(2,1)} %get-tuple-element.31.act_ref, bf16[128,128]{1,0:T(8,128)(2,1)} %get-tuple-element.32.soon_ref, bf16[896,128]{1,0:T(8,128)(2,1)} %get-tuple-element.33.late_ref, ...), custom_call_target="tpu_custom_call" | custom-call | flops 3221225472 | bytes 25165824 | tf_op jit(solution)/shard_map/weight_grads/pallas_call | solution.py:351
  160.0 44.2 %reduce-scatter.2.cloned.1.call-done = bf16[1,1024,256]{2,1,0:T(8,128)(2,1)} async-done(((bf16[16,1024,256]{2,1,0:T(8,128)(2,1)}), bf16[1,1024,256]{2,1,0:T(8,128)(2,1)}) %reduce-scatter.2.cloned.1.call-update) | async-done | bytes 524304 | tf_op jit(solution)/shard_map/reduce_scatter | solution.py:341
  204.1 15.1 %all_to_all.26 = bf16[16,64,256]{2,1,0:T(8,128)(2,1)S(1)} all-to-all(bf16[16,64,256]{2,1,0:T(8,128)(2,1)} %bitcast.47), channel_id=1, replica_groups=mesh['sp'=16,'z'=8,'c'=2] {'sp'}, dimensions={0} | all-to-all | bytes 1048576 | tf_op jit(solution)/shard_map/all_to_all | solution.py:392
  219.2 1.0 combine.1.refs_0_
  220.3 3.2 %collective-permute-start.11 = (bf16[256,256]{1,0:T(8,128)(2,1)}, bf16[256,256]{1,0:T(8,128)(2,1)S(1)}, u32[]{:S(2)}, u32[]{:S(2)}) collective-permute-start(bf16[256,256]{1,0:T(8,128)(2,1)} %combine.1.refs_0_), channel_id=1, source_target_pairs={{0,14},{2,0},{4,2},{6,4},{8,6},{10,8},{12,10},{14,12},{1,15},{3,1}... | collective-permute-start | bytes 393224 | tf_op jit(solution)/shard_map/ppermute | solution.py:220
  223.5 4.1 %collective-permute-start.13 = (bf16[256,256]{1,0:T(8,128)(2,1)}, bf16[256,256]{1,0:T(8,128)(2,1)S(1)}, u32[]{:S(2)}, u32[]{:S(2)}) collective-permute-start(bf16[256,256]{1,0:T(8,128)(2,1)} %combine.1.refs_0_), channel_id=1, source_target_pairs={{0,12},{2,14},{4,0},{6,2},{8,4},{10,6},{12,8},{14,10},{1,13},{3,15... | collective-permute-start | bytes 393224 | tf_op jit(solution)/shard_map/ppermute | solution.py:220
  227.6 5.0 %collective-permute-start.15 = (bf16[256,256]{1,0:T(8,128)(2,1)}, bf16[256,256]{1,0:T(8,128)(2,1)S(1)}, u32[]{:S(2)}, u32[]{:S(2)}) collective-permute-start(bf16[256,256]{1,0:T(8,128)(2,1)} %combine.1.refs_0_), channel_id=1, source_target_pairs={{0,10},{2,12},{4,14},{6,0},{8,2},{10,4},{12,6},{14,8},{1,11},{3,13... | collective-permute-start | bytes 393224 | tf_op jit(solution)/shard_map/ppermute | solution.py:220
  232.7 3.3 %collective-permute-start.16 = (bf16[256,256]{1,0:T(8,128)(2,1)}, bf16[256,256]{1,0:T(8,128)(2,1)S(1)}, u32[]{:S(2)}, u32[]{:S(2)}) collective-permute-start(bf16[256,256]{1,0:T(8,128)(2,1)} %combine.1.refs_0_), channel_id=1, source_target_pairs={{0,8},{2,10},{4,12},{6,14},{8,0},{10,2},{12,4},{14,6},{1,9},{3,11}... | collective-permute-start | bytes 393224 | tf_op jit(solution)/shard_map/ppermute | solution.py:220
  236.0 0.5 collective-permute-start.18
  236.5 7.5 %collective-permute-done.14.refs_5_ = bf16[256,256]{1,0:T(8,128)(2,1)S(1)} collective-permute-done((bf16[256,256]{1,0:T(8,128)(2,1)}, bf16[256,256]{1,0:T(8,128)(2,1)S(1)}, u32[]{:S(2)}, u32[]{:S(2)}) %collective-permute-start.14) | collective-permute-done | bytes 131104 | tf_op jit(solution)/shard_map/ppermute | solution.py:220
  244.0 1.9 collective-permute-done.15.refs_6_
  246.0 0.5 collective-permute-start.21
  246.5 0.1 collective-permute-start.22
  246.6 0.4 collective-permute-start.23
  247.0 0.1 collective-permute-start.24
  247.1 0.2 collective-permute-done.20.refs_11_
  247.3 0.2 collective-permute-done.21.refs_12_
  247.5 0.3 collective-permute-done.22.refs_13_
  247.8 0.2 collective-permute-done.23.refs_14_
  248.0 0.3 collective-permute-done.24.refs_15_
  248.5 0.2 copy-done.17
  248.7 0.7 copy-done.18
  249.3 3.1 %proj.1 = bf16[16,128,256]{2,1,0:T(8,128)(2,1)} custom-call(s32[16]{0:T(128)} %pad_add_fusion.slab_ref, bf16[128,256]{1,0:T(8,128)(2,1)} %get-tuple-element.42.act_ref, bf16[256,256]{1,0:T(8,128)(2,1)} %combine.1.refs_0_, bf16[256,256]{1,0:T(8,128)(2,1)} %copy-done.4, bf16[256,256]{1,0:T(8,128)(2,1)} %copy-done.5, bf16[256,256]{1,0:T(8,128)(2,1)} %copy-done.6, ...), custom_call_target="tpu_custom_call" | custom-call | flops 268435456 | bytes 4194304 | tf_op jit(solution)/shard_map/proj/pallas_call | solution.py:406
  252.4 5.9 %all-to-all-start.4 = ((bf16[16,128,256]{2,1,0:T(8,128)(2,1)}), bf16[16,128,256]{2,1,0:T(8,128)(2,1)S(1)}, u32[]{:S(2)}, u32[]{:S(2)}) async-start(bf16[16,128,256]{2,1,0:T(8,128)(2,1)} %proj.1), calls=%async_computation.5 | async-start | bytes 2097152 | tf_op jit(solution)/shard_map/all_to_all | solution.py:413
  258.3 3.5 %mixer.1 = (bf16[128,256]{1,0:T(8,128)(2,1)}, f32[128,256]{1,0:T(8,128)}) custom-call(s32[16]{0:T(128)} %pad_add_fusion.slab_ref, bf16[128,4096]{1,0:T(8,128)(2,1)} %proj_ref.1, f32[128,256]{1,0:T(8,128)} %get-tuple-element.43.conv_ref, bf16[128,256]{1,0:T(8,128)(2,1)} %outer_ref.1, bf16[256,256]{1,0:T(8,128)(2,1)} %combine.1.refs_0_, ...), custom_call_target="tpu_custom_call" | custom-call | flops 268435456 | bytes 4194304 | tf_op jit(solution)/shard_map/mixer/pallas_call | solution.py:415
  261.8 0.8 slice.60
  262.6 4.9 %collective-permute-start.25 = (f32[128,2]{1,0:T(8,128)S(1)}, f32[128,2]{1,0:T(8,128)S(1)}, u32[]{:S(2)}, u32[]{:S(2)}) collective-permute-start(f32[128,2]{1,0:T(8,128)S(1)} %slice.60), channel_id=1, source_target_pairs={{16,0},{32,16},{48,32},{64,48},{80,64},{96,80},{112,96},{128,112},... | collective-permute-start | bytes 3080 | tf_op jit(solution)/shard_map/ppermute | solution.py:227
  267.5 0.9 constant_dynamic-update-slice_fusion.1
  268.4 5.3 %collective-permute-done.25 = f32[128,2]{1,0:T(8,128)S(1)} collective-permute-done((f32[128,2]{1,0:T(8,128)S(1)}, f32[128,2]{1,0:T(8,128)S(1)}, u32[]{:S(2)}, u32[]{:S(2)}) %collective-permute-start.25) | collective-permute-done | bytes 1056 | tf_op jit(solution)/shard_map/ppermute | solution.py:227
  273.7 1.7 multiply_convert_fusion
  275.5 0.6 multiply_convert_fusion.1
  276.1 0.8 convert_reduce_fusion
  (94 shorter events, 0.7 us)
Async XLA Ops:
  7.2 107.4 %all-gather.3.cloned.1.call-start = ((), (), s32[]{:S(2)}) async-start(), calls=%async_computation.7 | async-start | bytes 10027008 | tf_op jit(solution)/shard_map/all_gather | solution.py:283
  9.9 18.5 %copy-start = (bf16[256,256]{1,0:T(8,128)(2,1)S(1)}, bf16[256,256]{1,0:T(8,128)(2,1)}, u32[]{:S(2)}) copy-start(bf16[256,256]{1,0:T(8,128)(2,1)} %cot_ref.3) | copy-start | bytes 393220
  28.4 9.9 %collective-permute-start = (bf16[256,256]{1,0:T(8,128)(2,1)S(1)}, bf16[256,256]{1,0:T(8,128)(2,1)S(1)}, u32[]{:S(2)}, u32[]{:S(2)}) collective-permute-start(bf16[256,256]{1,0:T(8,128)(2,1)S(1)} %copy-done), channel_id=1, source_target_pairs={{0,2},{2,4},{4,6},{6,8},{8,10},{10,12},{12,14},{14,0},{1,3},{3,5},... | collective-permute-start | bytes 393224 | tf_op jit(solution)/shard_map/ppermute | solution.py:220
  30.4 7.9 %collective-permute-start.1 = (bf16[256,256]{1,0:T(8,128)(2,1)S(1)}, bf16[256,256]{1,0:T(8,128)(2,1)S(1)}, u32[]{:S(2)}, u32[]{:S(2)}) collective-permute-start(bf16[256,256]{1,0:T(8,128)(2,1)S(1)} %copy-done), channel_id=1, source_target_pairs={{0,14},{2,0},{4,2},{6,4},{8,6},{10,8},{12,10},{14,12},{1,15},{3,1}... | collective-permute-start | bytes 393224 | tf_op jit(solution)/shard_map/ppermute | solution.py:220
  34.4 9.0 %collective-permute-start.2 = (bf16[256,256]{1,0:T(8,128)(2,1)S(1)}, bf16[256,256]{1,0:T(8,128)(2,1)S(1)}, u32[]{:S(2)}, u32[]{:S(2)}) collective-permute-start(bf16[256,256]{1,0:T(8,128)(2,1)S(1)} %copy-done), channel_id=1, source_target_pairs={{0,4},{2,6},{4,8},{6,10},{8,12},{10,14},{12,0},{14,2},{1,5},{3,7},... | collective-permute-start | bytes 393224 | tf_op jit(solution)/shard_map/ppermute | solution.py:220
  38.3 5.2 %copy-start.25 = (bf16[256,256]{1,0:T(8,128)(2,1)}, bf16[256,256]{1,0:T(8,128)(2,1)S(1)}, u32[]{:S(2)}) copy-start(bf16[256,256]{1,0:T(8,128)(2,1)S(1)} %collective-permute-done.refs_1_) | copy-start | bytes 393220
  38.3 5.2 %copy-start.27 = (bf16[256,256]{1,0:T(8,128)(2,1)}, bf16[256,256]{1,0:T(8,128)(2,1)S(1)}, u32[]{:S(2)}) copy-start(bf16[256,256]{1,0:T(8,128)(2,1)S(1)} %collective-permute-done.1.refs_2_) | copy-start | bytes 393220
  43.4 0.7 copy-start.28
  47.3 5.9 %copy-start.1 = (bf16[256,256]{1,0:T(8,128)(2,1)S(1)}, bf16[256,256]{1,0:T(8,128)(2,1)}, u32[]{:S(2)}) copy-start(bf16[256,256]{1,0:T(8,128)(2,1)} %cot_ref.3) | copy-start | bytes 393220
  47.3 36.1 %all-to-all-start.1 = ((bf16[16,56,1024]{2,1,0:T(8,128)(2,1)}), bf16[16,56,1024]{2,1,0:T(8,128)(2,1)S(1)}, u32[]{:S(2)}, u32[]{:S(2)}) async-start(bf16[16,56,1024]{2,1,0:T(8,128)(2,1)} %bitcast.40), calls=%async_computation.1 | async-start | bytes 3670016 | tf_op jit(solution)/shard_map/all_to_all | solution.py:296
  53.2 14.1 %collective-permute-start.3 = (bf16[256,256]{1,0:T(8,128)(2,1)S(1)}, bf16[256,256]{1,0:T(8,128)(2,1)S(1)}, u32[]{:S(2)}, u32[]{:S(2)}) collective-permute-start(bf16[256,256]{1,0:T(8,128)(2,1)S(1)} %copy-done.1), channel_id=1, source_target_pairs={{0,12},{2,14},{4,0},{6,2},{8,4},{10,6},{12,8},{14,10},{1,13},{3,15... | collective-permute-start | bytes 393224 | tf_op jit(solution)/shard_map/ppermute | solution.py:220
  53.8 15.5 %collective-permute-start.4 = (bf16[256,256]{1,0:T(8,128)(2,1)S(1)}, bf16[256,256]{1,0:T(8,128)(2,1)S(1)}, u32[]{:S(2)}, u32[]{:S(2)}) collective-permute-start(bf16[256,256]{1,0:T(8,128)(2,1)S(1)} %copy-done.1), channel_id=1, source_target_pairs={{0,6},{2,8},{4,10},{6,12},{8,14},{10,0},{12,2},{14,4},{1,7},{3,9},... | collective-permute-start | bytes 393224 | tf_op jit(solution)/shard_map/ppermute | solution.py:220
  54.0 20.4 %collective-permute-start.5 = (bf16[256,256]{1,0:T(8,128)(2,1)S(1)}, bf16[256,256]{1,0:T(8,128)(2,1)S(1)}, u32[]{:S(2)}, u32[]{:S(2)}) collective-permute-start(bf16[256,256]{1,0:T(8,128)(2,1)S(1)} %copy-done.1), channel_id=1, source_target_pairs={{0,10},{2,12},{4,14},{6,0},{8,2},{10,4},{12,6},{14,8},{1,11},{3,13... | collective-permute-start | bytes 393224 | tf_op jit(solution)/shard_map/ppermute | solution.py:220
  58.8 20.6 %collective-permute-start.6 = (bf16[256,256]{1,0:T(8,128)(2,1)S(1)}, bf16[256,256]{1,0:T(8,128)(2,1)S(1)}, u32[]{:S(2)}, u32[]{:S(2)}) collective-permute-start(bf16[256,256]{1,0:T(8,128)(2,1)S(1)} %copy-done.1), channel_id=1, source_target_pairs={{0,8},{2,10},{4,12},{6,14},{8,0},{10,2},{12,4},{14,6},{1,9},{3,11}... | collective-permute-start | bytes 393224 | tf_op jit(solution)/shard_map/ppermute | solution.py:220
  67.3 12.2 %copy-start.22 = (bf16[256,256]{1,0:T(8,128)(2,1)}, bf16[256,256]{1,0:T(8,128)(2,1)S(1)}, u32[]{:S(2)}) copy-start(bf16[256,256]{1,0:T(8,128)(2,1)S(1)} %collective-permute-done.3.refs_0_) | copy-start | bytes 393220
  69.3 10.2 %copy-start.23 = (bf16[256,256]{1,0:T(8,128)(2,1)}, bf16[256,256]{1,0:T(8,128)(2,1)S(1)}, u32[]{:S(2)}) copy-start(bf16[256,256]{1,0:T(8,128)(2,1)S(1)} %collective-permute-done.4.refs_1_) | copy-start | bytes 393220
  74.4 5.1 %copy-start.24 = (bf16[256,256]{1,0:T(8,128)(2,1)}, bf16[256,256]{1,0:T(8,128)(2,1)S(1)}, u32[]{:S(2)}) copy-start(bf16[256,256]{1,0:T(8,128)(2,1)S(1)} %collective-permute-done.5.refs_2_) | copy-start | bytes 393220
  79.5 0.6 copy-start.26
  83.4 7.3 %copy-start.3 = (bf16[16,56,1024]{2,1,0:T(8,128)(2,1)}, bf16[16,56,1024]{2,1,0:T(8,128)(2,1)S(1)}, u32[]{:S(2)}) copy-start(bf16[16,56,1024]{2,1,0:T(8,128)(2,1)S(1)} %all-to-all-done.1) | copy-start | bytes 5505028
  83.4 27.1 %copy-start.30 = (s32[8]{0:T(128)S(1)}, s32[8]{0:T(128)}, u32[]{:S(2)}) copy-start(s32[8]{0:T(128)} %constant.35) | copy-start | bytes 100
  83.4 27.0 %all-to-all-start.2 = ((bf16[16,56,1024]{2,1,0:T(8,128)(2,1)}), bf16[16,56,1024]{2,1,0:T(8,128)(2,1)}, u32[]{:S(2)}, u32[]{:S(2)}) async-start(bf16[16,56,1024]{2,1,0:T(8,128)(2,1)} %bitcast.41), calls=%async_computation.2 | async-start | bytes 3670016 | tf_op jit(solution)/shard_map/all_to_all | solution.py:296
  90.6 113.5 %reduce-scatter.2.cloned.1.call-start = ((), (), s32[]{:S(2)}) async-start(), calls=%async_computation.6 | async-start | bytes 8912896 | tf_op jit(solution)/shard_map/reduce_scatter | solution.py:341
  90.7 20.4 %collective-permute-start.7 = (bf16[896,1024]{1,0:T(8,128)(2,1)S(1)}, bf16[896,1024]{1,0:T(8,128)(2,1)}, u32[]{:S(2)}, u32[]{:S(2)}) collective-permute-start(bf16[896,1024]{1,0:T(8,128)(2,1)S(1)} %bitcast.37), channel_id=1, source_target_pairs={{0,1},{1,0},{2,3},{3,2},{4,5},{5,4},{6,7},{7,6},{8,9},{9,8},{10,11... | collective-permute-start | bytes 5505032 | tf_op jit(solution)/shard_map/ppermute | solution.py:299
  110.5 4.1 %collective-permute-start.8 = (bf16[896,1024]{1,0:T(8,128)(2,1)}, bf16[896,1024]{1,0:T(8,128)(2,1)}, u32[]{:S(2)}, u32[]{:S(2)}) collective-permute-start(bf16[896,1024]{1,0:T(8,128)(2,1)} %bitcast.9.mh_ref), channel_id=1, source_target_pairs={{0,1},{1,0},{2,3},{3,2},{4,5},{5,4},{6,7},{7,6},{8,9},{9,8},{10,11... | collective-permute-start | bytes 5505032 | tf_op jit(solution)/shard_map/ppermute | solution.py:299
  129.7 0.8 copy-start.20
  129.7 1.0 copy-start.19
  129.7 4.6 %copy-start.29 = (f32[3,128]{1,0:T(4,128)S(1)}, f32[3,128]{1,0:T(4,128)}, u32[]{:S(2)}) copy-start(f32[3,128]{1,0:T(4,128)} %param.16) | copy-start | bytes 4612
  129.7 9.7 %copy-start.21 = (bf16[128,256]{1,0:T(8,128)(2,1)S(1)}, bf16[128,256]{1,0:T(8,128)(2,1)}, u32[]{:S(2)}) copy-start(bf16[128,256]{1,0:T(8,128)(2,1)} %outer_ref.1) | copy-start | bytes 196612
  131.1 8.3 %collective-permute-start.9 = (bf16[2,128,2]{2,1,0:T(8,128)(2,1)S(1)}, bf16[2,128,2]{2,1,0:T(8,128)(2,1)S(1)}, u32[]{:S(2)}, u32[]{:S(2)}) collective-permute-start(bf16[2,128,2]{2,1,0:T(8,128)(2,1)S(1)} %copy.23), channel_id=1, source_target_pairs={{0,16},{16,32},{32,48},{48,64},{64,80},{80,96},{96,112},{112,128},... | collective-permute-start | bytes 3080 | tf_op jit(solution)/shard_map/ppermute | solution.py:227
  140.3 78.9 %copy-start.2 = (bf16[1024,256]{1,0:T(8,128)(2,1)S(1)}, bf16[1024,256]{1,0:T(8,128)(2,1)}, u32[]{:S(2)}) copy-start(bf16[1024,256]{1,0:T(8,128)(2,1)} %get-tuple-element.40.pick_ref) | copy-start | bytes 1572868
  220.3 7.4 %collective-permute-start.10 = (bf16[256,256]{1,0:T(8,128)(2,1)}, bf16[256,256]{1,0:T(8,128)(2,1)S(1)}, u32[]{:S(2)}, u32[]{:S(2)}) collective-permute-start(bf16[256,256]{1,0:T(8,128)(2,1)} %combine.1.refs_0_), channel_id=1, source_target_pairs={{0,2},{2,4},{4,6},{6,8},{8,10},{10,12},{12,14},{14,0},{1,3},{3,5},... | collective-permute-start | bytes 393224 | tf_op jit(solution)/shard_map/ppermute | solution.py:220
  220.3 12.4 %collective-permute-start.11 = (bf16[256,256]{1,0:T(8,128)(2,1)}, bf16[256,256]{1,0:T(8,128)(2,1)S(1)}, u32[]{:S(2)}, u32[]{:S(2)}) collective-permute-start(bf16[256,256]{1,0:T(8,128)(2,1)} %combine.1.refs_0_), channel_id=1, source_target_pairs={{0,14},{2,0},{4,2},{6,4},{8,6},{10,8},{12,10},{14,12},{1,15},{3,1}... | collective-permute-start | bytes 393224 | tf_op jit(solution)/shard_map/ppermute | solution.py:220
  223.5 12.5 %collective-permute-start.12 = (bf16[256,256]{1,0:T(8,128)(2,1)}, bf16[256,256]{1,0:T(8,128)(2,1)S(1)}, u32[]{:S(2)}, u32[]{:S(2)}) collective-permute-start(bf16[256,256]{1,0:T(8,128)(2,1)} %combine.1.refs_0_), channel_id=1, source_target_pairs={{0,4},{2,6},{4,8},{6,10},{8,12},{10,14},{12,0},{14,2},{1,5},{3,7},... | collective-permute-start | bytes 393224 | tf_op jit(solution)/shard_map/ppermute | solution.py:220
  223.5 12.5 %collective-permute-start.13 = (bf16[256,256]{1,0:T(8,128)(2,1)}, bf16[256,256]{1,0:T(8,128)(2,1)S(1)}, u32[]{:S(2)}, u32[]{:S(2)}) collective-permute-start(bf16[256,256]{1,0:T(8,128)(2,1)} %combine.1.refs_0_), channel_id=1, source_target_pairs={{0,12},{2,14},{4,0},{6,2},{8,4},{10,6},{12,8},{14,10},{1,13},{3,15... | collective-permute-start | bytes 393224 | tf_op jit(solution)/shard_map/ppermute | solution.py:220
  227.6 16.4 %collective-permute-start.14 = (bf16[256,256]{1,0:T(8,128)(2,1)}, bf16[256,256]{1,0:T(8,128)(2,1)S(1)}, u32[]{:S(2)}, u32[]{:S(2)}) collective-permute-start(bf16[256,256]{1,0:T(8,128)(2,1)} %combine.1.refs_0_), channel_id=1, source_target_pairs={{0,6},{2,8},{4,10},{6,12},{8,14},{10,0},{12,2},{14,4},{1,7},{3,9},... | collective-permute-start | bytes 393224 | tf_op jit(solution)/shard_map/ppermute | solution.py:220
  227.6 20.7 %copy-start.4 = (bf16[256,256]{1,0:T(8,128)(2,1)}, bf16[256,256]{1,0:T(8,128)(2,1)S(1)}, u32[]{:S(2)}) copy-start(bf16[256,256]{1,0:T(8,128)(2,1)S(1)} %collective-permute-done.10.refs_1_) | copy-start | bytes 393220
  227.6 18.3 %collective-permute-start.15 = (bf16[256,256]{1,0:T(8,128)(2,1)}, bf16[256,256]{1,0:T(8,128)(2,1)S(1)}, u32[]{:S(2)}, u32[]{:S(2)}) collective-permute-start(bf16[256,256]{1,0:T(8,128)(2,1)} %combine.1.refs_0_), channel_id=1, source_target_pairs={{0,10},{2,12},{4,14},{6,0},{8,2},{10,4},{12,6},{14,8},{1,11},{3,13... | collective-permute-start | bytes 393224 | tf_op jit(solution)/shard_map/ppermute | solution.py:220
  232.7 15.7 %copy-start.5 = (bf16[256,256]{1,0:T(8,128)(2,1)}, bf16[256,256]{1,0:T(8,128)(2,1)S(1)}, u32[]{:S(2)}) copy-start(bf16[256,256]{1,0:T(8,128)(2,1)S(1)} %collective-permute-done.11.refs_2_) | copy-start | bytes 393220
  232.7 13.3 %collective-permute-start.16 = (bf16[256,256]{1,0:T(8,128)(2,1)}, bf16[256,256]{1,0:T(8,128)(2,1)S(1)}, u32[]{:S(2)}, u32[]{:S(2)}) collective-permute-start(bf16[256,256]{1,0:T(8,128)(2,1)} %combine.1.refs_0_), channel_id=1, source_target_pairs={{0,8},{2,10},{4,12},{6,14},{8,0},{10,2},{12,4},{14,6},{1,9},{3,11}... | collective-permute-start | bytes 393224 | tf_op jit(solution)/shard_map/ppermute | solution.py:220
  236.0 12.4 %copy-start.6 = (bf16[256,256]{1,0:T(8,128)(2,1)}, bf16[256,256]{1,0:T(8,128)(2,1)S(1)}, u32[]{:S(2)}) copy-start(bf16[256,256]{1,0:T(8,128)(2,1)S(1)} %collective-permute-done.12.refs_3_) | copy-start | bytes 393220
  236.0 10.5 %collective-permute-start.17 = (bf16[256,256]{1,0:T(8,128)(2,1)}, bf16[256,256]{1,0:T(8,128)(2,1)S(1)}, u32[]{:S(2)}, u32[]{:S(2)}) collective-permute-start(bf16[256,256]{1,0:T(8,128)(2,1)} %combine.1.refs_0_), channel_id=1, source_target_pairs={{0,1},{1,0},{2,3},{3,2},{4,5},{5,4},{6,7},{7,6},{8,9},{9,8},{10,11... | collective-permute-start | bytes 393224 | tf_op jit(solution)/shard_map/ppermute | solution.py:403
  236.0 12.3 %copy-start.7 = (bf16[256,256]{1,0:T(8,128)(2,1)}, bf16[256,256]{1,0:T(8,128)(2,1)S(1)}, u32[]{:S(2)}) copy-start(bf16[256,256]{1,0:T(8,128)(2,1)S(1)} %collective-permute-done.13.refs_4_) | copy-start | bytes 393220
  236.0 10.6 %collective-permute-start.18 = (bf16[256,256]{1,0:T(8,128)(2,1)S(1)}, bf16[256,256]{1,0:T(8,128)(2,1)S(1)}, u32[]{:S(2)}, u32[]{:S(2)}) collective-permute-start(bf16[256,256]{1,0:T(8,128)(2,1)S(1)} %collective-permute-done.10.refs_1_), channel_id=1, source_target_pairs={{0,1},{1,0},{2,3},{3,2},{4,5},{5,4},{6,7},{7,6},{8,9},{9,8},{10,11... | collective-permute-start | bytes 393224 | tf_op jit(solution)/shard_map/ppermute | solution.py:403
  244.0 4.3 %copy-start.8 = (bf16[256,256]{1,0:T(8,128)(2,1)}, bf16[256,256]{1,0:T(8,128)(2,1)S(1)}, u32[]{:S(2)}) copy-start(bf16[256,256]{1,0:T(8,128)(2,1)S(1)} %collective-permute-done.14.refs_5_) | copy-start | bytes 393220
  244.0 3.0 %collective-permute-start.19 = (bf16[256,256]{1,0:T(8,128)(2,1)S(1)}, bf16[256,256]{1,0:T(8,128)(2,1)S(1)}, u32[]{:S(2)}, u32[]{:S(2)}) collective-permute-start(bf16[256,256]{1,0:T(8,128)(2,1)S(1)} %collective-permute-done.11.refs_2_), channel_id=1, source_target_pairs={{0,1},{1,0},{2,3},{3,2},{4,5},{5,4},{6,7},{7,6},{8,9},{9,8},{10,11... | collective-permute-start | bytes 393224 | tf_op jit(solution)/shard_map/ppermute | solution.py:403
  246.0 2.4 copy-start.9
  246.0 1.3 collective-permute-start.20
  246.0 2.4 copy-start.10
  246.0 1.5 collective-permute-start.21
  246.5 1.9 copy-start.11
  246.5 1.3 collective-permute-start.22
  246.6 1.8 copy-start.12
  246.6 1.4 collective-permute-start.23
  247.0 1.4 copy-start.13
  247.0 1.3 collective-permute-start.24
  247.3 1.1 copy-start.14
  247.5 1.0 copy-start.15
  247.8 0.6 copy-start.16
  248.0 0.6 copy-start.17
  248.7 0.7 copy-start.18
  252.4 23.7 %all-to-all-start.4 = ((bf16[16,128,256]{2,1,0:T(8,128)(2,1)}), bf16[16,128,256]{2,1,0:T(8,128)(2,1)S(1)}, u32[]{:S(2)}, u32[]{:S(2)}) async-start(bf16[16,128,256]{2,1,0:T(8,128)(2,1)} %proj.1), calls=%async_computation.5 | async-start | bytes 2097152 | tf_op jit(solution)/shard_map/all_to_all | solution.py:413
  262.6 11.1 %collective-permute-start.25 = (f32[128,2]{1,0:T(8,128)S(1)}, f32[128,2]{1,0:T(8,128)S(1)}, u32[]{:S(2)}, u32[]{:S(2)}) collective-permute-start(f32[128,2]{1,0:T(8,128)S(1)} %slice.60), channel_id=1, source_target_pairs={{16,0},{32,16},{48,32},{64,48},{80,64},{96,80},{112,96},{128,112},... | collective-permute-start | bytes 3080 | tf_op jit(solution)/shard_map/ppermute | solution.py:227
Sparse Core Ops, SparseCore 0:
  28.5 79.4 all-gather.2
  129.9 74.1 reduce-scatter.1
